TPU v7x, 128 devices: a whole 4x4x4 slice. The times are simulated.
128 devices in a mesh: sp: 16 (over z, y), tp: 8 (over x, core).
Axes of the slice: x: 4, y: 4, z: 4, core: 2. Of those that a mesh axis runs over, the one named last changes fastest.
Arguments:
- hidden_activations: bfloat16 [12288, 4096], P(('sp', 'tp')), may hold values from -6 to 6
- entry_rescale_vector: bfloat16 [4096], replicated, may hold values from 0.099609375 to 1.8984375
- probe_matrix: bfloat16 [4096, 2048], P('sp', 'tp'), may hold values from -0.09375 to 0.09375
- lookup_address_matrix: bfloat16 [4096, 2048], P('sp', 'tp'), may hold values from -0.09375 to 0.09375
- payload_matrix: bfloat16 [4096, 4096], P('sp', 'tp'), may hold values from -0.09375 to 0.09375
- postfilter_switch_matrix: bfloat16 [4096, 4096], P('sp', 'tp'), may hold values from -0.09375 to 0.09375
- prefilter_switch_matrix: bfloat16 [4096, 4096], P('sp', 'tp'), may hold values from -0.09375 to 0.09375
- filter_source_matrix: bfloat16 [4096, 4096], P('sp', 'tp'), may hold values from -0.09375 to 0.09375
- forget_left_factor: bfloat16 [4096, 64], replicated, may hold values from -0.09375 to 0.09375
- forget_right_factor: bfloat16 [64, 2048], P(None, 'tp'), may hold values from -0.75 to 0.75
- forget_offset_per_feature: float32 [2048], P('tp'), may hold values from -1 to 12
- forget_spike_additions: float32 [16, 12288], P('tp', 'sp'), may hold values from -3 to 0
- subspace_rescale_vector: bfloat16 [16, 256], P('tp'), may hold values from 0.099609375 to 1.8984375
- depthwise_filter_taps: bfloat16 [3, 4096], P(None, 'tp'), may hold values from -3.5 to 3.5
- mixer_result_matrix: bfloat16 [4096, 4096], P('tp'), may hold values from -0.09375 to 0.09375
- filter_result_matrix: bfloat16 [4096, 4096], P('tp'), may hold values from -0.09375 to 0.09375
Outputs:
- mixed: bfloat16 [12288, 4096], P(('sp', 'tp'))
All inputs are finite; a program needn't handle non-finite values.
Results may differ from a plain program's by a relative error of at most 0.02.
Values may be sent and summed in bfloat16 or wider, within the bound.
No kernel may reach another device: no remote copies, remote signals or barrier semaphores. Data moves between devices by JAX's collectives and lax.ppermute only.
A program may use at most 128 MiB of HBM per device.

v0:
```python
import functools

import jax
import jax.numpy as jnp
from jax import lax
from jax.experimental import pallas as pl
from jax.experimental.pallas import tpu as pltpu
from jax.sharding import Mesh
from jax.sharding import PartitionSpec as P

BLOCK = 64
SP = ("z", "y")
TP = ("x", "c")
ALL = ("z", "y", "x", "c")
RING = 4
PAIR = 2
HALO = 16

EPSILON = 1e-06
SOFTNESS = 16.0

F32 = jnp.float32
BF16 = jnp.bfloat16


def dot(a, b):
    return jnp.dot(a, b, preferred_element_type=F32)


def hop(value, axis, steps):
    return lax.ppermute(value, axis, [(i, (i + steps) % RING) for i in range(RING)])


def swap(value):
    return lax.ppermute(value, "c", [(0, 1), (1, 0)])


def onward(value, axis, steps):
    count = RING * RING if axis == SP else RING
    return lax.ppermute(value, axis, [(i, i + steps) for i in range(count - steps)])


def around(value, axis, half=None):
    half = half or value.shape[0] // 2
    below, above = hop(value, axis, 1), hop(value, axis, -1)
    top = hop(below[:half], axis, 1)
    bottom = hop(above[half:], axis, -1)
    return value, below, above, top, bottom


def vmem_kernel(kernel, out_shape, flops, *args, **kwargs):
    return pl.pallas_call(
        kernel,
        out_shape=out_shape,
        compiler_params=pltpu.CompilerParams(vmem_limit_bytes=kwargs.pop("limit", 16) << 20),
        cost_estimate=pl.CostEstimate(
            flops=flops, bytes_accessed=8_000_000, transcendentals=0
        ),
        **kwargs,
    )(*args)


def line_kernel(axis, own, below, above, top, bottom, *outs):
    me = lax.axis_index(axis)
    rows = own.shape[0]
    half = rows // 2
    at = 0
    for out in outs:
        cols = slice(at, at + out.shape[1])
        at += out.shape[1]
        for ref, step, offset in (
            (own, 0, 0),
            (below, 3, 0),
            (above, 1, 0),
            (top, 2, 0),
            (bottom, 2, half),
        ):
            start = pl.multiple_of(lax.rem(me + step, RING) * rows + offset, half)
            out[pl.ds(start, ref.shape[0]), :] = ref[:, cols]


def line_up(axis, pieces, widths):
    rows = pieces[0].shape[0] * RING
    return vmem_kernel(
        functools.partial(line_kernel, axis),
        tuple(jax.ShapeDtypeStruct((rows, w), BF16) for w in widths),
        1_000_000_000,
        *pieces,
    )


def chips_kernel(own, below, above, top, bottom, out):
    x = lax.axis_index("x")
    rows = own.shape[0]
    half = top.shape[0]
    for ref, step, offset in (
        (own, 0, 0),
        (below, 3, 0),
        (above, 1, 0),
        (top, 2, 0),
        (bottom, 2, half),
    ):
        start = pl.multiple_of(lax.rem(x + step, RING) * rows + offset, HALO)
        out[pl.ds(start, ref.shape[0]), :] = ref[...]


def rows_kernel(mine, other, out):
    c = lax.axis_index("c")
    block = mine.shape[0] // RING
    part = block - HALO
    for ref, core in ((mine, c), (other, 1 - c)):
        for chip in range(RING):
            start = pl.multiple_of(HALO + (chip * PAIR + core) * part, HALO)
            out[pl.ds(start, part), :] = ref[chip * block : chip * block + part]

        @pl.when(core == 1)
        def _(ref=ref):
            out[:HALO] = ref[RING * block - HALO :]


def gather_rows(shard):
    block, width = shard.shape
    part = block - HALO
    pieces = around(shard, "x", part // 2)
    mine = vmem_kernel(
        chips_kernel, jax.ShapeDtypeStruct((RING * block, width), BF16), 1_000_000_000, *pieces
    )
    return vmem_kernel(
        rows_kernel,
        jax.ShapeDtypeStruct((HALO + RING * PAIR * part, width), BF16),
        2_000_000_000,
        mine,
        swap(mine),
    )


def project(x_ref, lead, along, pieces, which, block):
    me = lax.axis_index("z" if along == 0 else "y")
    total = None
    for ref, index in zip(pieces, which):
        step, first = ((0, 0), (3, 0), (1, 0), (2, 0), (2, 2))[index]
        where = lax.rem(me + step, RING)
        count = ref.shape[0] // block
        if along == 0:
            start = pl.multiple_of((where * RING + first) * block, block)
            term = dot(x_ref[lead:, pl.ds(start, count * block)], ref[...])
            total = term if total is None else total + term
        else:
            for i in range(count):
                start = pl.multiple_of(((first + i) * RING + where) * block, block)
                term = dot(
                    x_ref[lead:, pl.ds(start, block)], ref[i * block : (i + 1) * block, :]
                )
                total = term if total is None else total + term
    return total


def project_kernel(lead, along, which, block, x_ref, *refs):
    *pieces, out = refs
    out[...] = project(x_ref, lead, along, pieces, which, block).astype(out.dtype)


def project_more_kernel(lead, along, which, block, x_ref, acc_ref, *refs):
    *pieces, out = refs
    total = acc_ref[...] + project(x_ref, lead, along, pieces, which, block)
    out[...] = total.astype(out.dtype)


def project_call(x, acc, pieces, which, along, lead, dtype, tile=256):
    block = x.shape[1] // (RING * RING)
    rows = x.shape[0] - lead
    width = pieces[0].shape[1]
    more = () if acc is None else (acc,)
    kernel = project_kernel if acc is None else project_more_kernel
    return vmem_kernel(
        functools.partial(kernel, lead, along, which, block),
        jax.ShapeDtypeStruct((rows, width), dtype),
        3_000_000_000,
        x,
        *more,
        *pieces,
        grid=(width // tile,),
        in_specs=[pl.BlockSpec(memory_space=pltpu.VMEM)]
        + [pl.BlockSpec((rows, tile), lambda i: (0, i)) for _ in more]
        + [pl.BlockSpec((p.shape[0], tile), lambda i: (0, i)) for p in pieces],
        out_specs=pl.BlockSpec((rows, tile), lambda i: (0, i)),
    )


def gate_kernel(along, which, block, x_ref, acc_ref, *refs):
    *pieces, taps_ref, out = refs
    sums = (acc_ref[...] + project(x_ref, 0, along, pieces, which, block)).astype(BF16)
    width = sums.shape[1] // 3
    length = sums.shape[0] - HALO
    gated = (sums[:, width : 2 * width].astype(F32) * sums[:, 2 * width :].astype(F32)).astype(BF16)
    gated = gated.astype(F32)
    taps = taps_ref.shape[0]
    conv = jnp.zeros((length, width), F32)
    for i in range(taps):
        lead = HALO + 1 - taps + i
        conv = conv + taps_ref[i : i + 1, :].astype(F32) * gated[lead : lead + length]
    out[...] = (conv * sums[HALO:, :width].astype(F32)).astype(BF16)


def gate_call(x, acc, pieces, which, taps, along):
    block = x.shape[1] // (RING * RING)
    return vmem_kernel(
        functools.partial(gate_kernel, along, which, block),
        jax.ShapeDtypeStruct((x.shape[0] - HALO, taps.shape[1]), BF16),
        2_000_000_000,
        x,
        acc,
        *pieces,
        taps,
        in_specs=[pl.BlockSpec(memory_space=pltpu.VMEM)] * (3 + len(pieces)),
        out_specs=pl.BlockSpec(memory_space=pltpu.VMEM),
    )


def norm_values(rows, gain):
    rows_f = rows.astype(F32)
    meansq = jnp.mean(rows_f * rows_f, axis=-1, keepdims=True)
    return rows_f * lax.rsqrt(meansq + EPSILON) * gain.astype(F32)


def decay_kernel(
    x_ref, left_ref, right_ref, offset_ref, spike_ref, in_ref, out_ref, tail_ref, far_ref, end_ref, total_ref
):
    length, width = in_ref.shape
    heads = spike_ref.shape[0]
    low_rank = across(x_ref[HALO:, :], left_ref[...]).astype(BF16)
    gate = dot(low_rank, right_ref[...]) + offset_ref[...]
    soft = jnp.minimum(gate, 0.0) - jnp.log1p(jnp.exp(-jnp.abs(gate)))
    head = lax.broadcasted_iota(jnp.int32, (heads, width), 0)
    feature = lax.broadcasted_iota(jnp.int32, (heads, width), 1)
    owner = jnp.where(feature // (width // heads) == head, 1.0, 0.0).astype(F32)
    spikes = lax.dot_general(
        spike_ref[...],
        owner,
        (((0,), (0,)), ((), ())),
        preferred_element_type=F32,
        precision=lax.Precision.HIGHEST,
    )
    rate = soft / SOFTNESS + spikes
    low = lax.broadcasted_iota(jnp.int32, (BLOCK, BLOCK), 0)
    high = lax.broadcasted_iota(jnp.int32, (BLOCK, BLOCK), 1)
    tri = jnp.where(high <= low, 1.0, 0.0).astype(F32)
    prefix = jnp.zeros((1, width), F32)
    tail_ref[...] = rate

    def step(n, prefix):
        rows = pl.ds(pl.multiple_of(n * BLOCK, BLOCK), BLOCK)
        within = jnp.dot(
            tri, tail_ref[rows, :], preferred_element_type=F32, precision=lax.Precision.HIGHEST
        )
        end = within[BLOCK - 1 :]
        grow = jnp.exp(within)
        in_ref[rows, :] = grow
        out_ref[rows, :] = jnp.exp(-within)
        tail_ref[rows, :] = jnp.exp(end - within)
        far_ref[rows, :] = grow * jnp.exp(prefix)
        end_ref[pl.ds(n, 1), :] = jnp.exp(end)
        return prefix + end

    total_ref[...] = jnp.exp(lax.fori_loop(0, length // BLOCK, step, prefix))


def decay_terms(x, left, right, offset, spike):
    length, width = x.shape[0] - HALO, right.shape[1]
    full = jax.ShapeDtypeStruct((length, width), F32)
    return vmem_kernel(
        decay_kernel,
        (
            full,
            full,
            full,
            full,
            jax.ShapeDtypeStruct((length // BLOCK, width), F32),
            jax.ShapeDtypeStruct((1, width), F32),
        ),
        4_000_000_000,
        x,
        jnp.transpose(left),
        right,
        offset[None],
        spike,
        in_specs=[pl.BlockSpec(memory_space=pltpu.VMEM)] * 5,
    )


def across(a, b):
    return lax.dot_general(a, b, (((1,), (1,)), ((), ())), preferred_element_type=F32)


def local_kernel(qk_ref, v_ref, in_ref, out_ref, tail_ref, far_ref, end_ref, part_ref, qfar_ref, state_ref):
    length = qk_ref.shape[0]
    heads = state_ref.shape[0]
    key_dim = qk_ref.shape[1] // heads // 2
    value_dim = v_ref.shape[1] // heads
    scale = key_dim ** (-0.5)
    low = lax.broadcasted_iota(jnp.int32, (BLOCK, BLOCK), 0)
    high = lax.broadcasted_iota(jnp.int32, (BLOCK, BLOCK), 1)
    causal = high <= low
    states = [jnp.zeros((value_dim, key_dim), F32) for _ in range(heads)]
    for n in range(length // BLOCK):
        rows = slice(n * BLOCK, (n + 1) * BLOCK)
        for h in range(heads):
            keys = slice(h * key_dim, (h + 1) * key_dim)
            values = slice(h * value_dim, (h + 1) * value_dim)
            q = qk_ref[rows, keys].astype(F32) * scale
            k = qk_ref[rows, heads * key_dim + h * key_dim : heads * key_dim + (h + 1) * key_dim].astype(F32)
            v = v_ref[rows, values]
            qd = (q * in_ref[rows, keys]).astype(BF16)
            ki = (k * out_ref[rows, keys]).astype(BF16)
            kt = (k * tail_ref[rows, keys]).astype(BF16)
            qfar_ref[rows, keys] = (q * far_ref[rows, keys]).astype(BF16)
            scores = jnp.where(causal, across(qd, ki), 0.0).astype(BF16)
            part = dot(scores, v)
            if n > 0:
                part = part + across(qd, states[h].astype(BF16))
            part_ref[rows, values] = part
            update = lax.dot_general(v, kt, (((0,), (0,)), ((), ())), preferred_element_type=F32)
            states[h] = states[h] * end_ref[n : n + 1, keys] + update
    for h in range(heads):
        state_ref[h] = states[h]


def local_attention(qk, v, terms, heads):
    length, width = qk.shape[0], qk.shape[1] // 2
    wide = v.shape[1]
    return vmem_kernel(
        local_kernel,
        (
            jax.ShapeDtypeStruct((length, wide), F32),
            jax.ShapeDtypeStruct((length, width), BF16),
            jax.ShapeDtypeStruct((heads, wide // heads, width // heads), F32),
        ),
        6_000_000_000,
        qk,
        v,
        *terms,
        in_specs=[pl.BlockSpec(memory_space=pltpu.VMEM)] * (2 + len(terms)),
    )


def finish_kernel(part_ref, qfar_ref, state_ref, gain_ref, mixed_ref):
    heads = state_ref.shape[0]
    key_dim = qfar_ref.shape[1] // heads
    value_dim = part_ref.shape[1] // heads
    for h in range(heads):
        keys = slice(h * key_dim, (h + 1) * key_dim)
        values = slice(h * value_dim, (h + 1) * value_dim)
        attended = part_ref[:, values] + across(qfar_ref[:, keys], state_ref[h])
        meansq = jnp.mean(attended * attended, axis=-1, keepdims=True)
        gain = gain_ref[h : h + 1].astype(F32)
        mixed_ref[:, values] = (attended * lax.rsqrt(meansq + EPSILON) * gain).astype(BF16)


def finish_attention(part, qfar, state, gain):
    length, wide = part.shape
    return vmem_kernel(
        finish_kernel,
        jax.ShapeDtypeStruct((length, wide), BF16),
        3_000_000_000,
        part,
        qfar,
        state,
        gain,
        in_specs=[pl.BlockSpec(memory_space=pltpu.VMEM)] * 4,
    )


def unpack(packed, value_dim):
    packed = packed.astype(F32)
    return packed[:, value_dim : value_dim + 1], packed[:, :value_dim]


def combine(earlier, later):
    return earlier[0] * later[0], later[0] * earlier[1] + later[1]


def pack(pair):
    decay, state = pair
    heads, _, key_dim = state.shape
    lines = jnp.broadcast_to(decay, (heads, 16, key_dim))
    return jnp.concatenate([state, lines], axis=1).astype(BF16)


def entering(decay, state):
    value_dim = state.shape[1]
    z, y = lax.axis_index("z"), lax.axis_index("y")
    own = pack((decay, state))
    empty = (jnp.ones_like(decay), jnp.zeros_like(state))

    def only(passed, pair):
        return tuple(jnp.where(passed, a, b) for a, b in zip(pair, empty))

    before = empty
    total = (decay, state)
    got = [unpack(hop(own, "y", step), value_dim) for step in (1, 2, 3)]
    for step in (1, 2, 3):
        pair = got[step - 1]
        before = combine(only(y >= step, pair), before)
    after = empty
    for step in (3, 2, 1):
        after = combine(after, only(y < step, got[step - 1]))
    total = combine(combine(before, total), after)
    line = pack(total)
    outer = empty
    for step in (1, 2, 3):
        pair = unpack(onward(line, "z", step), value_dim)
        outer = combine(only(z >= step, pair), outer)
    return combine(outer, before)[1].astype(BF16)


def term_kernel(step, attn_ref, t_ref, b_ref, mixer_ref, filter_ref, own_ref, other_ref):
    x, c = lax.axis_index("x"), lax.axis_index("c")
    part = own_ref.shape[0]
    base = lax.rem(x + step, RING) * PAIR * part
    spots = [pl.multiple_of(base + core * part, HALO) for core in (1 - c, c)]
    half = t_ref.shape[1]
    out = None
    for ref, matrix in (
        (attn_ref, mixer_ref[...]),
        (t_ref, filter_ref[:half]),
        (b_ref, filter_ref[half:]),
    ):
        rows = jnp.concatenate([ref[pl.ds(at, part), :] for at in spots], axis=0)
        term = dot(rows, matrix)
        out = term if out is None else out + term
    other_ref[...] = out[:part].astype(BF16)
    own_ref[...] = out[part:]


def term_call(step, attn, t, b, mixer, filt, part):
    width = mixer.shape[1]
    tile = 1024
    whole = pl.BlockSpec(memory_space=pltpu.VMEM)
    return vmem_kernel(
        functools.partial(term_kernel, step),
        (
            jax.ShapeDtypeStruct((part, width), F32),
            jax.ShapeDtypeStruct((part, width), BF16),
        ),
        2_000_000_000,
        attn,
        t,
        b,
        mixer,
        filt,
        grid=(width // tile,),
        in_specs=[whole, whole, whole]
        + [pl.BlockSpec((m.shape[0], tile), lambda i: (0, i)) for m in (mixer, filt)],
        out_specs=(
            pl.BlockSpec((part, tile), lambda i: (0, i)),
            pl.BlockSpec((part, tile), lambda i: (0, i)),
        ),
    )


def plus(*terms):
    total = terms[0].astype(F32)
    for term in terms[1:]:
        total = total + term.astype(F32)
    return total


def body(
    hidden,
    entry_gain,
    probe,
    lookup,
    payload,
    postfilter,
    prefilter,
    source,
    forget_left,
    forget_right,
    forget_offset,
    forget_spike,
    head_gain,
    taps,
    mixer_result,
    filter_result,
):
    heads, value_dim = head_gain.shape
    key_dim = probe.shape[1] // heads
    channels = taps.shape[1]
    half = channels // 2
    keys, values = 2 * heads * key_dim, heads * value_dim

    def shard(attn, cols):
        convs = [w[:, cols] for w in (postfilter, prefilter, source)]
        return jnp.concatenate(attn + convs, axis=1)

    tops = shard([probe, lookup], slice(0, half))
    bottoms = shard([payload], slice(half, channels))
    first = around(tops, "z")
    second = around(bottoms, "y")
    normed = norm_values(hidden, entry_gain).astype(BF16)
    part = normed.shape[0]
    rim = onward(normed[part - HALO :], SP, 1)
    x = gather_rows(jnp.concatenate([normed, rim], axis=0))

    line_qk, line_t = line_up("z", first, (keys, 3 * half))
    line_v, line_b = line_up("y", second, (values, 3 * half))
    w_qk = around(line_qk, "y")
    w_v = around(line_v, "z")
    w_t = around(line_t, "y")
    w_b = around(line_b, "z")

    *terms, total = decay_terms(x, forget_left, forget_right, forget_offset, forget_spike)
    total = total.reshape(heads, 1, key_dim)
    early, late = (0, 1, 2), (3, 4)
    acc_qk = project_call(x, None, w_qk[:3], early, 1, HALO, F32)
    acc_v = project_call(x, None, w_v[:3], early, 0, HALO, F32)
    qk = project_call(x, acc_qk, w_qk[3:], late, 1, HALO, BF16)
    v = project_call(x, acc_v, w_v[3:], late, 0, HALO, BF16)
    near, qfar, state = local_attention(qk, v, terms, heads)
    incoming = entering(total, state)
    mixed_attn = finish_attention(near, qfar, incoming, head_gain)

    acc_t = project_call(x, None, w_t[:3], early, 1, 0, F32)
    acc_b = project_call(x, None, w_b[:3], early, 0, 0, F32)
    mixed_t = gate_call(x, acc_t, w_t[3:], late, taps[:, :half], 1)
    mixed_b = gate_call(x, acc_b, w_b[3:], late, taps[:, half:], 0)

    def partial(step):
        own, other = term_call(
            step, mixed_attn, mixed_t, mixed_b, mixer_result, filter_result, part
        )
        return plus(own, swap(other))

    cut = part // 2
    far = partial(2).astype(BF16)
    far_up, far_down = hop(far[:cut], "x", 1), hop(far[cut:], "x", -1)
    up, down = partial(1), partial(3)
    plain_up = hop(up[cut:].astype(BF16), "x", 1)
    plain_down = hop(down[:cut].astype(BF16), "x", -1)
    last_up = hop(plus(up[:cut], far_up).astype(BF16), "x", 1)
    last_down = hop(plus(down[cut:], far_down).astype(BF16), "x", -1)
    from_below = jnp.concatenate([last_up, plain_up], axis=0)
    from_above = jnp.concatenate([plain_down, last_down], axis=0)
    return plus(partial(0), from_below, from_above).astype(BF16)


def solution(mesh):
    split = Mesh(mesh.devices.reshape(RING, RING, RING, PAIR), ALL)
    in_specs = (
        P(ALL, None),
        P(),
        P(SP, TP),
        P(SP, TP),
        P(SP, TP),
        P(SP, TP),
        P(SP, TP),
        P(SP, TP),
        P(),
        P(None, TP),
        P(TP),
        P(TP, SP),
        P(TP, None),
        P(None, TP),
        P(TP, None),
        P(TP, None),
    )

    return jax.shard_map(
        body, mesh=split, in_specs=in_specs, out_specs=P(ALL, None), check_vma=False
    )
```

profile of v0, /device:TPU:1, one launch (start us, length us, event | category | flops | bytes accessed | tf_op | source)
XLA Modules:
  0.0 250.0 jit_solution(1881421709022138258)
XLA Ops:
  0.7 1.4 fusion
  2.1 1.4 fusion.2
  3.6 4.2 %collective-permute-start = (bf16[16,4096]{1,0:T(8,128)(2,1)S(1)}, bf16[16,4096]{1,0:T(8,128)(2,1)S(1)}, u32[]{:S(2)}, u32[]{:S(2)}) collective-permute-start(bf16[16,4096]{1,0:T(8,128)(2,1)S(1)} %slice.166), channel_id=1, source_target_pairs={{0,8},{8,16},{16,24},{24,32},{32,40},{40,48},{48,56},{56,64},{64,7... | collective-permute-start | bytes 393224 | tf_op jit(solution)/shard_map/ppermute | solution.py:40
  7.8 2.2 collective-permute-done
  10.0 2.5 %collective-permute-start.2 = (bf16[112,4096]{1,0:T(8,128)(2,1)S(1)}, bf16[112,4096]{1,0:T(8,128)(2,1)S(1)}, u32[]{:S(2)}, u32[]{:S(2)}) collective-permute-start(bf16[112,4096]{1,0:T(8,128)(2,1)S(1)} %pad_maximum_fusion.own), channel_id=1, source_target_pairs={{0,6},{2,0},{4,2},{6,4},{1,7},{3,1},{5,3},{7,5},{8,14},{10,8},{12,... | collective-permute-start | bytes 2752520 | tf_op jit(solution)/shard_map/ppermute | solution.py:31
  12.7 18.1 %collective-permute-done.2.above = bf16[112,4096]{1,0:T(8,128)(2,1)S(1)} collective-permute-done((bf16[112,4096]{1,0:T(8,128)(2,1)S(1)}, bf16[112,4096]{1,0:T(8,128)(2,1)S(1)}, u32[]{:S(2)}, u32[]{:S(2)}) %collective-permute-start.2) | collective-permute-done | bytes 917536 | tf_op jit(solution)/shard_map/ppermute | solution.py:31
  30.8 3.5 %collective-permute-start.4 = (bf16[64,4096]{1,0:T(8,128)(2,1)S(1)}, bf16[64,4096]{1,0:T(8,128)(2,1)S(1)}, u32[]{:S(2)}, u32[]{:S(2)}) collective-permute-start(bf16[64,4096]{1,0:T(8,128)(2,1)S(1)} %slice.168), channel_id=1, source_target_pairs={{0,6},{2,0},{4,2},{6,4},{1,7},{3,1},{5,3},{7,5},{8,14},{10,8},{12,... | collective-permute-start | bytes 1572872 | tf_op jit(solution)/shard_map/ppermute | solution.py:31
  34.5 2.3 collective-permute-start.14
  36.8 1.5 collective-permute-start.15
  38.3 3.6 %collective-permute-start.6 = (bf16[256,1280]{1,0:T(8,128)(2,1)S(1)}, bf16[256,1280]{1,0:T(8,128)(2,1)S(1)}, u32[]{:S(2)}, u32[]{:S(2)}) collective-permute-start(bf16[256,1280]{1,0:T(8,128)(2,1)S(1)} %get-tuple-element.64.own), channel_id=1, source_target_pairs={{0,32},{32,64},{64,96},{96,0},{1,33},{33,65},{65,97},{97,1},{2,34}... | collective-permute-start | bytes 1966088 | tf_op jit(solution)/shard_map/ppermute | solution.py:31
  41.9 1.7 collective-permute-done.3.top
  43.6 6.8 %collective-permute-start.7 = (bf16[256,1280]{1,0:T(8,128)(2,1)S(1)}, bf16[256,1280]{1,0:T(8,128)(2,1)S(1)}, u32[]{:S(2)}, u32[]{:S(2)}) collective-permute-start(bf16[256,1280]{1,0:T(8,128)(2,1)S(1)} %get-tuple-element.64.own), channel_id=1, source_target_pairs={{0,96},{32,0},{64,32},{96,64},{1,97},{33,1},{65,33},{97,65},{2,98}... | collective-permute-start | bytes 1966088 | tf_op jit(solution)/shard_map/ppermute | solution.py:31
  50.4 2.1 shard_map.154.mine
  52.4 3.8 %collective-permute-start.5 = (bf16[448,4096]{1,0:T(8,128)(2,1)}, bf16[448,4096]{1,0:T(8,128)(2,1)}, u32[]{:S(2)}, u32[]{:S(2)}) collective-permute-start(bf16[448,4096]{1,0:T(8,128)(2,1)} %shard_map.154.mine), channel_id=1, source_target_pairs={{0,1},{1,0},{2,3},{3,2},{4,5},{5,4},{6,7},{7,6},{8,9},{9,8},{10,11... | collective-permute-start | bytes 11010056 | tf_op jit(solution)/shard_map/ppermute | solution.py:35
  56.4 2.7 %collective-permute-start.17 = (bf16[128,1280]{1,0:T(8,128)(2,1)S(1)}, bf16[128,1280]{1,0:T(8,128)(2,1)S(1)}, u32[]{:S(2)}, u32[]{:S(2)}) collective-permute-start(bf16[128,1280]{1,0:T(8,128)(2,1)S(1)} %slice.174), channel_id=1, source_target_pairs={{0,24},{8,0},{16,8},{24,16},{1,25},{9,1},{17,9},{25,17},{2,26},{10... | collective-permute-start | bytes 983048 | tf_op jit(solution)/shard_map/ppermute | solution.py:31
  59.2 1.7 collective-permute-done.7.above
  61.0 3.5 %collective-permute-start.9 = (bf16[128,1280]{1,0:T(8,128)(2,1)S(1)}, bf16[128,1280]{1,0:T(8,128)(2,1)S(1)}, u32[]{:S(2)}, u32[]{:S(2)}) collective-permute-start(bf16[128,1280]{1,0:T(8,128)(2,1)S(1)} %slice.170), channel_id=1, source_target_pairs={{0,96},{32,0},{64,32},{96,64},{1,97},{33,1},{65,33},{97,65},{2,98}... | collective-permute-start | bytes 983048 | tf_op jit(solution)/shard_map/ppermute | solution.py:31
  64.4 2.4 collective-permute-done.16.top
  66.8 1.4 shard_map.159
  68.2 2.7 %collective-permute-start.19 = (bf16[1024,512]{1,0:T(8,128)(2,1)S(1)}, bf16[1024,512]{1,0:T(8,128)(2,1)S(1)}, u32[]{:S(2)}, u32[]{:S(2)}) collective-permute-start(bf16[1024,512]{1,0:T(8,128)(2,1)S(1)} %get-tuple-element.27.refs_0_), channel_id=1, source_target_pairs={{0,96},{32,0},{64,32},{96,64},{1,97},{33,1},{65,33},{97,65},{2,98}... | collective-permute-start | bytes 3145736 | tf_op jit(solution)/shard_map/ppermute | solution.py:31
  70.9 1.3 shard_map.156
  72.2 2.7 %collective-permute-start.11 = (bf16[1024,512]{1,0:T(8,128)(2,1)S(1)}, bf16[1024,512]{1,0:T(8,128)(2,1)}, u32[]{:S(2)}, u32[]{:S(2)}) collective-permute-start(bf16[1024,512]{1,0:T(8,128)(2,1)S(1)} %get-tuple-element.26.refs_0_), channel_id=1, source_target_pairs={{0,24},{8,0},{16,8},{24,16},{1,25},{9,1},{17,9},{25,17},{2,26},{10... | collective-permute-start | bytes 3145736 | tf_op jit(solution)/shard_map/ppermute | solution.py:31
  75.9 16.0 %collective-permute-done.18.refs_1_ = bf16[1024,512]{1,0:T(8,128)(2,1)S(1)} collective-permute-done((bf16[1024,512]{1,0:T(8,128)(2,1)S(1)}, bf16[1024,512]{1,0:T(8,128)(2,1)S(1)}, u32[]{:S(2)}, u32[]{:S(2)}) %collective-permute-start.18) | collective-permute-done | bytes 1048608 | tf_op jit(solution)/shard_map/ppermute | solution.py:31
  94.9 3.5 %collective-permute-start.33 = (bf16[1024,768]{1,0:T(8,128)(2,1)}, bf16[1024,768]{1,0:T(8,128)(2,1)S(1)}, u32[]{:S(2)}, u32[]{:S(2)}) collective-permute-start(bf16[1024,768]{1,0:T(8,128)(2,1)} %get-tuple-element.38.refs_0_), channel_id=1, source_target_pairs={{0,96},{32,0},{64,32},{96,64},{1,97},{33,1},{65,33},{97,65},{2,98}... | collective-permute-start | bytes 4718600 | tf_op jit(solution)/shard_map/ppermute | solution.py:31
  98.4 2.7 %collective-permute-start.29 = (bf16[1024,768]{1,0:T(8,128)(2,1)}, bf16[1024,768]{1,0:T(8,128)(2,1)}, u32[]{:S(2)}, u32[]{:S(2)}) collective-permute-start(bf16[1024,768]{1,0:T(8,128)(2,1)} %get-tuple-element.37.refs_0_), channel_id=1, source_target_pairs={{0,24},{8,0},{16,8},{24,16},{1,25},{9,1},{17,9},{25,17},{2,26},{10... | collective-permute-start | bytes 4718600 | tf_op jit(solution)/shard_map/ppermute | solution.py:31
  105.4 21.0 %collective-permute-done.32.refs_1_ = bf16[1024,768]{1,0:T(8,128)(2,1)S(1)} collective-permute-done((bf16[1024,768]{1,0:T(8,128)(2,1)}, bf16[1024,768]{1,0:T(8,128)(2,1)S(1)}, u32[]{:S(2)}, u32[]{:S(2)}) %collective-permute-start.32) | collective-permute-done | bytes 1572896 | tf_op jit(solution)/shard_map/ppermute | solution.py:31
  126.4 3.8 %collective-permute-done.33.refs_2_ = bf16[1024,768]{1,0:T(8,128)(2,1)S(1)} collective-permute-done((bf16[1024,768]{1,0:T(8,128)(2,1)}, bf16[1024,768]{1,0:T(8,128)(2,1)S(1)}, u32[]{:S(2)}, u32[]{:S(2)}) %collective-permute-start.33) | collective-permute-done | bytes 1572896 | tf_op jit(solution)/shard_map/ppermute | solution.py:31
  130.3 3.4 %collective-permute-start.21 = (bf16[512,512]{1,0:T(8,128)(2,1)S(1)}, bf16[512,512]{1,0:T(8,128)(2,1)S(1)}, u32[]{:S(2)}, u32[]{:S(2)}) collective-permute-start(bf16[512,512]{1,0:T(8,128)(2,1)S(1)} %slice.176), channel_id=1, source_target_pairs={{0,96},{32,0},{64,32},{96,64},{1,97},{33,1},{65,33},{97,65},{2,98}... | collective-permute-start | bytes 1572872 | tf_op jit(solution)/shard_map/ppermute | solution.py:31
  135.0 2.7 %collective-permute-start.13 = (bf16[512,512]{1,0:T(8,128)(2,1)S(1)}, bf16[512,512]{1,0:T(8,128)(2,1)S(1)}, u32[]{:S(2)}, u32[]{:S(2)}) collective-permute-start(bf16[512,512]{1,0:T(8,128)(2,1)S(1)} %slice.172), channel_id=1, source_target_pairs={{0,24},{8,0},{16,8},{24,16},{1,25},{9,1},{17,9},{25,17},{2,26},{10... | collective-permute-start | bytes 1572872 | tf_op jit(solution)/shard_map/ppermute | solution.py:31
  139.3 3.7 %shard_map.155.x_ref = bf16[784,4096]{1,0:T(8,128)(2,1)S(1)} custom-call(bf16[448,4096]{1,0:T(8,128)(2,1)} %shard_map.154.mine, bf16[448,4096]{1,0:T(8,128)(2,1)} %collective-permute-done.5.other), custom_call_target="tpu_custom_call" | custom-call | flops 2000000000 | bytes 8000000 | tf_op jit(solution)/shard_map/pallas_call | solution.py:52
  143.0 3.1 %shard_map.160.acc_ref = f32[768,512]{1,0:T(8,128)S(1)} custom-call(bf16[784,4096]{1,0:T(8,128)(2,1)S(1)} %shard_map.155.x_ref, bf16[1024,512]{1,0:T(8,128)(2,1)S(1)} %copy-done.7, bf16[1024,512]{1,0:T(8,128)(2,1)S(1)} %copy-done.3, bf16[1024,512]{1,0:T(8,128)(2,1)S(1)} %copy-done.5), custom_call_target="tpu_custom_call" | custom-call | flops 3000000000 | bytes 8000000 | tf_op jit(solution)/shard_map/pallas_call | solution.py:52
  146.2 4.1 %shard_map.157.acc_ref = f32[768,512]{1,0:T(8,128)S(1)} custom-call(bf16[784,4096]{1,0:T(8,128)(2,1)S(1)} %shard_map.155.x_ref, bf16[1024,512]{1,0:T(8,128)(2,1)S(1)} %copy-done.9, bf16[1024,512]{1,0:T(8,128)(2,1)} %collective-permute-done.10.refs_1_, bf16[1024,512]{1,0:T(8,128)(2,1)} %collective-permute-done.11.refs_2_), custom_call_target="tpu_custom_call" | custom-call | flops 3000000000 | bytes 8000000 | tf_op jit(solution)/shard_map/pallas_call | solution.py:52
  150.4 2.6 %collective-permute-start.35 = (bf16[512,768]{1,0:T(8,128)(2,1)S(1)}, bf16[512,768]{1,0:T(8,128)(2,1)S(1)}, u32[]{:S(2)}, u32[]{:S(2)}) collective-permute-start(bf16[512,768]{1,0:T(8,128)(2,1)S(1)} %slice.191), channel_id=1, source_target_pairs={{0,96},{32,0},{64,32},{96,64},{1,97},{33,1},{65,33},{97,65},{2,98}... | collective-permute-start | bytes 2359304 | tf_op jit(solution)/shard_map/ppermute | solution.py:31
  153.0 1.4 shard_map.161.v_ref
  154.4 6.4 %shard_map.162 = (f32[768,256]{1,0:T(8,128)S(1)}, f32[768,256]{1,0:T(8,128)S(1)}, f32[768,256]{1,0:T(8,128)S(1)}, f32[768,256]{1,0:T(8,128)S(1)}, f32[12,256]{1,0:T(8,128)S(1)}, /*index=5*/f32[1,256]{1,0:T(1,128)S(1)}) custom-call(bf16[784,4096]{1,0:T(8,128)(2,1)S(1)} %shard_map.155.x_ref, bf16[64,4096]{1,0:T(8,128)(2,1)S(1)} %bitcast.23, ...), custom_call_target="tpu_custom_call" | custom-call | flops 4000000000 | bytes 8000000 | tf_op jit(solution)/shard_map/pallas_call | solution.py:52
  160.9 2.7 %collective-permute-start.31 = (bf16[512,768]{1,0:T(8,128)(2,1)S(1)}, bf16[512,768]{1,0:T(8,128)(2,1)S(1)}, u32[]{:S(2)}, u32[]{:S(2)}) collective-permute-start(bf16[512,768]{1,0:T(8,128)(2,1)S(1)} %slice.189), channel_id=1, source_target_pairs={{0,24},{8,0},{16,8},{24,16},{1,25},{9,1},{17,9},{25,17},{2,26},{10... | collective-permute-start | bytes 2359304 | tf_op jit(solution)/shard_map/ppermute | solution.py:31
  163.6 1.4 shard_map.158.qk_ref
  165.0 2.3 shard_map.163
  167.6 5.5 %shard_map.167.acc_ref = f32[784,768]{1,0:T(8,128)S(1)} custom-call(bf16[784,4096]{1,0:T(8,128)(2,1)S(1)} %shard_map.155.x_ref, bf16[1024,768]{1,0:T(8,128)(2,1)} %get-tuple-element.38.refs_0_, bf16[1024,768]{1,0:T(8,128)(2,1)S(1)} %collective-permute-done.32.refs_1_, bf16[1024,768]{1,0:T(8,128)(2,1)S(1)} %collective-permute-done.33.refs_2_), custom_call_target="tpu_custom_call" | custom-call | flops 3000000000 | bytes 8000000 | tf_op jit(solution)/shard_map/pallas_call | solution.py:52
  173.0 5.8 %shard_map.165.acc_ref = f32[784,768]{1,0:T(8,128)S(1)} custom-call(bf16[784,4096]{1,0:T(8,128)(2,1)S(1)} %shard_map.155.x_ref, bf16[1024,768]{1,0:T(8,128)(2,1)} %get-tuple-element.37.refs_0_, bf16[1024,768]{1,0:T(8,128)(2,1)} %collective-permute-done.28.refs_1_, bf16[1024,768]{1,0:T(8,128)(2,1)} %collective-permute-done.29.refs_2_), custom_call_target="tpu_custom_call" | custom-call | flops 3000000000 | bytes 8000000 | tf_op jit(solution)/shard_map/pallas_call | solution.py:52
  180.7 1.8 shard_map.168.b_ref
  182.5 2.1 collective-permute-done.23
  184.6 1.4 collective-permute-done.24
  186.3 1.3 collective-permute-start.25
  187.6 3.2 %collective-permute-start.26 = (bf16[2,272,128]{2,1,0:T(8,128)(2,1)S(1)}, bf16[2,272,128]{2,1,0:T(8,128)(2,1)S(1)}, u32[]{:S(2)}, u32[]{:S(2)}) collective-permute-start(bf16[2,272,128]{2,1,0:T(8,128)(2,1)S(1)} %pad_maximum_fusion.3), channel_id=1, source_target_pairs={{0,32},{32,64},{64,96},{1,33},{33,65},{65,97},{2,34},{34,66},{66,9... | collective-permute-start | bytes 417800 | tf_op jit(solution)/shard_map/ppermute | solution.py:40
  190.9 1.9 shard_map.166.t_ref
  192.7 1.3 collective-permute-start.27
  194.1 3.4 %collective-permute-done.27 = bf16[2,272,128]{2,1,0:T(8,128)(2,1)S(1)} collective-permute-done((bf16[2,272,128]{2,1,0:T(8,128)(2,1)S(1)}, bf16[2,272,128]{2,1,0:T(8,128)(2,1)S(1)}, u32[]{:S(2)}, u32[]{:S(2)}) %collective-permute-start.27) | collective-permute-done | bytes 139296 | tf_op jit(solution)/shard_map/ppermute | solution.py:40
  198.3 1.6 copy-done
  199.9 1.3 copy-done.1
  201.2 3.1 %shard_map.171 = (f32[96,4096]{1,0:T(8,128)S(1)}, bf16[96,4096]{1,0:T(8,128)(2,1)S(1)}) custom-call(bf16[768,512]{1,0:T(8,128)(2,1)S(1)} %shard_map.164.attn_ref, bf16[768,256]{1,0:T(8,128)(2,1)S(1)} %shard_map.166.t_ref, bf16[768,256]{1,0:T(8,128)(2,1)S(1)} %shard_map.168.b_ref, bf16[512,4096]{1,0:T(8,128)(2,1)S(1)} %copy-done, bf16[512,4096]{1,0:T(8,128)(2,1)S(1)} %copy-done.1), custom_call_target="tpu_custom_call" | custom-call | flops 2000000000 | bytes 8000000 | tf_op jit(solution)/shard_map/pallas_call | solution.py:52
  204.2 5.5 %collective-permute-start.38 = (bf16[96,4096]{1,0:T(8,128)(2,1)S(1)}, bf16[96,4096]{1,0:T(8,128)(2,1)S(1)}, u32[]{:S(2)}, u32[]{:S(2)}) collective-permute-start(bf16[96,4096]{1,0:T(8,128)(2,1)S(1)} %get-tuple-element.44), channel_id=1, source_target_pairs={{0,1},{1,0},{2,3},{3,2},{4,5},{5,4},{6,7},{7,6},{8,9},{9,8},{10,11... | collective-permute-start | bytes 2359304 | tf_op jit(solution)/shard_map/ppermute | solution.py:35
  209.8 3.1 %shard_map.172 = (f32[96,4096]{1,0:T(8,128)S(1)}, bf16[96,4096]{1,0:T(8,128)(2,1)S(1)}) custom-call(bf16[768,512]{1,0:T(8,128)(2,1)S(1)} %shard_map.164.attn_ref, bf16[768,256]{1,0:T(8,128)(2,1)S(1)} %shard_map.166.t_ref, bf16[768,256]{1,0:T(8,128)(2,1)S(1)} %shard_map.168.b_ref, bf16[512,4096]{1,0:T(8,128)(2,1)S(1)} %copy-done, bf16[512,4096]{1,0:T(8,128)(2,1)S(1)} %copy-done.1), custom_call_target="tpu_custom_call" | custom-call | flops 2000000000 | bytes 8000000 | tf_op jit(solution)/shard_map/pallas_call | solution.py:52
  213.0 3.1 %shard_map.170 = (f32[96,4096]{1,0:T(8,128)S(1)}, bf16[96,4096]{1,0:T(8,128)(2,1)S(1)}) custom-call(bf16[768,512]{1,0:T(8,128)(2,1)S(1)} %shard_map.164.attn_ref, bf16[768,256]{1,0:T(8,128)(2,1)S(1)} %shard_map.166.t_ref, bf16[768,256]{1,0:T(8,128)(2,1)S(1)} %shard_map.168.b_ref, bf16[512,4096]{1,0:T(8,128)(2,1)S(1)} %copy-done, bf16[512,4096]{1,0:T(8,128)(2,1)S(1)} %copy-done.1), custom_call_target="tpu_custom_call" | custom-call | flops 2000000000 | bytes 8000000 | tf_op jit(solution)/shard_map/pallas_call | solution.py:52
  216.6 3.1 %shard_map.169 = (f32[96,4096]{1,0:T(8,128)S(1)}, bf16[96,4096]{1,0:T(8,128)(2,1)S(1)}) custom-call(bf16[768,512]{1,0:T(8,128)(2,1)S(1)} %shard_map.164.attn_ref, bf16[768,256]{1,0:T(8,128)(2,1)S(1)} %shard_map.166.t_ref, bf16[768,256]{1,0:T(8,128)(2,1)S(1)} %shard_map.168.b_ref, bf16[512,4096]{1,0:T(8,128)(2,1)S(1)} %copy-done, bf16[512,4096]{1,0:T(8,128)(2,1)S(1)} %copy-done.1), custom_call_target="tpu_custom_call" | custom-call | flops 2000000000 | bytes 8000000 | tf_op jit(solution)/shard_map/pallas_call | solution.py:52
  220.4 1.5 collective-permute-start.39
  222.1 1.5 collective-permute-start.41
  223.6 6.7 %collective-permute-done.44 = bf16[48,4096]{1,0:T(8,128)(2,1)S(1)} collective-permute-done((bf16[48,4096]{1,0:T(8,128)(2,1)S(1)}, bf16[48,4096]{1,0:T(8,128)(2,1)S(1)}, u32[]{:S(2)}, u32[]{:S(2)}) %collective-permute-start.44) | collective-permute-done | bytes 393248 | tf_op jit(solution)/shard_map/ppermute | solution.py:31
  230.4 1.6 collective-permute-start.45
  232.1 6.6 %collective-permute-done.43 = bf16[48,4096]{1,0:T(8,128)(2,1)S(1)} collective-permute-done((bf16[48,4096]{1,0:T(8,128)(2,1)S(1)}, bf16[48,4096]{1,0:T(8,128)(2,1)S(1)}, u32[]{:S(2)}, u32[]{:S(2)}) %collective-permute-start.43) | collective-permute-done | bytes 393248 | tf_op jit(solution)/shard_map/ppermute | solution.py:31
  238.7 1.6 collective-permute-done.41
  240.3 6.8 %collective-permute-done.45 = bf16[48,4096]{1,0:T(8,128)(2,1)S(1)} collective-permute-done((bf16[48,4096]{1,0:T(8,128)(2,1)S(1)}, bf16[48,4096]{1,0:T(8,128)(2,1)S(1)}, u32[]{:S(2)}, u32[]{:S(2)}) %collective-permute-start.45) | collective-permute-done | bytes 393248 | tf_op jit(solution)/shard_map/ppermute | solution.py:31
  247.1 1.6 collective-permute-done.40
  248.7 1.3 add_convert_fusion
  (143 shorter events, 17.3 us)
Async XLA Ops:
  2.1 10.4 %copy-start.19 = (bf16[256,256]{1,0:T(8,128)(2,1)S(1)}, bf16[256,256]{1,0:T(8,128)(2,1)}, u32[]{:S(2)}) copy-start(bf16[256,256]{1,0:T(8,128)(2,1)} %param.18) | copy-start | bytes 393220
  3.5 9.0 %copy-start.20 = (bf16[256,256]{1,0:T(8,128)(2,1)S(1)}, bf16[256,256]{1,0:T(8,128)(2,1)}, u32[]{:S(2)}) copy-start(bf16[256,256]{1,0:T(8,128)(2,1)} %param.19) | copy-start | bytes 393220
  3.6 9.0 %copy-start.16 = (bf16[256,512]{1,0:T(8,128)(2,1)S(1)}, bf16[256,512]{1,0:T(8,128)(2,1)}, u32[]{:S(2)}) copy-start(bf16[256,512]{1,0:T(8,128)(2,1)} %param.21) | copy-start | bytes 786436
  3.6 30.7 %copy-start.17 = (bf16[256,512]{1,0:T(8,128)(2,1)S(1)}, bf16[256,512]{1,0:T(8,128)(2,1)}, u32[]{:S(2)}) copy-start(bf16[256,512]{1,0:T(8,128)(2,1)} %param.22) | copy-start | bytes 786436
  3.6 6.3 %collective-permute-start = (bf16[16,4096]{1,0:T(8,128)(2,1)S(1)}, bf16[16,4096]{1,0:T(8,128)(2,1)S(1)}, u32[]{:S(2)}, u32[]{:S(2)}) collective-permute-start(bf16[16,4096]{1,0:T(8,128)(2,1)S(1)} %slice.166), channel_id=1, source_target_pairs={{0,8},{8,16},{16,24},{24,32},{32,40},{40,48},{48,56},{56,64},{64,7... | collective-permute-start | bytes 393224 | tf_op jit(solution)/shard_map/ppermute | solution.py:40
  10.0 20.7 %collective-permute-start.2 = (bf16[112,4096]{1,0:T(8,128)(2,1)S(1)}, bf16[112,4096]{1,0:T(8,128)(2,1)S(1)}, u32[]{:S(2)}, u32[]{:S(2)}) collective-permute-start(bf16[112,4096]{1,0:T(8,128)(2,1)S(1)} %pad_maximum_fusion.own), channel_id=1, source_target_pairs={{0,6},{2,0},{4,2},{6,4},{1,7},{3,1},{5,3},{7,5},{8,14},{10,8},{12,... | collective-permute-start | bytes 2752520 | tf_op jit(solution)/shard_map/ppermute | solution.py:31
  12.5 21.7 %collective-permute-start.1 = (bf16[112,4096]{1,0:T(8,128)(2,1)S(1)}, bf16[112,4096]{1,0:T(8,128)(2,1)S(1)}, u32[]{:S(2)}, u32[]{:S(2)}) collective-permute-start(bf16[112,4096]{1,0:T(8,128)(2,1)S(1)} %pad_maximum_fusion.own), channel_id=1, source_target_pairs={{0,2},{2,4},{4,6},{6,0},{1,3},{3,5},{5,7},{7,1},{8,10},{10,12},{12... | collective-permute-start | bytes 2752520 | tf_op jit(solution)/shard_map/ppermute | solution.py:31
  12.6 21.8 %copy-start.18 = (bf16[256,512]{1,0:T(8,128)(2,1)S(1)}, bf16[256,512]{1,0:T(8,128)(2,1)}, u32[]{:S(2)}) copy-start(bf16[256,512]{1,0:T(8,128)(2,1)} %param.23) | copy-start | bytes 786436
  12.6 21.8 %copy-start.15 = (bf16[256,512]{1,0:T(8,128)(2,1)S(1)}, bf16[256,512]{1,0:T(8,128)(2,1)}, u32[]{:S(2)}) copy-start(bf16[256,512]{1,0:T(8,128)(2,1)} %param.20) | copy-start | bytes 786436
  30.8 19.6 %collective-permute-start.4 = (bf16[64,4096]{1,0:T(8,128)(2,1)S(1)}, bf16[64,4096]{1,0:T(8,128)(2,1)S(1)}, u32[]{:S(2)}, u32[]{:S(2)}) collective-permute-start(bf16[64,4096]{1,0:T(8,128)(2,1)S(1)} %slice.168), channel_id=1, source_target_pairs={{0,6},{2,0},{4,2},{6,4},{1,7},{3,1},{5,3},{7,5},{8,14},{10,8},{12,... | collective-permute-start | bytes 1572872 | tf_op jit(solution)/shard_map/ppermute | solution.py:31
  34.3 9.3 %collective-permute-start.3 = (bf16[48,4096]{1,0:T(8,128)(2,1)S(1)}, bf16[48,4096]{1,0:T(8,128)(2,1)S(1)}, u32[]{:S(2)}, u32[]{:S(2)}) collective-permute-start(bf16[48,4096]{1,0:T(8,128)(2,1)S(1)} %slice.167), channel_id=1, source_target_pairs={{0,2},{2,4},{4,6},{6,0},{1,3},{3,5},{5,7},{7,1},{8,10},{10,12},{12... | collective-permute-start | bytes 1179656 | tf_op jit(solution)/shard_map/ppermute | solution.py:31
  34.5 21.7 %collective-permute-start.14 = (bf16[256,1280]{1,0:T(8,128)(2,1)S(1)}, bf16[256,1280]{1,0:T(8,128)(2,1)S(1)}, u32[]{:S(2)}, u32[]{:S(2)}) collective-permute-start(bf16[256,1280]{1,0:T(8,128)(2,1)S(1)} %pad_maximum_fusion.1.own), channel_id=1, source_target_pairs={{0,8},{8,16},{16,24},{24,0},{1,9},{9,17},{17,25},{25,1},{2,10},{10... | collective-permute-start | bytes 1966088 | tf_op jit(solution)/shard_map/ppermute | solution.py:31
  36.8 19.6 %collective-permute-start.15 = (bf16[256,1280]{1,0:T(8,128)(2,1)S(1)}, bf16[256,1280]{1,0:T(8,128)(2,1)S(1)}, u32[]{:S(2)}, u32[]{:S(2)}) collective-permute-start(bf16[256,1280]{1,0:T(8,128)(2,1)S(1)} %pad_maximum_fusion.1.own), channel_id=1, source_target_pairs={{0,24},{8,0},{16,8},{24,16},{1,25},{9,1},{17,9},{25,17},{2,26},{10... | collective-permute-start | bytes 1966088 | tf_op jit(solution)/shard_map/ppermute | solution.py:31
  38.3 20.8 %collective-permute-start.6 = (bf16[256,1280]{1,0:T(8,128)(2,1)S(1)}, bf16[256,1280]{1,0:T(8,128)(2,1)S(1)}, u32[]{:S(2)}, u32[]{:S(2)}) collective-permute-start(bf16[256,1280]{1,0:T(8,128)(2,1)S(1)} %get-tuple-element.64.own), channel_id=1, source_target_pairs={{0,32},{32,64},{64,96},{96,0},{1,33},{33,65},{65,97},{97,1},{2,34}... | collective-permute-start | bytes 1966088 | tf_op jit(solution)/shard_map/ppermute | solution.py:31
  43.6 17.3 %collective-permute-start.7 = (bf16[256,1280]{1,0:T(8,128)(2,1)S(1)}, bf16[256,1280]{1,0:T(8,128)(2,1)S(1)}, u32[]{:S(2)}, u32[]{:S(2)}) collective-permute-start(bf16[256,1280]{1,0:T(8,128)(2,1)S(1)} %get-tuple-element.64.own), channel_id=1, source_target_pairs={{0,96},{32,0},{64,32},{96,64},{1,97},{33,1},{65,33},{97,65},{2,98}... | collective-permute-start | bytes 1966088 | tf_op jit(solution)/shard_map/ppermute | solution.py:31
  52.4 86.5 %collective-permute-start.5 = (bf16[448,4096]{1,0:T(8,128)(2,1)}, bf16[448,4096]{1,0:T(8,128)(2,1)}, u32[]{:S(2)}, u32[]{:S(2)}) collective-permute-start(bf16[448,4096]{1,0:T(8,128)(2,1)} %shard_map.154.mine), channel_id=1, source_target_pairs={{0,1},{1,0},{2,3},{3,2},{4,5},{5,4},{6,7},{7,6},{8,9},{9,8},{10,11... | collective-permute-start | bytes 11010056 | tf_op jit(solution)/shard_map/ppermute | solution.py:35
  56.3 10.5 %collective-permute-start.16 = (bf16[128,1280]{1,0:T(8,128)(2,1)S(1)}, bf16[128,1280]{1,0:T(8,128)(2,1)S(1)}, u32[]{:S(2)}, u32[]{:S(2)}) collective-permute-start(bf16[128,1280]{1,0:T(8,128)(2,1)S(1)} %slice.173), channel_id=1, source_target_pairs={{0,8},{8,16},{16,24},{24,0},{1,9},{9,17},{17,25},{25,1},{2,10},{10... | collective-permute-start | bytes 983048 | tf_op jit(solution)/shard_map/ppermute | solution.py:31
  56.4 10.4 %collective-permute-start.17 = (bf16[128,1280]{1,0:T(8,128)(2,1)S(1)}, bf16[128,1280]{1,0:T(8,128)(2,1)S(1)}, u32[]{:S(2)}, u32[]{:S(2)}) collective-permute-start(bf16[128,1280]{1,0:T(8,128)(2,1)S(1)} %slice.174), channel_id=1, source_target_pairs={{0,24},{8,0},{16,8},{24,16},{1,25},{9,1},{17,9},{25,17},{2,26},{10... | collective-permute-start | bytes 983048 | tf_op jit(solution)/shard_map/ppermute | solution.py:31
  59.1 11.8 %collective-permute-start.8 = (bf16[128,1280]{1,0:T(8,128)(2,1)S(1)}, bf16[128,1280]{1,0:T(8,128)(2,1)S(1)}, u32[]{:S(2)}, u32[]{:S(2)}) collective-permute-start(bf16[128,1280]{1,0:T(8,128)(2,1)S(1)} %slice.169), channel_id=1, source_target_pairs={{0,32},{32,64},{64,96},{96,0},{1,33},{33,65},{65,97},{97,1},{2,34}... | collective-permute-start | bytes 983048 | tf_op jit(solution)/shard_map/ppermute | solution.py:31
  61.0 9.9 %collective-permute-start.9 = (bf16[128,1280]{1,0:T(8,128)(2,1)S(1)}, bf16[128,1280]{1,0:T(8,128)(2,1)S(1)}, u32[]{:S(2)}, u32[]{:S(2)}) collective-permute-start(bf16[128,1280]{1,0:T(8,128)(2,1)S(1)} %slice.170), channel_id=1, source_target_pairs={{0,96},{32,0},{64,32},{96,64},{1,97},{33,1},{65,33},{97,65},{2,98}... | collective-permute-start | bytes 983048 | tf_op jit(solution)/shard_map/ppermute | solution.py:31
  68.2 4.0 %copy-start.6 = (bf16[1024,512]{1,0:T(8,128)(2,1)}, bf16[1024,512]{1,0:T(8,128)(2,1)S(1)}, u32[]{:S(2)}) copy-start(bf16[1024,512]{1,0:T(8,128)(2,1)S(1)} %get-tuple-element.27.refs_0_) | copy-start | bytes 3145732
  68.2 32.9 %copy-start.21 = (bf16[3,512]{1,0:T(4,128)(2,1)S(1)}, bf16[3,512]{1,0:T(4,128)(2,1)}, u32[]{:S(2)}) copy-start(bf16[3,512]{1,0:T(4,128)(2,1)} %param.29) | copy-start | bytes 9220
  68.2 23.7 %collective-permute-start.18 = (bf16[1024,512]{1,0:T(8,128)(2,1)S(1)}, bf16[1024,512]{1,0:T(8,128)(2,1)S(1)}, u32[]{:S(2)}, u32[]{:S(2)}) collective-permute-start(bf16[1024,512]{1,0:T(8,128)(2,1)S(1)} %get-tuple-element.27.refs_0_), channel_id=1, source_target_pairs={{0,32},{32,64},{64,96},{96,0},{1,33},{33,65},{65,97},{97,1},{2,34}... | collective-permute-start | bytes 3145736 | tf_op jit(solution)/shard_map/ppermute | solution.py:31
  68.2 25.7 %collective-permute-start.19 = (bf16[1024,512]{1,0:T(8,128)(2,1)S(1)}, bf16[1024,512]{1,0:T(8,128)(2,1)S(1)}, u32[]{:S(2)}, u32[]{:S(2)}) collective-permute-start(bf16[1024,512]{1,0:T(8,128)(2,1)S(1)} %get-tuple-element.27.refs_0_), channel_id=1, source_target_pairs={{0,96},{32,0},{64,32},{96,64},{1,97},{33,1},{65,33},{97,65},{2,98}... | collective-permute-start | bytes 3145736 | tf_op jit(solution)/shard_map/ppermute | solution.py:31
  72.2 26.2 %collective-permute-start.10 = (bf16[1024,512]{1,0:T(8,128)(2,1)S(1)}, bf16[1024,512]{1,0:T(8,128)(2,1)}, u32[]{:S(2)}, u32[]{:S(2)}) collective-permute-start(bf16[1024,512]{1,0:T(8,128)(2,1)S(1)} %get-tuple-element.26.refs_0_), channel_id=1, source_target_pairs={{0,8},{8,16},{16,24},{24,0},{1,9},{9,17},{17,25},{25,1},{2,10},{10... | collective-permute-start | bytes 3145736 | tf_op jit(solution)/shard_map/ppermute | solution.py:31
  72.2 26.2 %collective-permute-start.11 = (bf16[1024,512]{1,0:T(8,128)(2,1)S(1)}, bf16[1024,512]{1,0:T(8,128)(2,1)}, u32[]{:S(2)}, u32[]{:S(2)}) collective-permute-start(bf16[1024,512]{1,0:T(8,128)(2,1)S(1)} %get-tuple-element.26.refs_0_), channel_id=1, source_target_pairs={{0,24},{8,0},{16,8},{24,16},{1,25},{9,1},{17,9},{25,17},{2,26},{10... | collective-permute-start | bytes 3145736 | tf_op jit(solution)/shard_map/ppermute | solution.py:31
  92.0 34.4 %collective-permute-start.32 = (bf16[1024,768]{1,0:T(8,128)(2,1)}, bf16[1024,768]{1,0:T(8,128)(2,1)S(1)}, u32[]{:S(2)}, u32[]{:S(2)}) collective-permute-start(bf16[1024,768]{1,0:T(8,128)(2,1)} %get-tuple-element.38.refs_0_), channel_id=1, source_target_pairs={{0,32},{32,64},{64,96},{96,0},{1,33},{33,65},{65,97},{97,1},{2,34}... | collective-permute-start | bytes 4718600 | tf_op jit(solution)/shard_map/ppermute | solution.py:31
  94.9 35.4 %collective-permute-start.33 = (bf16[1024,768]{1,0:T(8,128)(2,1)}, bf16[1024,768]{1,0:T(8,128)(2,1)S(1)}, u32[]{:S(2)}, u32[]{:S(2)}) collective-permute-start(bf16[1024,768]{1,0:T(8,128)(2,1)} %get-tuple-element.38.refs_0_), channel_id=1, source_target_pairs={{0,96},{32,0},{64,32},{96,64},{1,97},{33,1},{65,33},{97,65},{2,98}... | collective-permute-start | bytes 4718600 | tf_op jit(solution)/shard_map/ppermute | solution.py:31
  98.4 35.3 %collective-permute-start.28 = (bf16[1024,768]{1,0:T(8,128)(2,1)}, bf16[1024,768]{1,0:T(8,128)(2,1)}, u32[]{:S(2)}, u32[]{:S(2)}) collective-permute-start(bf16[1024,768]{1,0:T(8,128)(2,1)} %get-tuple-element.37.refs_0_), channel_id=1, source_target_pairs={{0,8},{8,16},{16,24},{24,0},{1,9},{9,17},{17,25},{25,1},{2,10},{10... | collective-permute-start | bytes 4718600 | tf_op jit(solution)/shard_map/ppermute | solution.py:31
  98.4 36.6 %collective-permute-start.29 = (bf16[1024,768]{1,0:T(8,128)(2,1)}, bf16[1024,768]{1,0:T(8,128)(2,1)}, u32[]{:S(2)}, u32[]{:S(2)}) collective-permute-start(bf16[1024,768]{1,0:T(8,128)(2,1)} %get-tuple-element.37.refs_0_), channel_id=1, source_target_pairs={{0,24},{8,0},{16,8},{24,16},{1,25},{9,1},{17,9},{25,17},{2,26},{10... | collective-permute-start | bytes 4718600 | tf_op jit(solution)/shard_map/ppermute | solution.py:31
  126.4 24.0 %collective-permute-start.20 = (bf16[512,512]{1,0:T(8,128)(2,1)S(1)}, bf16[512,512]{1,0:T(8,128)(2,1)S(1)}, u32[]{:S(2)}, u32[]{:S(2)}) collective-permute-start(bf16[512,512]{1,0:T(8,128)(2,1)S(1)} %slice.175), channel_id=1, source_target_pairs={{0,32},{32,64},{64,96},{96,0},{1,33},{33,65},{65,97},{97,1},{2,34}... | collective-permute-start | bytes 1572872 | tf_op jit(solution)/shard_map/ppermute | solution.py:31
  130.3 22.7 %collective-permute-start.21 = (bf16[512,512]{1,0:T(8,128)(2,1)S(1)}, bf16[512,512]{1,0:T(8,128)(2,1)S(1)}, u32[]{:S(2)}, u32[]{:S(2)}) collective-permute-start(bf16[512,512]{1,0:T(8,128)(2,1)S(1)} %slice.176), channel_id=1, source_target_pairs={{0,96},{32,0},{64,32},{96,64},{1,97},{33,1},{65,33},{97,65},{2,98}... | collective-permute-start | bytes 1572872 | tf_op jit(solution)/shard_map/ppermute | solution.py:31
  133.8 27.1 %collective-permute-start.12 = (bf16[512,512]{1,0:T(8,128)(2,1)S(1)}, bf16[512,512]{1,0:T(8,128)(2,1)S(1)}, u32[]{:S(2)}, u32[]{:S(2)}) collective-permute-start(bf16[512,512]{1,0:T(8,128)(2,1)S(1)} %slice.171), channel_id=1, source_target_pairs={{0,8},{8,16},{16,24},{24,0},{1,9},{9,17},{17,25},{25,1},{2,10},{10... | collective-permute-start | bytes 1572872 | tf_op jit(solution)/shard_map/ppermute | solution.py:31
  135.0 28.6 %collective-permute-start.13 = (bf16[512,512]{1,0:T(8,128)(2,1)S(1)}, bf16[512,512]{1,0:T(8,128)(2,1)S(1)}, u32[]{:S(2)}, u32[]{:S(2)}) collective-permute-start(bf16[512,512]{1,0:T(8,128)(2,1)S(1)} %slice.172), channel_id=1, source_target_pairs={{0,24},{8,0},{16,8},{24,16},{1,25},{9,1},{17,9},{25,17},{2,26},{10... | collective-permute-start | bytes 1572872 | tf_op jit(solution)/shard_map/ppermute | solution.py:31
  139.0 4.0 %copy-start.3 = (bf16[1024,512]{1,0:T(8,128)(2,1)S(1)}, bf16[1024,512]{1,0:T(8,128)(2,1)}, u32[]{:S(2)}) copy-start(bf16[1024,512]{1,0:T(8,128)(2,1)} %copy-done.2) | copy-start | bytes 3145732
  139.0 4.0 %copy-start.5 = (bf16[1024,512]{1,0:T(8,128)(2,1)S(1)}, bf16[1024,512]{1,0:T(8,128)(2,1)}, u32[]{:S(2)}) copy-start(bf16[1024,512]{1,0:T(8,128)(2,1)} %copy-done.4) | copy-start | bytes 3145732
  139.0 4.0 %copy-start.7 = (bf16[1024,512]{1,0:T(8,128)(2,1)S(1)}, bf16[1024,512]{1,0:T(8,128)(2,1)}, u32[]{:S(2)}) copy-start(bf16[1024,512]{1,0:T(8,128)(2,1)} %copy-done.6) | copy-start | bytes 3145732
  139.0 39.8 %collective-permute-start.34 = (bf16[512,768]{1,0:T(8,128)(2,1)S(1)}, bf16[512,768]{1,0:T(8,128)(2,1)S(1)}, u32[]{:S(2)}, u32[]{:S(2)}) collective-permute-start(bf16[512,768]{1,0:T(8,128)(2,1)S(1)} %slice.190), channel_id=1, source_target_pairs={{0,32},{32,64},{64,96},{96,0},{1,33},{33,65},{65,97},{97,1},{2,34}... | collective-permute-start | bytes 2359304 | tf_op jit(solution)/shard_map/ppermute | solution.py:31
  143.0 3.1 %copy-start.9 = (bf16[1024,512]{1,0:T(8,128)(2,1)S(1)}, bf16[1024,512]{1,0:T(8,128)(2,1)}, u32[]{:S(2)}) copy-start(bf16[1024,512]{1,0:T(8,128)(2,1)} %copy-done.8) | copy-start | bytes 3145732
  150.3 4.1 %copy-start.10 = (bf16[4096,64]{0,1:T(8,128)(2,1)S(1)}, bf16[4096,64]{0,1:T(8,128)(2,1)}, u32[]{:S(2)}) copy-start(bf16[4096,64]{0,1:T(8,128)(2,1)} %param.24) | copy-start | bytes 1572868
  150.3 4.1 %copy-start.11 = (bf16[64,256]{1,0:T(8,128)(2,1)S(1)}, bf16[64,256]{1,0:T(8,128)(2,1)}, u32[]{:S(2)}) copy-start(bf16[64,256]{1,0:T(8,128)(2,1)} %right_ref.1) | copy-start | bytes 98308
  150.3 4.1 %copy-start.12 = (f32[2,768]{1,0:T(2,128)S(1)}, f32[2,768]{1,0:T(2,128)}, u32[]{:S(2)}) copy-start(f32[2,768]{1,0:T(2,128)} %spike_ref.1) | copy-start | bytes 18436
  150.3 4.1 %copy-start.13 = (f32[256]{0:T(256)S(1)}, f32[256]{0:T(256)}, u32[]{:S(2)}) copy-start(f32[256]{0:T(256)} %param.26) | copy-start | bytes 3076
  150.4 29.4 %collective-permute-start.35 = (bf16[512,768]{1,0:T(8,128)(2,1)S(1)}, bf16[512,768]{1,0:T(8,128)(2,1)S(1)}, u32[]{:S(2)}, u32[]{:S(2)}) collective-permute-start(bf16[512,768]{1,0:T(8,128)(2,1)S(1)} %slice.191), channel_id=1, source_target_pairs={{0,96},{32,0},{64,32},{96,64},{1,97},{33,1},{65,33},{97,65},{2,98}... | collective-permute-start | bytes 2359304 | tf_op jit(solution)/shard_map/ppermute | solution.py:31
  153.0 37.9 %collective-permute-start.30 = (bf16[512,768]{1,0:T(8,128)(2,1)S(1)}, bf16[512,768]{1,0:T(8,128)(2,1)S(1)}, u32[]{:S(2)}, u32[]{:S(2)}) collective-permute-start(bf16[512,768]{1,0:T(8,128)(2,1)S(1)} %slice.188), channel_id=1, source_target_pairs={{0,8},{8,16},{16,24},{24,0},{1,9},{9,17},{17,25},{25,1},{2,10},{10... | collective-permute-start | bytes 2359304 | tf_op jit(solution)/shard_map/ppermute | solution.py:31
  160.9 30.0 %collective-permute-start.31 = (bf16[512,768]{1,0:T(8,128)(2,1)S(1)}, bf16[512,768]{1,0:T(8,128)(2,1)S(1)}, u32[]{:S(2)}, u32[]{:S(2)}) collective-permute-start(bf16[512,768]{1,0:T(8,128)(2,1)S(1)} %slice.189), channel_id=1, source_target_pairs={{0,24},{8,0},{16,8},{24,16},{1,25},{9,1},{17,9},{25,17},{2,26},{10... | collective-permute-start | bytes 2359304 | tf_op jit(solution)/shard_map/ppermute | solution.py:31
  167.4 15.1 %collective-permute-start.22 = (bf16[2,272,128]{2,1,0:T(8,128)(2,1)S(1)}, bf16[2,272,128]{2,1,0:T(8,128)(2,1)S(1)}, u32[]{:S(2)}, u32[]{:S(2)}) collective-permute-start(bf16[2,272,128]{2,1,0:T(8,128)(2,1)S(1)} %pad_maximum_fusion.2), channel_id=1, source_target_pairs={{0,24},{8,0},{16,8},{24,16},{1,25},{9,1},{17,9},{25,17},{2,26},{10... | collective-permute-start | bytes 417800 | tf_op jit(solution)/shard_map/ppermute | solution.py:31
  178.8 5.8 %collective-permute-start.23 = (bf16[2,272,128]{2,1,0:T(8,128)(2,1)S(1)}, bf16[2,272,128]{2,1,0:T(8,128)(2,1)S(1)}, u32[]{:S(2)}, u32[]{:S(2)}) collective-permute-start(bf16[2,272,128]{2,1,0:T(8,128)(2,1)S(1)} %pad_maximum_fusion.2), channel_id=1, source_target_pairs={{0,16},{8,24},{16,0},{24,8},{1,17},{9,25},{17,1},{25,9},{2,18},{10... | collective-permute-start | bytes 417800 | tf_op jit(solution)/shard_map/ppermute | solution.py:31
  179.7 6.3 %collective-permute-start.24 = (bf16[2,272,128]{2,1,0:T(8,128)(2,1)S(1)}, bf16[2,272,128]{2,1,0:T(8,128)(2,1)S(1)}, u32[]{:S(2)}, u32[]{:S(2)}) collective-permute-start(bf16[2,272,128]{2,1,0:T(8,128)(2,1)S(1)} %pad_maximum_fusion.2), channel_id=1, source_target_pairs={{0,8},{8,16},{16,24},{24,0},{1,9},{9,17},{17,25},{25,1},{2,10},{10... | collective-permute-start | bytes 417800 | tf_op jit(solution)/shard_map/ppermute | solution.py:31
  186.3 7.7 %collective-permute-start.25 = (bf16[2,272,128]{2,1,0:T(8,128)(2,1)S(1)}, bf16[2,272,128]{2,1,0:T(8,128)(2,1)S(1)}, u32[]{:S(2)}, u32[]{:S(2)}) collective-permute-start(bf16[2,272,128]{2,1,0:T(8,128)(2,1)S(1)} %pad_maximum_fusion.3), channel_id=1, source_target_pairs={{0,64},{32,96},{1,65},{33,97},{2,66},{34,98},{3,67},{35,99},{4,68}... | collective-permute-start | bytes 417800 | tf_op jit(solution)/shard_map/ppermute | solution.py:40
  187.6 6.4 %collective-permute-start.26 = (bf16[2,272,128]{2,1,0:T(8,128)(2,1)S(1)}, bf16[2,272,128]{2,1,0:T(8,128)(2,1)S(1)}, u32[]{:S(2)}, u32[]{:S(2)}) collective-permute-start(bf16[2,272,128]{2,1,0:T(8,128)(2,1)S(1)} %pad_maximum_fusion.3), channel_id=1, source_target_pairs={{0,32},{32,64},{64,96},{1,33},{33,65},{65,97},{2,34},{34,66},{66,9... | collective-permute-start | bytes 417800 | tf_op jit(solution)/shard_map/ppermute | solution.py:40
  192.7 5.0 %copy-start.14 = (bf16[2,256]{1,0:T(2,128)(2,1)S(1)}, bf16[2,256]{1,0:T(2,128)(2,1)}, u32[]{:S(2)}) copy-start(bf16[2,256]{1,0:T(2,128)(2,1)} %gain_ref.1) | copy-start | bytes 3076
  192.7 4.8 %collective-permute-start.27 = (bf16[2,272,128]{2,1,0:T(8,128)(2,1)S(1)}, bf16[2,272,128]{2,1,0:T(8,128)(2,1)S(1)}, u32[]{:S(2)}, u32[]{:S(2)}) collective-permute-start(bf16[2,272,128]{2,1,0:T(8,128)(2,1)S(1)} %pad_maximum_fusion.3), channel_id=1, source_target_pairs={{0,96},{1,97},{2,98},{3,99},{4,100},{5,101},{6,102},{7,103},{8,104... | collective-permute-start | bytes 417800 | tf_op jit(solution)/shard_map/ppermute | solution.py:40
  197.7 3.5 %copy-start.1 = (bf16[512,4096]{1,0:T(8,128)(2,1)S(1)}, bf16[512,4096]{1,0:T(8,128)(2,1)}, u32[]{:S(2)}) copy-start(bf16[512,4096]{1,0:T(8,128)(2,1)} %filter_ref.7) | copy-start | bytes 12582916
  204.2 15.6 %collective-permute-start.38 = (bf16[96,4096]{1,0:T(8,128)(2,1)S(1)}, bf16[96,4096]{1,0:T(8,128)(2,1)S(1)}, u32[]{:S(2)}, u32[]{:S(2)}) collective-permute-start(bf16[96,4096]{1,0:T(8,128)(2,1)S(1)} %get-tuple-element.44), channel_id=1, source_target_pairs={{0,1},{1,0},{2,3},{3,2},{4,5},{5,4},{6,7},{7,6},{8,9},{9,8},{10,11... | collective-permute-start | bytes 2359304 | tf_op jit(solution)/shard_map/ppermute | solution.py:35
  212.8 7.3 %collective-permute-start.42 = (bf16[96,4096]{1,0:T(8,128)(2,1)S(1)}, bf16[96,4096]{1,0:T(8,128)(2,1)S(1)}, u32[]{:S(2)}, u32[]{:S(2)}) collective-permute-start(bf16[96,4096]{1,0:T(8,128)(2,1)S(1)} %get-tuple-element.46), channel_id=1, source_target_pairs={{0,1},{1,0},{2,3},{3,2},{4,5},{5,4},{6,7},{7,6},{8,9},{9,8},{10,11... | collective-permute-start | bytes 2359304 | tf_op jit(solution)/shard_map/ppermute | solution.py:35
  216.0 5.9 %collective-permute-start.37 = (bf16[96,4096]{1,0:T(8,128)(2,1)S(1)}, bf16[96,4096]{1,0:T(8,128)(2,1)S(1)}, u32[]{:S(2)}, u32[]{:S(2)}) collective-permute-start(bf16[96,4096]{1,0:T(8,128)(2,1)S(1)} %get-tuple-element.42), channel_id=1, source_target_pairs={{0,1},{1,0},{2,3},{3,2},{4,5},{5,4},{6,7},{7,6},{8,9},{9,8},{10,11... | collective-permute-start | bytes 2359304 | tf_op jit(solution)/shard_map/ppermute | solution.py:35
  219.7 12.4 %collective-permute-start.36 = (bf16[96,4096]{1,0:T(8,128)(2,1)S(1)}, bf16[96,4096]{1,0:T(8,128)(2,1)S(1)}, u32[]{:S(2)}, u32[]{:S(2)}) collective-permute-start(bf16[96,4096]{1,0:T(8,128)(2,1)S(1)} %get-tuple-element.40), channel_id=1, source_target_pairs={{0,1},{1,0},{2,3},{3,2},{4,5},{5,4},{6,7},{7,6},{8,9},{9,8},{10,11... | collective-permute-start | bytes 2359304 | tf_op jit(solution)/shard_map/ppermute | solution.py:35
  220.0 10.3 %collective-permute-start.44 = (bf16[48,4096]{1,0:T(8,128)(2,1)S(1)}, bf16[48,4096]{1,0:T(8,128)(2,1)S(1)}, u32[]{:S(2)}, u32[]{:S(2)}) collective-permute-start(bf16[48,4096]{1,0:T(8,128)(2,1)S(1)} %get-tuple-element.56), channel_id=1, source_target_pairs={{0,6},{2,0},{4,2},{6,4},{1,7},{3,1},{5,3},{7,5},{8,14},{10,8},{12,... | collective-permute-start | bytes 1179656 | tf_op jit(solution)/shard_map/ppermute | solution.py:31
  220.3 18.4 %collective-permute-start.43 = (bf16[48,4096]{1,0:T(8,128)(2,1)S(1)}, bf16[48,4096]{1,0:T(8,128)(2,1)S(1)}, u32[]{:S(2)}, u32[]{:S(2)}) collective-permute-start(bf16[48,4096]{1,0:T(8,128)(2,1)S(1)} %slice.245), channel_id=1, source_target_pairs={{0,6},{2,0},{4,2},{6,4},{1,7},{3,1},{5,3},{7,5},{8,14},{10,8},{12,... | collective-permute-start | bytes 1179656 | tf_op jit(solution)/shard_map/ppermute | solution.py:31
  220.4 11.5 %collective-permute-start.39 = (bf16[48,4096]{1,0:T(8,128)(2,1)S(1)}, bf16[48,4096]{1,0:T(8,128)(2,1)S(1)}, u32[]{:S(2)}, u32[]{:S(2)}) collective-permute-start(bf16[48,4096]{1,0:T(8,128)(2,1)S(1)} %get-tuple-element.57), channel_id=1, source_target_pairs={{0,2},{2,4},{4,6},{6,0},{1,3},{3,5},{5,7},{7,1},{8,10},{10,12},{12... | collective-permute-start | bytes 1179656 | tf_op jit(solution)/shard_map/ppermute | solution.py:31
  222.1 18.2 %collective-permute-start.41 = (bf16[48,4096]{1,0:T(8,128)(2,1)S(1)}, bf16[48,4096]{1,0:T(8,128)(2,1)S(1)}, u32[]{:S(2)}, u32[]{:S(2)}) collective-permute-start(bf16[48,4096]{1,0:T(8,128)(2,1)S(1)} %slice.246), channel_id=1, source_target_pairs={{0,2},{2,4},{4,6},{6,0},{1,3},{3,5},{5,7},{7,1},{8,10},{10,12},{12... | collective-permute-start | bytes 1179656 | tf_op jit(solution)/shard_map/ppermute | solution.py:31
  230.4 16.8 %collective-permute-start.45 = (bf16[48,4096]{1,0:T(8,128)(2,1)S(1)}, bf16[48,4096]{1,0:T(8,128)(2,1)S(1)}, u32[]{:S(2)}, u32[]{:S(2)}) collective-permute-start(bf16[48,4096]{1,0:T(8,128)(2,1)S(1)} %fusion.3), channel_id=1, source_target_pairs={{0,6},{2,0},{4,2},{6,4},{1,7},{3,1},{5,3},{7,5},{8,14},{10,8},{12,... | collective-permute-start | bytes 1179656 | tf_op jit(solution)/shard_map/ppermute | solution.py:31
  232.0 16.7 %collective-permute-start.40 = (bf16[48,4096]{1,0:T(8,128)(2,1)S(1)}, bf16[48,4096]{1,0:T(8,128)(2,1)S(1)}, u32[]{:S(2)}, u32[]{:S(2)}) collective-permute-start(bf16[48,4096]{1,0:T(8,128)(2,1)S(1)} %fusion.4), channel_id=1, source_target_pairs={{0,2},{2,4},{4,6},{6,0},{1,3},{3,5},{5,7},{7,1},{8,10},{10,12},{12... | collective-permute-start | bytes 1179656 | tf_op jit(solution)/shard_map/ppermute | solution.py:31
  (4 other events, 5.2 us)
where the time goes:
time: 251 us; the launch traced here: 250 us
  waiting for transfers between devices  98.1 us (39%)
  starting transfers between devices  76.8 us (31%)
  Pallas kernels  55.1 us (22%)
  local copies, waits for them, and re-layouts  13.1 us (5%)
  other arithmetic  6.01 us (2%)
    ppermute x37, waiting for transfers between devices, hop(): lax.ppermute(value, axis, [(i, (i + steps) % RING) for i in range(RING)])  92.5 us
    ppermute x37, starting transfers between devices, hop(): lax.ppermute(value, axis, [(i, (i + steps) % RING) for i in range(RING)])  56.7 us
    pallas_call x19, Pallas kernels, vmem_kernel(): pl.pallas_call(kernel, out_shape=out_shape, compiler_params=pltpu.Compile...  55.1 us
    ppermute x5, starting transfers between devices, swap(): return lax.ppermute(value, 'c', [(0, 1), (1, 0)])  10.1 us
    ppermute x4, starting transfers between devices, onward(): lax.ppermute(value, axis, [(i, i + steps) for i in range(count - steps)])  9.95 us
    unnamed x47, local copies, waits for them, and re-layouts  5.99 us
    ppermute x4, waiting for transfers between devices, onward(): lax.ppermute(value, axis, [(i, i + steps) for i in range(count - steps)])  5.54 us
  transfers between devices with their start and end apart: 46, of which 17 were waited for; matrix products, arithmetic and copies ran while one was open for 3% of the time, Pallas kernels for 21%

commit v1 on v0

--- a/solution.py
+++ b/solution.py
@@ -217,10 +217,17 @@
     )
 
 
-def norm_values(rows, gain):
-    rows_f = rows.astype(F32)
-    meansq = jnp.mean(rows_f * rows_f, axis=-1, keepdims=True)
-    return rows_f * lax.rsqrt(meansq + EPSILON) * gain.astype(F32)
+def norm_kernel(rows_ref, gain_ref, out_ref):
+    rows = rows_ref[...].astype(F32)
+    meansq = jnp.mean(rows * rows, axis=-1, keepdims=True)
+    normed = rows * lax.rsqrt(meansq + EPSILON) * gain_ref[...].astype(F32)
+    out_ref[...] = normed.astype(BF16)
+
+
+def norm_rows(rows, gain):
+    return vmem_kernel(
+        norm_kernel, jax.ShapeDtypeStruct(rows.shape, BF16), 1_000_000, rows, gain[None]
+    )
 
 
 def decay_kernel(
@@ -361,7 +368,7 @@
     return vmem_kernel(
         finish_kernel,
         jax.ShapeDtypeStruct((length, wide), BF16),
-        3_000_000_000,
+        100_000_000,
         part,
         qfar,
         state,
@@ -413,11 +420,15 @@
     return combine(outer, before)[1].astype(BF16)
 
 
-def term_kernel(step, attn_ref, t_ref, b_ref, mixer_ref, filter_ref, own_ref, other_ref):
+def term_kernel(steps, attn_ref, t_ref, b_ref, mixer_ref, filter_ref, own_ref, other_ref):
     x, c = lax.axis_index("x"), lax.axis_index("c")
-    part = own_ref.shape[0]
-    base = lax.rem(x + step, RING) * PAIR * part
-    spots = [pl.multiple_of(base + core * part, HALO) for core in (1 - c, c)]
+    count = own_ref.shape[0]
+    part = count // len(steps)
+    spots = [
+        pl.multiple_of((lax.rem(x + step, RING) * PAIR + core) * part, HALO)
+        for core in (1 - c, c)
+        for step in steps
+    ]
     half = t_ref.shape[1]
     out = None
     for ref, matrix in (
@@ -428,16 +439,17 @@
         rows = jnp.concatenate([ref[pl.ds(at, part), :] for at in spots], axis=0)
         term = dot(rows, matrix)
         out = term if out is None else out + term
-    other_ref[...] = out[:part].astype(BF16)
-    own_ref[...] = out[part:]
-
-
-def term_call(step, attn, t, b, mixer, filt, part):
+    other_ref[...] = out[:count].astype(BF16)
+    own_ref[...] = out[count:]
+
+
+def term_call(steps, attn, t, b, mixer, filt, part):
     width = mixer.shape[1]
+    part = part * len(steps)
     tile = 1024
     whole = pl.BlockSpec(memory_space=pltpu.VMEM)
     return vmem_kernel(
-        functools.partial(term_kernel, step),
+        functools.partial(term_kernel, steps),
         (
             jax.ShapeDtypeStruct((part, width), F32),
             jax.ShapeDtypeStruct((part, width), BF16),
@@ -489,17 +501,17 @@
     half = channels // 2
     keys, values = 2 * heads * key_dim, heads * value_dim
 
-    def shard(attn, cols):
-        convs = [w[:, cols] for w in (postfilter, prefilter, source)]
-        return jnp.concatenate(attn + convs, axis=1)
-
-    tops = shard([probe, lookup], slice(0, half))
-    bottoms = shard([payload], slice(half, channels))
+    def shard(attn, convs, cols):
+        return jnp.concatenate(attn + [w[:, cols] for w in convs], axis=1)
+
+    normed = norm_rows(hidden, entry_gain)
+    part = normed.shape[0]
+    rim = onward(normed[part - HALO :], SP, 1)
+    convs = (postfilter, prefilter, source)
+    tops = shard([probe, lookup], convs, slice(0, half))
+    bottoms = shard([payload], lax.optimization_barrier(convs), slice(half, channels))
     first = around(tops, "z")
     second = around(bottoms, "y")
-    normed = norm_values(hidden, entry_gain).astype(BF16)
-    part = normed.shape[0]
-    rim = onward(normed[part - HALO :], SP, 1)
     x = gather_rows(jnp.concatenate([normed, rim], axis=0))
 
     line_qk, line_t = line_up("z", first, (keys, 3 * half))
@@ -525,16 +537,17 @@
     mixed_t = gate_call(x, acc_t, w_t[3:], late, taps[:, :half], 1)
     mixed_b = gate_call(x, acc_b, w_b[3:], late, taps[:, half:], 0)
 
-    def partial(step):
+    def partial(*steps):
         own, other = term_call(
-            step, mixed_attn, mixed_t, mixed_b, mixer_result, filter_result, part
+            steps, mixed_attn, mixed_t, mixed_b, mixer_result, filter_result, part
         )
         return plus(own, swap(other))
 
     cut = part // 2
     far = partial(2).astype(BF16)
     far_up, far_down = hop(far[:cut], "x", 1), hop(far[cut:], "x", -1)
-    up, down = partial(1), partial(3)
+    near_terms = partial(1, 3)
+    up, down = near_terms[:part], near_terms[part:]
     plain_up = hop(up[cut:].astype(BF16), "x", 1)
     plain_down = hop(down[:cut].astype(BF16), "x", -1)
     last_up = hop(plus(up[:cut], far_up).astype(BF16), "x", 1)

time: 251 us -> 250 us (level)
  starting transfers between devices: 76.8 us -> 81.2 us
  other arithmetic: 6.01 us -> 2.76 us
    ppermute x37, starting transfers between devices: 56.7 us -> 61.3 us  [hop(): lax.ppermute(value, axis, [(i, (i + steps) % RING) for i in range(RING)])]
    unnamed x47 -> x51, local copies, waits for them, and re-layouts: 5.99 us -> 5.62 us
    ppermute x5 -> x4, starting transfers between devices: 10.1 us -> 9.96 us  [swap(): return lax.ppermute(value, 'c', [(0, 1), (1, 0)])]
  transfers between devices with their start and end apart: 46 -> 45, of which waited for: 17 -> 15; matrix products, arithmetic and copies ran while one was open for 3% -> 3% of each run, Pallas kernels for 21% -> 20%
where the time goes in v1:
time: 250 us; the launch traced here: 249 us
  waiting for transfers between devices  96.2 us (38%)
  starting transfers between devices  81.2 us (32%)
  Pallas kernels  54.2 us (22%)
  local copies, waits for them, and re-layouts  13.4 us (5%)
  other arithmetic  2.76 us (1%)
    ppermute x37, waiting for transfers between devices, hop(): lax.ppermute(value, axis, [(i, (i + steps) % RING) for i in range(RING)])  90.7 us
    ppermute x37, starting transfers between devices, hop(): lax.ppermute(value, axis, [(i, (i + steps) % RING) for i in range(RING)])  61.3 us
    pallas_call x19, Pallas kernels, vmem_kernel(): pl.pallas_call(kernel, out_shape=out_shape, compiler_params=pltpu.Compile...  54.2 us
    ppermute x4, starting transfers between devices, swap(): return lax.ppermute(value, 'c', [(0, 1), (1, 0)])  9.96 us
    ppermute x4, starting transfers between devices, onward(): lax.ppermute(value, axis, [(i, i + steps) for i in range(count - steps)])  9.96 us
    unnamed x51, local copies, waits for them, and re-layouts  5.62 us
    ppermute x4, waiting for transfers between devices, onward(): lax.ppermute(value, axis, [(i, i + steps) for i in range(count - steps)])  5.54 us
  transfers between devices with their start and end apart: 45, of which 15 were waited for; matrix products, arithmetic and copies ran while one was open for 3% of the time, Pallas kernels for 20%

profile of v1, /device:TPU:1, one launch (start us, length us, event | category | flops | bytes accessed | tf_op | source)
XLA Modules:
  0.0 248.7 jit_solution(9319841159091178852)
XLA Ops:
  0.7 1.1 copy-done.10
  2.4 4.2 %collective-permute-start = (bf16[16,4096]{1,0:T(8,128)(2,1)S(1)}, bf16[16,4096]{1,0:T(8,128)(2,1)S(1)}, u32[]{:S(2)}, u32[]{:S(2)}) collective-permute-start(bf16[16,4096]{1,0:T(8,128)(2,1)S(1)} %slice.172), channel_id=1, source_target_pairs={{0,8},{8,16},{16,24},{24,32},{32,40},{40,48},{48,56},{56,64},{64,7... | collective-permute-start | bytes 393224 | tf_op jit(solution)/shard_map/ppermute | solution.py:40
  6.5 2.2 collective-permute-done
  8.8 2.5 %collective-permute-start.2 = (bf16[112,4096]{1,0:T(8,128)(2,1)S(1)}, bf16[112,4096]{1,0:T(8,128)(2,1)S(1)}, u32[]{:S(2)}, u32[]{:S(2)}) collective-permute-start(bf16[112,4096]{1,0:T(8,128)(2,1)S(1)} %pad_maximum_fusion.own), channel_id=1, source_target_pairs={{0,6},{2,0},{4,2},{6,4},{1,7},{3,1},{5,3},{7,5},{8,14},{10,8},{12,... | collective-permute-start | bytes 2752520 | tf_op jit(solution)/shard_map/ppermute | solution.py:31
  11.4 2.3 collective-permute-start.14
  13.7 1.5 collective-permute-start.15
  15.3 14.2 %collective-permute-done.2.above = bf16[112,4096]{1,0:T(8,128)(2,1)S(1)} collective-permute-done((bf16[112,4096]{1,0:T(8,128)(2,1)S(1)}, bf16[112,4096]{1,0:T(8,128)(2,1)S(1)}, u32[]{:S(2)}, u32[]{:S(2)}) %collective-permute-start.2) | collective-permute-done | bytes 917536 | tf_op jit(solution)/shard_map/ppermute | solution.py:31
  29.5 3.5 %collective-permute-start.4 = (bf16[64,4096]{1,0:T(8,128)(2,1)S(1)}, bf16[64,4096]{1,0:T(8,128)(2,1)S(1)}, u32[]{:S(2)}, u32[]{:S(2)}) collective-permute-start(bf16[64,4096]{1,0:T(8,128)(2,1)S(1)} %slice.174), channel_id=1, source_target_pairs={{0,6},{2,0},{4,2},{6,4},{1,7},{3,1},{5,3},{7,5},{8,14},{10,8},{12,... | collective-permute-start | bytes 1572872 | tf_op jit(solution)/shard_map/ppermute | solution.py:31
  33.2 4.7 %collective-permute-start.6 = (bf16[256,1280]{1,0:T(8,128)(2,1)S(1)}, bf16[256,1280]{1,0:T(8,128)(2,1)S(1)}, u32[]{:S(2)}, u32[]{:S(2)}) collective-permute-start(bf16[256,1280]{1,0:T(8,128)(2,1)S(1)} %slice_dynamic-update-slice_fusion.own), channel_id=1, source_target_pairs={{0,32},{32,64},{64,96},{96,0},{1,33},{33,65},{65,97},{97,1},{2,34}... | collective-permute-start | bytes 1966088 | tf_op jit(solution)/shard_map/ppermute | solution.py:31
  38.0 4.4 %collective-permute-done.3.top = bf16[48,4096]{1,0:T(8,128)(2,1)S(1)} collective-permute-done((bf16[48,4096]{1,0:T(8,128)(2,1)S(1)}, bf16[48,4096]{1,0:T(8,128)(2,1)S(1)}, u32[]{:S(2)}, u32[]{:S(2)}) %collective-permute-start.3) | collective-permute-done | bytes 393248 | tf_op jit(solution)/shard_map/ppermute | solution.py:31
  42.4 6.8 %collective-permute-start.7 = (bf16[256,1280]{1,0:T(8,128)(2,1)S(1)}, bf16[256,1280]{1,0:T(8,128)(2,1)S(1)}, u32[]{:S(2)}, u32[]{:S(2)}) collective-permute-start(bf16[256,1280]{1,0:T(8,128)(2,1)S(1)} %slice_dynamic-update-slice_fusion.own), channel_id=1, source_target_pairs={{0,96},{32,0},{64,32},{96,64},{1,97},{33,1},{65,33},{97,65},{2,98}... | collective-permute-start | bytes 1966088 | tf_op jit(solution)/shard_map/ppermute | solution.py:31
  49.2 2.1 shard_map.155.mine
  51.2 3.8 %collective-permute-start.5 = (bf16[448,4096]{1,0:T(8,128)(2,1)}, bf16[448,4096]{1,0:T(8,128)(2,1)}, u32[]{:S(2)}, u32[]{:S(2)}) collective-permute-start(bf16[448,4096]{1,0:T(8,128)(2,1)} %shard_map.155.mine), channel_id=1, source_target_pairs={{0,1},{1,0},{2,3},{3,2},{4,5},{5,4},{6,7},{7,6},{8,9},{9,8},{10,11... | collective-permute-start | bytes 11010056 | tf_op jit(solution)/shard_map/ppermute | solution.py:35
  55.2 2.7 %collective-permute-start.17 = (bf16[128,1280]{1,0:T(8,128)(2,1)S(1)}, bf16[128,1280]{1,0:T(8,128)(2,1)S(1)}, u32[]{:S(2)}, u32[]{:S(2)}) collective-permute-start(bf16[128,1280]{1,0:T(8,128)(2,1)S(1)} %slice.180), channel_id=1, source_target_pairs={{0,24},{8,0},{16,8},{24,16},{1,25},{9,1},{17,9},{25,17},{2,26},{10... | collective-permute-start | bytes 983048 | tf_op jit(solution)/shard_map/ppermute | solution.py:31
  58.0 1.7 collective-permute-done.7.above
  59.7 3.5 %collective-permute-start.9 = (bf16[128,1280]{1,0:T(8,128)(2,1)S(1)}, bf16[128,1280]{1,0:T(8,128)(2,1)S(1)}, u32[]{:S(2)}, u32[]{:S(2)}) collective-permute-start(bf16[128,1280]{1,0:T(8,128)(2,1)S(1)} %slice.176), channel_id=1, source_target_pairs={{0,96},{32,0},{64,32},{96,64},{1,97},{33,1},{65,33},{97,65},{2,98}... | collective-permute-start | bytes 983048 | tf_op jit(solution)/shard_map/ppermute | solution.py:31
  63.2 2.4 collective-permute-done.16.top
  65.6 1.4 shard_map.160
  67.0 2.7 %collective-permute-start.19 = (bf16[1024,512]{1,0:T(8,128)(2,1)S(1)}, bf16[1024,512]{1,0:T(8,128)(2,1)S(1)}, u32[]{:S(2)}, u32[]{:S(2)}) collective-permute-start(bf16[1024,512]{1,0:T(8,128)(2,1)S(1)} %get-tuple-element.31.refs_0_), channel_id=1, source_target_pairs={{0,96},{32,0},{64,32},{96,64},{1,97},{33,1},{65,33},{97,65},{2,98}... | collective-permute-start | bytes 3145736 | tf_op jit(solution)/shard_map/ppermute | solution.py:31
  69.7 1.3 shard_map.157
  71.0 2.7 %collective-permute-start.11 = (bf16[1024,512]{1,0:T(8,128)(2,1)S(1)}, bf16[1024,512]{1,0:T(8,128)(2,1)}, u32[]{:S(2)}, u32[]{:S(2)}) collective-permute-start(bf16[1024,512]{1,0:T(8,128)(2,1)S(1)} %get-tuple-element.27.refs_0_), channel_id=1, source_target_pairs={{0,24},{8,0},{16,8},{24,16},{1,25},{9,1},{17,9},{25,17},{2,26},{10... | collective-permute-start | bytes 3145736 | tf_op jit(solution)/shard_map/ppermute | solution.py:31
  74.7 16.1 %collective-permute-done.18.refs_1_ = bf16[1024,512]{1,0:T(8,128)(2,1)S(1)} collective-permute-done((bf16[1024,512]{1,0:T(8,128)(2,1)S(1)}, bf16[1024,512]{1,0:T(8,128)(2,1)S(1)}, u32[]{:S(2)}, u32[]{:S(2)}) %collective-permute-start.18) | collective-permute-done | bytes 1048608 | tf_op jit(solution)/shard_map/ppermute | solution.py:31
  93.6 3.5 %collective-permute-start.33 = (bf16[1024,768]{1,0:T(8,128)(2,1)}, bf16[1024,768]{1,0:T(8,128)(2,1)S(1)}, u32[]{:S(2)}, u32[]{:S(2)}) collective-permute-start(bf16[1024,768]{1,0:T(8,128)(2,1)} %get-tuple-element.42.refs_0_), channel_id=1, source_target_pairs={{0,96},{32,0},{64,32},{96,64},{1,97},{33,1},{65,33},{97,65},{2,98}... | collective-permute-start | bytes 4718600 | tf_op jit(solution)/shard_map/ppermute | solution.py:31
  97.2 2.7 %collective-permute-start.29 = (bf16[1024,768]{1,0:T(8,128)(2,1)}, bf16[1024,768]{1,0:T(8,128)(2,1)}, u32[]{:S(2)}, u32[]{:S(2)}) collective-permute-start(bf16[1024,768]{1,0:T(8,128)(2,1)} %get-tuple-element.41.refs_0_), channel_id=1, source_target_pairs={{0,24},{8,0},{16,8},{24,16},{1,25},{9,1},{17,9},{25,17},{2,26},{10... | collective-permute-start | bytes 4718600 | tf_op jit(solution)/shard_map/ppermute | solution.py:31
  100.9 1.1 slice.182
  102.0 1.1 slice.177
  103.1 1.1 slice.178
  104.2 21.1 %collective-permute-done.32.refs_1_ = bf16[1024,768]{1,0:T(8,128)(2,1)S(1)} collective-permute-done((bf16[1024,768]{1,0:T(8,128)(2,1)}, bf16[1024,768]{1,0:T(8,128)(2,1)S(1)}, u32[]{:S(2)}, u32[]{:S(2)}) %collective-permute-start.32) | collective-permute-done | bytes 1572896 | tf_op jit(solution)/shard_map/ppermute | solution.py:31
  125.3 3.7 %collective-permute-done.33.refs_2_ = bf16[1024,768]{1,0:T(8,128)(2,1)S(1)} collective-permute-done((bf16[1024,768]{1,0:T(8,128)(2,1)}, bf16[1024,768]{1,0:T(8,128)(2,1)S(1)}, u32[]{:S(2)}, u32[]{:S(2)}) %collective-permute-start.33) | collective-permute-done | bytes 1572896 | tf_op jit(solution)/shard_map/ppermute | solution.py:31
  129.0 3.4 %collective-permute-start.21 = (bf16[512,512]{1,0:T(8,128)(2,1)S(1)}, bf16[512,512]{1,0:T(8,128)(2,1)S(1)}, u32[]{:S(2)}, u32[]{:S(2)}) collective-permute-start(bf16[512,512]{1,0:T(8,128)(2,1)S(1)} %slice.182), channel_id=1, source_target_pairs={{0,96},{32,0},{64,32},{96,64},{1,97},{33,1},{65,33},{97,65},{2,98}... | collective-permute-start | bytes 1572872 | tf_op jit(solution)/shard_map/ppermute | solution.py:31
  132.6 1.2 slice.194
  133.8 2.7 %collective-permute-start.13 = (bf16[512,512]{1,0:T(8,128)(2,1)S(1)}, bf16[512,512]{1,0:T(8,128)(2,1)S(1)}, u32[]{:S(2)}, u32[]{:S(2)}) collective-permute-start(bf16[512,512]{1,0:T(8,128)(2,1)S(1)} %slice.178), channel_id=1, source_target_pairs={{0,24},{8,0},{16,8},{24,16},{1,25},{9,1},{17,9},{25,17},{2,26},{10... | collective-permute-start | bytes 1572872 | tf_op jit(solution)/shard_map/ppermute | solution.py:31
  136.5 1.2 slice.195
  138.0 3.7 %shard_map.156.x_ref = bf16[784,4096]{1,0:T(8,128)(2,1)S(1)} custom-call(bf16[448,4096]{1,0:T(8,128)(2,1)} %shard_map.155.mine, bf16[448,4096]{1,0:T(8,128)(2,1)} %collective-permute-done.5.other), custom_call_target="tpu_custom_call" | custom-call | flops 2000000000 | bytes 8000000 | tf_op jit(solution)/shard_map/pallas_call | solution.py:52
  141.8 3.1 %shard_map.161.acc_ref = f32[768,512]{1,0:T(8,128)S(1)} custom-call(bf16[784,4096]{1,0:T(8,128)(2,1)S(1)} %shard_map.156.x_ref, bf16[1024,512]{1,0:T(8,128)(2,1)S(1)} %copy-done.7, bf16[1024,512]{1,0:T(8,128)(2,1)S(1)} %copy-done.3, bf16[1024,512]{1,0:T(8,128)(2,1)S(1)} %copy-done.5), custom_call_target="tpu_custom_call" | custom-call | flops 3000000000 | bytes 8000000 | tf_op jit(solution)/shard_map/pallas_call | solution.py:52
  144.9 4.1 %shard_map.158.acc_ref = f32[768,512]{1,0:T(8,128)S(1)} custom-call(bf16[784,4096]{1,0:T(8,128)(2,1)S(1)} %shard_map.156.x_ref, bf16[1024,512]{1,0:T(8,128)(2,1)S(1)} %copy-done.9, bf16[1024,512]{1,0:T(8,128)(2,1)} %collective-permute-done.10.refs_1_, bf16[1024,512]{1,0:T(8,128)(2,1)} %collective-permute-done.11.refs_2_), custom_call_target="tpu_custom_call" | custom-call | flops 3000000000 | bytes 8000000 | tf_op jit(solution)/shard_map/pallas_call | solution.py:52
  149.1 2.6 %collective-permute-start.35 = (bf16[512,768]{1,0:T(8,128)(2,1)S(1)}, bf16[512,768]{1,0:T(8,128)(2,1)S(1)}, u32[]{:S(2)}, u32[]{:S(2)}) collective-permute-start(bf16[512,768]{1,0:T(8,128)(2,1)S(1)} %slice.197), channel_id=1, source_target_pairs={{0,96},{32,0},{64,32},{96,64},{1,97},{33,1},{65,33},{97,65},{2,98}... | collective-permute-start | bytes 2359304 | tf_op jit(solution)/shard_map/ppermute | solution.py:31
  151.7 1.4 shard_map.162.v_ref
  153.2 6.4 %shard_map.163 = (f32[768,256]{1,0:T(8,128)S(1)}, f32[768,256]{1,0:T(8,128)S(1)}, f32[768,256]{1,0:T(8,128)S(1)}, f32[768,256]{1,0:T(8,128)S(1)}, f32[12,256]{1,0:T(8,128)S(1)}, /*index=5*/f32[1,256]{1,0:T(1,128)S(1)}) custom-call(bf16[784,4096]{1,0:T(8,128)(2,1)S(1)} %shard_map.156.x_ref, bf16[64,4096]{1,0:T(8,128)(2,1)S(1)} %bitcast.23, ...), custom_call_target="tpu_custom_call" | custom-call | flops 4000000000 | bytes 8000000 | tf_op jit(solution)/shard_map/pallas_call | solution.py:52
  159.6 2.7 %collective-permute-start.31 = (bf16[512,768]{1,0:T(8,128)(2,1)S(1)}, bf16[512,768]{1,0:T(8,128)(2,1)S(1)}, u32[]{:S(2)}, u32[]{:S(2)}) collective-permute-start(bf16[512,768]{1,0:T(8,128)(2,1)S(1)} %slice.195), channel_id=1, source_target_pairs={{0,24},{8,0},{16,8},{24,16},{1,25},{9,1},{17,9},{25,17},{2,26},{10... | collective-permute-start | bytes 2359304 | tf_op jit(solution)/shard_map/ppermute | solution.py:31
  162.4 1.4 shard_map.159.qk_ref
  163.8 2.3 shard_map.164
  166.3 5.5 %shard_map.168.acc_ref = f32[784,768]{1,0:T(8,128)S(1)} custom-call(bf16[784,4096]{1,0:T(8,128)(2,1)S(1)} %shard_map.156.x_ref, bf16[1024,768]{1,0:T(8,128)(2,1)} %get-tuple-element.42.refs_0_, bf16[1024,768]{1,0:T(8,128)(2,1)S(1)} %collective-permute-done.32.refs_1_, bf16[1024,768]{1,0:T(8,128)(2,1)S(1)} %collective-permute-done.33.refs_2_), custom_call_target="tpu_custom_call" | custom-call | flops 3000000000 | bytes 8000000 | tf_op jit(solution)/shard_map/pallas_call | solution.py:52
  171.8 5.8 %shard_map.166.acc_ref = f32[784,768]{1,0:T(8,128)S(1)} custom-call(bf16[784,4096]{1,0:T(8,128)(2,1)S(1)} %shard_map.156.x_ref, bf16[1024,768]{1,0:T(8,128)(2,1)} %get-tuple-element.41.refs_0_, bf16[1024,768]{1,0:T(8,128)(2,1)} %collective-permute-done.28.refs_1_, bf16[1024,768]{1,0:T(8,128)(2,1)} %collective-permute-done.29.refs_2_), custom_call_target="tpu_custom_call" | custom-call | flops 3000000000 | bytes 8000000 | tf_op jit(solution)/shard_map/pallas_call | solution.py:52
  179.4 1.8 shard_map.169.b_ref
  181.3 2.1 collective-permute-done.23
  183.4 1.4 collective-permute-done.24
  185.1 1.3 collective-permute-start.25
  186.4 3.2 %collective-permute-start.26 = (bf16[2,272,128]{2,1,0:T(8,128)(2,1)S(1)}, bf16[2,272,128]{2,1,0:T(8,128)(2,1)S(1)}, u32[]{:S(2)}, u32[]{:S(2)}) collective-permute-start(bf16[2,272,128]{2,1,0:T(8,128)(2,1)S(1)} %pad_maximum_fusion.3), channel_id=1, source_target_pairs={{0,32},{32,64},{64,96},{1,33},{33,65},{65,97},{2,34},{34,66},{66,9... | collective-permute-start | bytes 417800 | tf_op jit(solution)/shard_map/ppermute | solution.py:40
  189.6 1.9 shard_map.167.t_ref
  191.5 1.3 collective-permute-start.27
  192.9 3.4 %collective-permute-done.27 = bf16[2,272,128]{2,1,0:T(8,128)(2,1)S(1)} collective-permute-done((bf16[2,272,128]{2,1,0:T(8,128)(2,1)S(1)}, bf16[2,272,128]{2,1,0:T(8,128)(2,1)S(1)}, u32[]{:S(2)}, u32[]{:S(2)}) %collective-permute-start.27) | collective-permute-done | bytes 139296 | tf_op jit(solution)/shard_map/ppermute | solution.py:40
  197.0 1.4 copy-done
  198.4 3.1 %shard_map.172 = (f32[96,4096]{1,0:T(8,128)S(1)}, bf16[96,4096]{1,0:T(8,128)(2,1)S(1)}) custom-call(bf16[768,512]{1,0:T(8,128)(2,1)S(1)} %shard_map.165.attn_ref, bf16[768,256]{1,0:T(8,128)(2,1)S(1)} %shard_map.167.t_ref, bf16[768,256]{1,0:T(8,128)(2,1)S(1)} %shard_map.169.b_ref, bf16[512,4096]{1,0:T(8,128)(2,1)S(1)} %copy-done, bf16[512,4096]{1,0:T(8,128)(2,1)S(1)} %copy-done.1), custom_call_target="tpu_custom_call" | custom-call | flops 2000000000 | bytes 8000000 | tf_op jit(solution)/shard_map/pallas_call | solution.py:52
  201.6 5.5 %collective-permute-start.38 = (bf16[96,4096]{1,0:T(8,128)(2,1)S(1)}, bf16[96,4096]{1,0:T(8,128)(2,1)S(1)}, u32[]{:S(2)}, u32[]{:S(2)}) collective-permute-start(bf16[96,4096]{1,0:T(8,128)(2,1)S(1)} %get-tuple-element.48), channel_id=1, source_target_pairs={{0,1},{1,0},{2,3},{3,2},{4,5},{5,4},{6,7},{7,6},{8,9},{9,8},{10,11... | collective-permute-start | bytes 2359304 | tf_op jit(solution)/shard_map/ppermute | solution.py:35
  207.0 4.8 %shard_map.171 = (f32[192,4096]{1,0:T(8,128)S(1)}, bf16[192,4096]{1,0:T(8,128)(2,1)S(1)}) custom-call(bf16[768,512]{1,0:T(8,128)(2,1)S(1)} %shard_map.165.attn_ref, bf16[768,256]{1,0:T(8,128)(2,1)S(1)} %shard_map.167.t_ref, bf16[768,256]{1,0:T(8,128)(2,1)S(1)} %shard_map.169.b_ref, bf16[512,4096]{1,0:T(8,128)(2,1)S(1)} %copy-done, ...), custom_call_target="tpu_custom_call" | custom-call | flops 2000000000 | bytes 8000000 | tf_op jit(solution)/shard_map/pallas_call | solution.py:52
  211.9 3.1 %shard_map.170 = (f32[96,4096]{1,0:T(8,128)S(1)}, bf16[96,4096]{1,0:T(8,128)(2,1)S(1)}) custom-call(bf16[768,512]{1,0:T(8,128)(2,1)S(1)} %shard_map.165.attn_ref, bf16[768,256]{1,0:T(8,128)(2,1)S(1)} %shard_map.167.t_ref, bf16[768,256]{1,0:T(8,128)(2,1)S(1)} %shard_map.169.b_ref, bf16[512,4096]{1,0:T(8,128)(2,1)S(1)} %copy-done, bf16[512,4096]{1,0:T(8,128)(2,1)S(1)} %copy-done.1), custom_call_target="tpu_custom_call" | custom-call | flops 2000000000 | bytes 8000000 | tf_op jit(solution)/shard_map/pallas_call | solution.py:52
  215.9 2.7 %collective-permute-start.43 = (bf16[48,4096]{1,0:T(8,128)(2,1)S(1)}, bf16[48,4096]{1,0:T(8,128)(2,1)S(1)}, u32[]{:S(2)}, u32[]{:S(2)}) collective-permute-start(bf16[48,4096]{1,0:T(8,128)(2,1)S(1)} %get-tuple-element.64), channel_id=1, source_target_pairs={{0,6},{2,0},{4,2},{6,4},{1,7},{3,1},{5,3},{7,5},{8,14},{10,8},{12,... | collective-permute-start | bytes 1179656 | tf_op jit(solution)/shard_map/ppermute | solution.py:31
  219.1 8.6 %collective-permute-done.39 = bf16[48,4096]{1,0:T(8,128)(2,1)S(1)} collective-permute-done((bf16[48,4096]{1,0:T(8,128)(2,1)S(1)}, bf16[48,4096]{1,0:T(8,128)(2,1)S(1)}, u32[]{:S(2)}, u32[]{:S(2)}) %collective-permute-start.39) | collective-permute-done | bytes 393248 | tf_op jit(solution)/shard_map/ppermute | solution.py:31
  228.0 2.7 %collective-permute-start.44 = (bf16[48,4096]{1,0:T(8,128)(2,1)S(1)}, bf16[48,4096]{1,0:T(8,128)(2,1)S(1)}, u32[]{:S(2)}, u32[]{:S(2)}) collective-permute-start(bf16[48,4096]{1,0:T(8,128)(2,1)S(1)} %get-tuple-element.60), channel_id=1, source_target_pairs={{0,6},{2,0},{4,2},{6,4},{1,7},{3,1},{5,3},{7,5},{8,14},{10,8},{12,... | collective-permute-start | bytes 1179656 | tf_op jit(solution)/shard_map/ppermute | solution.py:31
  230.8 2.7 %collective-permute-start.42 = (bf16[48,4096]{1,0:T(8,128)(2,1)S(1)}, bf16[48,4096]{1,0:T(8,128)(2,1)S(1)}, u32[]{:S(2)}, u32[]{:S(2)}) collective-permute-start(bf16[48,4096]{1,0:T(8,128)(2,1)S(1)} %get-tuple-element.62), channel_id=1, source_target_pairs={{0,6},{2,0},{4,2},{6,4},{1,7},{3,1},{5,3},{7,5},{8,14},{10,8},{12,... | collective-permute-start | bytes 1179656 | tf_op jit(solution)/shard_map/ppermute | solution.py:31
  233.5 5.5 %collective-permute-done.40 = bf16[48,4096]{1,0:T(8,128)(2,1)S(1)} collective-permute-done((bf16[48,4096]{1,0:T(8,128)(2,1)S(1)}, bf16[48,4096]{1,0:T(8,128)(2,1)S(1)}, u32[]{:S(2)}, u32[]{:S(2)}) %collective-permute-start.40) | collective-permute-done | bytes 393248 | tf_op jit(solution)/shard_map/ppermute | solution.py:31
  239.0 8.4 %collective-permute-done.41 = bf16[48,4096]{1,0:T(8,128)(2,1)S(1)} collective-permute-done((bf16[48,4096]{1,0:T(8,128)(2,1)S(1)}, bf16[48,4096]{1,0:T(8,128)(2,1)S(1)}, u32[]{:S(2)}, u32[]{:S(2)}) %collective-permute-start.41) | collective-permute-done | bytes 393248 | tf_op jit(solution)/shard_map/ppermute | solution.py:31
  247.4 1.3 add_convert_fusion
  (143 shorter events, 12.2 us)
Async XLA Ops:
  2.3 9.0 %slice-start = ((bf16[256,512]{1,0:T(8,128)(2,1)}), bf16[256,256]{1,0:T(8,128)(2,1)S(1)}, s32[]{:S(2)}) async-start(bf16[256,512]{1,0:T(8,128)(2,1)} %param.21), calls=%async_computation | async-start | bytes 262144 | tf_op jit(solution)/shard_map/slice | solution.py:505
  2.3 9.0 %slice-start.1 = ((bf16[256,512]{1,0:T(8,128)(2,1)}), bf16[256,256]{1,0:T(8,128)(2,1)S(1)}, s32[]{:S(2)}) async-start(bf16[256,512]{1,0:T(8,128)(2,1)} %param.22), calls=%async_computation.1 | async-start | bytes 262144 | tf_op jit(solution)/shard_map/slice | solution.py:505
  2.3 9.0 %slice-start.2 = ((bf16[256,512]{1,0:T(8,128)(2,1)}), bf16[256,256]{1,0:T(8,128)(2,1)S(1)}, s32[]{:S(2)}) async-start(bf16[256,512]{1,0:T(8,128)(2,1)} %param.23), calls=%async_computation.2 | async-start | bytes 262144 | tf_op jit(solution)/shard_map/slice | solution.py:505
  2.3 9.0 %copy-start.19 = (bf16[256,512]{1,0:T(8,128)(2,1)S(1)}, bf16[256,512]{1,0:T(8,128)(2,1)}, u32[]{:S(2)}) copy-start(bf16[256,512]{1,0:T(8,128)(2,1)} %param.20) | copy-start | bytes 786436
  2.4 12.9 %copy-start.20 = (bf16[256,256]{1,0:T(8,128)(2,1)S(1)}, bf16[256,256]{1,0:T(8,128)(2,1)}, u32[]{:S(2)}) copy-start(bf16[256,256]{1,0:T(8,128)(2,1)} %param.18) | copy-start | bytes 393220
  2.4 6.3 %collective-permute-start = (bf16[16,4096]{1,0:T(8,128)(2,1)S(1)}, bf16[16,4096]{1,0:T(8,128)(2,1)S(1)}, u32[]{:S(2)}, u32[]{:S(2)}) collective-permute-start(bf16[16,4096]{1,0:T(8,128)(2,1)S(1)} %slice.172), channel_id=1, source_target_pairs={{0,8},{8,16},{16,24},{24,32},{32,40},{40,48},{48,56},{56,64},{64,7... | collective-permute-start | bytes 393224 | tf_op jit(solution)/shard_map/ppermute | solution.py:40
  8.8 6.5 %copy-start.21 = (bf16[256,256]{1,0:T(8,128)(2,1)S(1)}, bf16[256,256]{1,0:T(8,128)(2,1)}, u32[]{:S(2)}) copy-start(bf16[256,256]{1,0:T(8,128)(2,1)} %param.19) | copy-start | bytes 393220
  8.8 20.7 %collective-permute-start.2 = (bf16[112,4096]{1,0:T(8,128)(2,1)S(1)}, bf16[112,4096]{1,0:T(8,128)(2,1)S(1)}, u32[]{:S(2)}, u32[]{:S(2)}) collective-permute-start(bf16[112,4096]{1,0:T(8,128)(2,1)S(1)} %pad_maximum_fusion.own), channel_id=1, source_target_pairs={{0,6},{2,0},{4,2},{6,4},{1,7},{3,1},{5,3},{7,5},{8,14},{10,8},{12,... | collective-permute-start | bytes 2752520 | tf_op jit(solution)/shard_map/ppermute | solution.py:31
  11.3 21.7 %collective-permute-start.1 = (bf16[112,4096]{1,0:T(8,128)(2,1)S(1)}, bf16[112,4096]{1,0:T(8,128)(2,1)S(1)}, u32[]{:S(2)}, u32[]{:S(2)}) collective-permute-start(bf16[112,4096]{1,0:T(8,128)(2,1)S(1)} %pad_maximum_fusion.own), channel_id=1, source_target_pairs={{0,2},{2,4},{4,6},{6,0},{1,3},{3,5},{5,7},{7,1},{8,10},{10,12},{12... | collective-permute-start | bytes 2752520 | tf_op jit(solution)/shard_map/ppermute | solution.py:31
  11.3 21.7 %copy-start.16 = (bf16[256,512]{1,0:T(8,128)(2,1)S(1)}, bf16[256,512]{1,0:T(8,128)(2,1)}, u32[]{:S(2)}) copy-start(bf16[256,512]{1,0:T(8,128)(2,1)} %param.21) | copy-start | bytes 786436
  11.4 21.8 %copy-start.17 = (bf16[256,512]{1,0:T(8,128)(2,1)S(1)}, bf16[256,512]{1,0:T(8,128)(2,1)}, u32[]{:S(2)}) copy-start(bf16[256,512]{1,0:T(8,128)(2,1)} %param.22) | copy-start | bytes 786436
  11.4 21.8 %copy-start.18 = (bf16[256,512]{1,0:T(8,128)(2,1)S(1)}, bf16[256,512]{1,0:T(8,128)(2,1)}, u32[]{:S(2)}) copy-start(bf16[256,512]{1,0:T(8,128)(2,1)} %param.23) | copy-start | bytes 786436
  11.4 43.6 %collective-permute-start.14 = (bf16[256,1280]{1,0:T(8,128)(2,1)S(1)}, bf16[256,1280]{1,0:T(8,128)(2,1)S(1)}, u32[]{:S(2)}, u32[]{:S(2)}) collective-permute-start(bf16[256,1280]{1,0:T(8,128)(2,1)S(1)} %pad_maximum_fusion.1.own), channel_id=1, source_target_pairs={{0,8},{8,16},{16,24},{24,0},{1,9},{9,17},{17,25},{25,1},{2,10},{10... | collective-permute-start | bytes 1966088 | tf_op jit(solution)/shard_map/ppermute | solution.py:31
  13.7 41.4 %collective-permute-start.15 = (bf16[256,1280]{1,0:T(8,128)(2,1)S(1)}, bf16[256,1280]{1,0:T(8,128)(2,1)S(1)}, u32[]{:S(2)}, u32[]{:S(2)}) collective-permute-start(bf16[256,1280]{1,0:T(8,128)(2,1)S(1)} %pad_maximum_fusion.1.own), channel_id=1, source_target_pairs={{0,24},{8,0},{16,8},{24,16},{1,25},{9,1},{17,9},{25,17},{2,26},{10... | collective-permute-start | bytes 1966088 | tf_op jit(solution)/shard_map/ppermute | solution.py:31
  29.5 19.6 %collective-permute-start.4 = (bf16[64,4096]{1,0:T(8,128)(2,1)S(1)}, bf16[64,4096]{1,0:T(8,128)(2,1)S(1)}, u32[]{:S(2)}, u32[]{:S(2)}) collective-permute-start(bf16[64,4096]{1,0:T(8,128)(2,1)S(1)} %slice.174), channel_id=1, source_target_pairs={{0,6},{2,0},{4,2},{6,4},{1,7},{3,1},{5,3},{7,5},{8,14},{10,8},{12,... | collective-permute-start | bytes 1572872 | tf_op jit(solution)/shard_map/ppermute | solution.py:31
  33.1 9.3 %collective-permute-start.3 = (bf16[48,4096]{1,0:T(8,128)(2,1)S(1)}, bf16[48,4096]{1,0:T(8,128)(2,1)S(1)}, u32[]{:S(2)}, u32[]{:S(2)}) collective-permute-start(bf16[48,4096]{1,0:T(8,128)(2,1)S(1)} %slice.173), channel_id=1, source_target_pairs={{0,2},{2,4},{4,6},{6,0},{1,3},{3,5},{5,7},{7,1},{8,10},{10,12},{12... | collective-permute-start | bytes 1179656 | tf_op jit(solution)/shard_map/ppermute | solution.py:31
  33.2 24.7 %collective-permute-start.6 = (bf16[256,1280]{1,0:T(8,128)(2,1)S(1)}, bf16[256,1280]{1,0:T(8,128)(2,1)S(1)}, u32[]{:S(2)}, u32[]{:S(2)}) collective-permute-start(bf16[256,1280]{1,0:T(8,128)(2,1)S(1)} %slice_dynamic-update-slice_fusion.own), channel_id=1, source_target_pairs={{0,32},{32,64},{64,96},{96,0},{1,33},{33,65},{65,97},{97,1},{2,34}... | collective-permute-start | bytes 1966088 | tf_op jit(solution)/shard_map/ppermute | solution.py:31
  42.4 17.3 %collective-permute-start.7 = (bf16[256,1280]{1,0:T(8,128)(2,1)S(1)}, bf16[256,1280]{1,0:T(8,128)(2,1)S(1)}, u32[]{:S(2)}, u32[]{:S(2)}) collective-permute-start(bf16[256,1280]{1,0:T(8,128)(2,1)S(1)} %slice_dynamic-update-slice_fusion.own), channel_id=1, source_target_pairs={{0,96},{32,0},{64,32},{96,64},{1,97},{33,1},{65,33},{97,65},{2,98}... | collective-permute-start | bytes 1966088 | tf_op jit(solution)/shard_map/ppermute | solution.py:31
  51.2 86.5 %collective-permute-start.5 = (bf16[448,4096]{1,0:T(8,128)(2,1)}, bf16[448,4096]{1,0:T(8,128)(2,1)}, u32[]{:S(2)}, u32[]{:S(2)}) collective-permute-start(bf16[448,4096]{1,0:T(8,128)(2,1)} %shard_map.155.mine), channel_id=1, source_target_pairs={{0,1},{1,0},{2,3},{3,2},{4,5},{5,4},{6,7},{7,6},{8,9},{9,8},{10,11... | collective-permute-start | bytes 11010056 | tf_op jit(solution)/shard_map/ppermute | solution.py:35
  55.1 10.5 %collective-permute-start.16 = (bf16[128,1280]{1,0:T(8,128)(2,1)S(1)}, bf16[128,1280]{1,0:T(8,128)(2,1)S(1)}, u32[]{:S(2)}, u32[]{:S(2)}) collective-permute-start(bf16[128,1280]{1,0:T(8,128)(2,1)S(1)} %slice.179), channel_id=1, source_target_pairs={{0,8},{8,16},{16,24},{24,0},{1,9},{9,17},{17,25},{25,1},{2,10},{10... | collective-permute-start | bytes 983048 | tf_op jit(solution)/shard_map/ppermute | solution.py:31
  55.2 10.4 %collective-permute-start.17 = (bf16[128,1280]{1,0:T(8,128)(2,1)S(1)}, bf16[128,1280]{1,0:T(8,128)(2,1)S(1)}, u32[]{:S(2)}, u32[]{:S(2)}) collective-permute-start(bf16[128,1280]{1,0:T(8,128)(2,1)S(1)} %slice.180), channel_id=1, source_target_pairs={{0,24},{8,0},{16,8},{24,16},{1,25},{9,1},{17,9},{25,17},{2,26},{10... | collective-permute-start | bytes 983048 | tf_op jit(solution)/shard_map/ppermute | solution.py:31
  57.9 11.7 %collective-permute-start.8 = (bf16[128,1280]{1,0:T(8,128)(2,1)S(1)}, bf16[128,1280]{1,0:T(8,128)(2,1)S(1)}, u32[]{:S(2)}, u32[]{:S(2)}) collective-permute-start(bf16[128,1280]{1,0:T(8,128)(2,1)S(1)} %slice.175), channel_id=1, source_target_pairs={{0,32},{32,64},{64,96},{96,0},{1,33},{33,65},{65,97},{97,1},{2,34}... | collective-permute-start | bytes 983048 | tf_op jit(solution)/shard_map/ppermute | solution.py:31
  59.7 9.9 %collective-permute-start.9 = (bf16[128,1280]{1,0:T(8,128)(2,1)S(1)}, bf16[128,1280]{1,0:T(8,128)(2,1)S(1)}, u32[]{:S(2)}, u32[]{:S(2)}) collective-permute-start(bf16[128,1280]{1,0:T(8,128)(2,1)S(1)} %slice.176), channel_id=1, source_target_pairs={{0,96},{32,0},{64,32},{96,64},{1,97},{33,1},{65,33},{97,65},{2,98}... | collective-permute-start | bytes 983048 | tf_op jit(solution)/shard_map/ppermute | solution.py:31
  67.0 4.0 %copy-start.6 = (bf16[1024,512]{1,0:T(8,128)(2,1)}, bf16[1024,512]{1,0:T(8,128)(2,1)S(1)}, u32[]{:S(2)}) copy-start(bf16[1024,512]{1,0:T(8,128)(2,1)S(1)} %get-tuple-element.31.refs_0_) | copy-start | bytes 3145732
  67.0 32.8 %copy-start.22 = (bf16[3,512]{1,0:T(4,128)(2,1)S(1)}, bf16[3,512]{1,0:T(4,128)(2,1)}, u32[]{:S(2)}) copy-start(bf16[3,512]{1,0:T(4,128)(2,1)} %param.29) | copy-start | bytes 9220
  67.0 23.8 %collective-permute-start.18 = (bf16[1024,512]{1,0:T(8,128)(2,1)S(1)}, bf16[1024,512]{1,0:T(8,128)(2,1)S(1)}, u32[]{:S(2)}, u32[]{:S(2)}) collective-permute-start(bf16[1024,512]{1,0:T(8,128)(2,1)S(1)} %get-tuple-element.31.refs_0_), channel_id=1, source_target_pairs={{0,32},{32,64},{64,96},{96,0},{1,33},{33,65},{65,97},{97,1},{2,34}... | collective-permute-start | bytes 3145736 | tf_op jit(solution)/shard_map/ppermute | solution.py:31
  67.0 25.6 %collective-permute-start.19 = (bf16[1024,512]{1,0:T(8,128)(2,1)S(1)}, bf16[1024,512]{1,0:T(8,128)(2,1)S(1)}, u32[]{:S(2)}, u32[]{:S(2)}) collective-permute-start(bf16[1024,512]{1,0:T(8,128)(2,1)S(1)} %get-tuple-element.31.refs_0_), channel_id=1, source_target_pairs={{0,96},{32,0},{64,32},{96,64},{1,97},{33,1},{65,33},{97,65},{2,98}... | collective-permute-start | bytes 3145736 | tf_op jit(solution)/shard_map/ppermute | solution.py:31
  71.0 26.1 %collective-permute-start.10 = (bf16[1024,512]{1,0:T(8,128)(2,1)S(1)}, bf16[1024,512]{1,0:T(8,128)(2,1)}, u32[]{:S(2)}, u32[]{:S(2)}) collective-permute-start(bf16[1024,512]{1,0:T(8,128)(2,1)S(1)} %get-tuple-element.27.refs_0_), channel_id=1, source_target_pairs={{0,8},{8,16},{16,24},{24,0},{1,9},{9,17},{17,25},{25,1},{2,10},{10... | collective-permute-start | bytes 3145736 | tf_op jit(solution)/shard_map/ppermute | solution.py:31
  71.0 26.1 %collective-permute-start.11 = (bf16[1024,512]{1,0:T(8,128)(2,1)S(1)}, bf16[1024,512]{1,0:T(8,128)(2,1)}, u32[]{:S(2)}, u32[]{:S(2)}) collective-permute-start(bf16[1024,512]{1,0:T(8,128)(2,1)S(1)} %get-tuple-element.27.refs_0_), channel_id=1, source_target_pairs={{0,24},{8,0},{16,8},{24,16},{1,25},{9,1},{17,9},{25,17},{2,26},{10... | collective-permute-start | bytes 3145736 | tf_op jit(solution)/shard_map/ppermute | solution.py:31
  90.8 34.5 %collective-permute-start.32 = (bf16[1024,768]{1,0:T(8,128)(2,1)}, bf16[1024,768]{1,0:T(8,128)(2,1)S(1)}, u32[]{:S(2)}, u32[]{:S(2)}) collective-permute-start(bf16[1024,768]{1,0:T(8,128)(2,1)} %get-tuple-element.42.refs_0_), channel_id=1, source_target_pairs={{0,32},{32,64},{64,96},{96,0},{1,33},{33,65},{65,97},{97,1},{2,34}... | collective-permute-start | bytes 4718600 | tf_op jit(solution)/shard_map/ppermute | solution.py:31
  93.6 35.4 %collective-permute-start.33 = (bf16[1024,768]{1,0:T(8,128)(2,1)}, bf16[1024,768]{1,0:T(8,128)(2,1)S(1)}, u32[]{:S(2)}, u32[]{:S(2)}) collective-permute-start(bf16[1024,768]{1,0:T(8,128)(2,1)} %get-tuple-element.42.refs_0_), channel_id=1, source_target_pairs={{0,96},{32,0},{64,32},{96,64},{1,97},{33,1},{65,33},{97,65},{2,98}... | collective-permute-start | bytes 4718600 | tf_op jit(solution)/shard_map/ppermute | solution.py:31
  97.1 35.4 %collective-permute-start.28 = (bf16[1024,768]{1,0:T(8,128)(2,1)}, bf16[1024,768]{1,0:T(8,128)(2,1)}, u32[]{:S(2)}, u32[]{:S(2)}) collective-permute-start(bf16[1024,768]{1,0:T(8,128)(2,1)} %get-tuple-element.41.refs_0_), channel_id=1, source_target_pairs={{0,8},{8,16},{16,24},{24,0},{1,9},{9,17},{17,25},{25,1},{2,10},{10... | collective-permute-start | bytes 4718600 | tf_op jit(solution)/shard_map/ppermute | solution.py:31
  97.2 36.6 %collective-permute-start.29 = (bf16[1024,768]{1,0:T(8,128)(2,1)}, bf16[1024,768]{1,0:T(8,128)(2,1)}, u32[]{:S(2)}, u32[]{:S(2)}) collective-permute-start(bf16[1024,768]{1,0:T(8,128)(2,1)} %get-tuple-element.41.refs_0_), channel_id=1, source_target_pairs={{0,24},{8,0},{16,8},{24,16},{1,25},{9,1},{17,9},{25,17},{2,26},{10... | collective-permute-start | bytes 4718600 | tf_op jit(solution)/shard_map/ppermute | solution.py:31
  125.2 23.9 %collective-permute-start.20 = (bf16[512,512]{1,0:T(8,128)(2,1)S(1)}, bf16[512,512]{1,0:T(8,128)(2,1)S(1)}, u32[]{:S(2)}, u32[]{:S(2)}) collective-permute-start(bf16[512,512]{1,0:T(8,128)(2,1)S(1)} %slice.181), channel_id=1, source_target_pairs={{0,32},{32,64},{64,96},{96,0},{1,33},{33,65},{65,97},{97,1},{2,34}... | collective-permute-start | bytes 1572872 | tf_op jit(solution)/shard_map/ppermute | solution.py:31
  129.0 22.7 %collective-permute-start.21 = (bf16[512,512]{1,0:T(8,128)(2,1)S(1)}, bf16[512,512]{1,0:T(8,128)(2,1)S(1)}, u32[]{:S(2)}, u32[]{:S(2)}) collective-permute-start(bf16[512,512]{1,0:T(8,128)(2,1)S(1)} %slice.182), channel_id=1, source_target_pairs={{0,96},{32,0},{64,32},{96,64},{1,97},{33,1},{65,33},{97,65},{2,98}... | collective-permute-start | bytes 1572872 | tf_op jit(solution)/shard_map/ppermute | solution.py:31
  132.5 27.1 %collective-permute-start.12 = (bf16[512,512]{1,0:T(8,128)(2,1)S(1)}, bf16[512,512]{1,0:T(8,128)(2,1)S(1)}, u32[]{:S(2)}, u32[]{:S(2)}) collective-permute-start(bf16[512,512]{1,0:T(8,128)(2,1)S(1)} %slice.177), channel_id=1, source_target_pairs={{0,8},{8,16},{16,24},{24,0},{1,9},{9,17},{17,25},{25,1},{2,10},{10... | collective-permute-start | bytes 1572872 | tf_op jit(solution)/shard_map/ppermute | solution.py:31
  133.8 28.6 %collective-permute-start.13 = (bf16[512,512]{1,0:T(8,128)(2,1)S(1)}, bf16[512,512]{1,0:T(8,128)(2,1)S(1)}, u32[]{:S(2)}, u32[]{:S(2)}) collective-permute-start(bf16[512,512]{1,0:T(8,128)(2,1)S(1)} %slice.178), channel_id=1, source_target_pairs={{0,24},{8,0},{16,8},{24,16},{1,25},{9,1},{17,9},{25,17},{2,26},{10... | collective-permute-start | bytes 1572872 | tf_op jit(solution)/shard_map/ppermute | solution.py:31
  137.7 4.0 %copy-start.3 = (bf16[1024,512]{1,0:T(8,128)(2,1)S(1)}, bf16[1024,512]{1,0:T(8,128)(2,1)}, u32[]{:S(2)}) copy-start(bf16[1024,512]{1,0:T(8,128)(2,1)} %copy-done.2) | copy-start | bytes 3145732
  137.7 4.0 %copy-start.5 = (bf16[1024,512]{1,0:T(8,128)(2,1)S(1)}, bf16[1024,512]{1,0:T(8,128)(2,1)}, u32[]{:S(2)}) copy-start(bf16[1024,512]{1,0:T(8,128)(2,1)} %copy-done.4) | copy-start | bytes 3145732
  137.7 39.8 %collective-permute-start.34 = (bf16[512,768]{1,0:T(8,128)(2,1)S(1)}, bf16[512,768]{1,0:T(8,128)(2,1)S(1)}, u32[]{:S(2)}, u32[]{:S(2)}) collective-permute-start(bf16[512,768]{1,0:T(8,128)(2,1)S(1)} %slice.196), channel_id=1, source_target_pairs={{0,32},{32,64},{64,96},{96,0},{1,33},{33,65},{65,97},{97,1},{2,34}... | collective-permute-start | bytes 2359304 | tf_op jit(solution)/shard_map/ppermute | solution.py:31
  149.1 4.1 %copy-start.12 = (bf16[4096,64]{0,1:T(8,128)(2,1)S(1)}, bf16[4096,64]{0,1:T(8,128)(2,1)}, u32[]{:S(2)}) copy-start(bf16[4096,64]{0,1:T(8,128)(2,1)} %param.24) | copy-start | bytes 1572868
  149.1 4.1 %copy-start.13 = (bf16[64,256]{1,0:T(8,128)(2,1)S(1)}, bf16[64,256]{1,0:T(8,128)(2,1)}, u32[]{:S(2)}) copy-start(bf16[64,256]{1,0:T(8,128)(2,1)} %right_ref.1) | copy-start | bytes 98308
  149.1 4.1 %copy-start.14 = (f32[2,768]{1,0:T(2,128)S(1)}, f32[2,768]{1,0:T(2,128)}, u32[]{:S(2)}) copy-start(f32[2,768]{1,0:T(2,128)} %spike_ref.1) | copy-start | bytes 18436
  149.1 4.1 %copy-start.15 = (f32[256]{0:T(256)S(1)}, f32[256]{0:T(256)}, u32[]{:S(2)}) copy-start(f32[256]{0:T(256)} %param.26) | copy-start | bytes 3076
  149.1 29.4 %collective-permute-start.35 = (bf16[512,768]{1,0:T(8,128)(2,1)S(1)}, bf16[512,768]{1,0:T(8,128)(2,1)S(1)}, u32[]{:S(2)}, u32[]{:S(2)}) collective-permute-start(bf16[512,768]{1,0:T(8,128)(2,1)S(1)} %slice.197), channel_id=1, source_target_pairs={{0,96},{32,0},{64,32},{96,64},{1,97},{33,1},{65,33},{97,65},{2,98}... | collective-permute-start | bytes 2359304 | tf_op jit(solution)/shard_map/ppermute | solution.py:31
  151.7 37.9 %collective-permute-start.30 = (bf16[512,768]{1,0:T(8,128)(2,1)S(1)}, bf16[512,768]{1,0:T(8,128)(2,1)S(1)}, u32[]{:S(2)}, u32[]{:S(2)}) collective-permute-start(bf16[512,768]{1,0:T(8,128)(2,1)S(1)} %slice.194), channel_id=1, source_target_pairs={{0,8},{8,16},{16,24},{24,0},{1,9},{9,17},{17,25},{25,1},{2,10},{10... | collective-permute-start | bytes 2359304 | tf_op jit(solution)/shard_map/ppermute | solution.py:31
  159.6 30.0 %collective-permute-start.31 = (bf16[512,768]{1,0:T(8,128)(2,1)S(1)}, bf16[512,768]{1,0:T(8,128)(2,1)S(1)}, u32[]{:S(2)}, u32[]{:S(2)}) collective-permute-start(bf16[512,768]{1,0:T(8,128)(2,1)S(1)} %slice.195), channel_id=1, source_target_pairs={{0,24},{8,0},{16,8},{24,16},{1,25},{9,1},{17,9},{25,17},{2,26},{10... | collective-permute-start | bytes 2359304 | tf_op jit(solution)/shard_map/ppermute | solution.py:31
  166.2 15.0 %collective-permute-start.22 = (bf16[2,272,128]{2,1,0:T(8,128)(2,1)S(1)}, bf16[2,272,128]{2,1,0:T(8,128)(2,1)S(1)}, u32[]{:S(2)}, u32[]{:S(2)}) collective-permute-start(bf16[2,272,128]{2,1,0:T(8,128)(2,1)S(1)} %pad_maximum_fusion.2), channel_id=1, source_target_pairs={{0,24},{8,0},{16,8},{24,16},{1,25},{9,1},{17,9},{25,17},{2,26},{10... | collective-permute-start | bytes 417800 | tf_op jit(solution)/shard_map/ppermute | solution.py:31
  177.6 5.8 %collective-permute-start.23 = (bf16[2,272,128]{2,1,0:T(8,128)(2,1)S(1)}, bf16[2,272,128]{2,1,0:T(8,128)(2,1)S(1)}, u32[]{:S(2)}, u32[]{:S(2)}) collective-permute-start(bf16[2,272,128]{2,1,0:T(8,128)(2,1)S(1)} %pad_maximum_fusion.2), channel_id=1, source_target_pairs={{0,16},{8,24},{16,0},{24,8},{1,17},{9,25},{17,1},{25,9},{2,18},{10... | collective-permute-start | bytes 417800 | tf_op jit(solution)/shard_map/ppermute | solution.py:31
  178.5 6.3 %collective-permute-start.24 = (bf16[2,272,128]{2,1,0:T(8,128)(2,1)S(1)}, bf16[2,272,128]{2,1,0:T(8,128)(2,1)S(1)}, u32[]{:S(2)}, u32[]{:S(2)}) collective-permute-start(bf16[2,272,128]{2,1,0:T(8,128)(2,1)S(1)} %pad_maximum_fusion.2), channel_id=1, source_target_pairs={{0,8},{8,16},{16,24},{24,0},{1,9},{9,17},{17,25},{25,1},{2,10},{10... | collective-permute-start | bytes 417800 | tf_op jit(solution)/shard_map/ppermute | solution.py:31
  185.1 7.7 %collective-permute-start.25 = (bf16[2,272,128]{2,1,0:T(8,128)(2,1)S(1)}, bf16[2,272,128]{2,1,0:T(8,128)(2,1)S(1)}, u32[]{:S(2)}, u32[]{:S(2)}) collective-permute-start(bf16[2,272,128]{2,1,0:T(8,128)(2,1)S(1)} %pad_maximum_fusion.3), channel_id=1, source_target_pairs={{0,64},{32,96},{1,65},{33,97},{2,66},{34,98},{3,67},{35,99},{4,68}... | collective-permute-start | bytes 417800 | tf_op jit(solution)/shard_map/ppermute | solution.py:40
  186.4 6.5 %collective-permute-start.26 = (bf16[2,272,128]{2,1,0:T(8,128)(2,1)S(1)}, bf16[2,272,128]{2,1,0:T(8,128)(2,1)S(1)}, u32[]{:S(2)}, u32[]{:S(2)}) collective-permute-start(bf16[2,272,128]{2,1,0:T(8,128)(2,1)S(1)} %pad_maximum_fusion.3), channel_id=1, source_target_pairs={{0,32},{32,64},{64,96},{1,33},{33,65},{65,97},{2,34},{34,66},{66,9... | collective-permute-start | bytes 417800 | tf_op jit(solution)/shard_map/ppermute | solution.py:40
  189.6 7.4 %copy-start.1 = (bf16[512,4096]{1,0:T(8,128)(2,1)S(1)}, bf16[512,4096]{1,0:T(8,128)(2,1)}, u32[]{:S(2)}) copy-start(bf16[512,4096]{1,0:T(8,128)(2,1)} %filter_ref.5) | copy-start | bytes 12582916
  191.5 5.0 %copy-start.11 = (bf16[2,256]{1,0:T(2,128)(2,1)S(1)}, bf16[2,256]{1,0:T(2,128)(2,1)}, u32[]{:S(2)}) copy-start(bf16[2,256]{1,0:T(2,128)(2,1)} %gain_ref.1) | copy-start | bytes 3076
  191.5 4.8 %collective-permute-start.27 = (bf16[2,272,128]{2,1,0:T(8,128)(2,1)S(1)}, bf16[2,272,128]{2,1,0:T(8,128)(2,1)S(1)}, u32[]{:S(2)}, u32[]{:S(2)}) collective-permute-start(bf16[2,272,128]{2,1,0:T(8,128)(2,1)S(1)} %pad_maximum_fusion.3), channel_id=1, source_target_pairs={{0,96},{1,97},{2,98},{3,99},{4,100},{5,101},{6,102},{7,103},{8,104... | collective-permute-start | bytes 417800 | tf_op jit(solution)/shard_map/ppermute | solution.py:40
  201.6 14.0 %collective-permute-start.38 = (bf16[96,4096]{1,0:T(8,128)(2,1)S(1)}, bf16[96,4096]{1,0:T(8,128)(2,1)S(1)}, u32[]{:S(2)}, u32[]{:S(2)}) collective-permute-start(bf16[96,4096]{1,0:T(8,128)(2,1)S(1)} %get-tuple-element.48), channel_id=1, source_target_pairs={{0,1},{1,0},{2,3},{3,2},{4,5},{5,4},{6,7},{7,6},{8,9},{9,8},{10,11... | collective-permute-start | bytes 2359304 | tf_op jit(solution)/shard_map/ppermute | solution.py:35
  211.8 6.7 %collective-permute-start.37 = (bf16[192,4096]{1,0:T(8,128)(2,1)S(1)}, bf16[192,4096]{1,0:T(8,128)(2,1)S(1)}, u32[]{:S(2)}, u32[]{:S(2)}) collective-permute-start(bf16[192,4096]{1,0:T(8,128)(2,1)S(1)} %get-tuple-element.46), channel_id=1, source_target_pairs={{0,1},{1,0},{2,3},{3,2},{4,5},{5,4},{6,7},{7,6},{8,9},{9,8},{10,11... | collective-permute-start | bytes 4718600 | tf_op jit(solution)/shard_map/ppermute | solution.py:35
  215.0 18.4 %collective-permute-start.36 = (bf16[96,4096]{1,0:T(8,128)(2,1)S(1)}, bf16[96,4096]{1,0:T(8,128)(2,1)S(1)}, u32[]{:S(2)}, u32[]{:S(2)}) collective-permute-start(bf16[96,4096]{1,0:T(8,128)(2,1)S(1)} %get-tuple-element.44), channel_id=1, source_target_pairs={{0,1},{1,0},{2,3},{3,2},{4,5},{5,4},{6,7},{7,6},{8,9},{9,8},{10,11... | collective-permute-start | bytes 2359304 | tf_op jit(solution)/shard_map/ppermute | solution.py:35
  215.8 11.9 %collective-permute-start.39 = (bf16[48,4096]{1,0:T(8,128)(2,1)S(1)}, bf16[48,4096]{1,0:T(8,128)(2,1)S(1)}, u32[]{:S(2)}, u32[]{:S(2)}) collective-permute-start(bf16[48,4096]{1,0:T(8,128)(2,1)S(1)} %get-tuple-element.65), channel_id=1, source_target_pairs={{0,2},{2,4},{4,6},{6,0},{1,3},{3,5},{5,7},{7,1},{8,10},{10,12},{12... | collective-permute-start | bytes 1179656 | tf_op jit(solution)/shard_map/ppermute | solution.py:31
  215.9 11.9 %collective-permute-start.43 = (bf16[48,4096]{1,0:T(8,128)(2,1)S(1)}, bf16[48,4096]{1,0:T(8,128)(2,1)S(1)}, u32[]{:S(2)}, u32[]{:S(2)}) collective-permute-start(bf16[48,4096]{1,0:T(8,128)(2,1)S(1)} %get-tuple-element.64), channel_id=1, source_target_pairs={{0,6},{2,0},{4,2},{6,4},{1,7},{3,1},{5,3},{7,5},{8,14},{10,8},{12,... | collective-permute-start | bytes 1179656 | tf_op jit(solution)/shard_map/ppermute | solution.py:31
  227.9 11.1 %collective-permute-start.40 = (bf16[48,4096]{1,0:T(8,128)(2,1)S(1)}, bf16[48,4096]{1,0:T(8,128)(2,1)S(1)}, u32[]{:S(2)}, u32[]{:S(2)}) collective-permute-start(bf16[48,4096]{1,0:T(8,128)(2,1)S(1)} %get-tuple-element.61), channel_id=1, source_target_pairs={{0,2},{2,4},{4,6},{6,0},{1,3},{3,5},{5,7},{7,1},{8,10},{10,12},{12... | collective-permute-start | bytes 1179656 | tf_op jit(solution)/shard_map/ppermute | solution.py:31
  228.0 11.0 %collective-permute-start.44 = (bf16[48,4096]{1,0:T(8,128)(2,1)S(1)}, bf16[48,4096]{1,0:T(8,128)(2,1)S(1)}, u32[]{:S(2)}, u32[]{:S(2)}) collective-permute-start(bf16[48,4096]{1,0:T(8,128)(2,1)S(1)} %get-tuple-element.60), channel_id=1, source_target_pairs={{0,6},{2,0},{4,2},{6,4},{1,7},{3,1},{5,3},{7,5},{8,14},{10,8},{12,... | collective-permute-start | bytes 1179656 | tf_op jit(solution)/shard_map/ppermute | solution.py:31
  230.7 16.7 %collective-permute-start.41 = (bf16[48,4096]{1,0:T(8,128)(2,1)S(1)}, bf16[48,4096]{1,0:T(8,128)(2,1)S(1)}, u32[]{:S(2)}, u32[]{:S(2)}) collective-permute-start(bf16[48,4096]{1,0:T(8,128)(2,1)S(1)} %get-tuple-element.63), channel_id=1, source_target_pairs={{0,2},{2,4},{4,6},{6,0},{1,3},{3,5},{5,7},{7,1},{8,10},{10,12},{12... | collective-permute-start | bytes 1179656 | tf_op jit(solution)/shard_map/ppermute | solution.py:31
  230.8 16.6 %collective-permute-start.42 = (bf16[48,4096]{1,0:T(8,128)(2,1)S(1)}, bf16[48,4096]{1,0:T(8,128)(2,1)S(1)}, u32[]{:S(2)}, u32[]{:S(2)}) collective-permute-start(bf16[48,4096]{1,0:T(8,128)(2,1)S(1)} %get-tuple-element.62), channel_id=1, source_target_pairs={{0,6},{2,0},{4,2},{6,4},{1,7},{3,1},{5,3},{7,5},{8,14},{10,8},{12,... | collective-permute-start | bytes 1179656 | tf_op jit(solution)/shard_map/ppermute | solution.py:31
  (7 other events, 13.4 us)

commit v2 on v1

--- a/solution.py
+++ b/solution.py
@@ -52,7 +52,7 @@
     return pl.pallas_call(
         kernel,
         out_shape=out_shape,
-        compiler_params=pltpu.CompilerParams(vmem_limit_bytes=kwargs.pop("limit", 16) << 20),
+        compiler_params=pltpu.CompilerParams(vmem_limit_bytes=kwargs.pop("limit", 10) << 20),
         cost_estimate=pl.CostEstimate(
             flops=flops, bytes_accessed=8_000_000, transcendentals=0
         ),
@@ -123,7 +123,11 @@
     part = block - HALO
     pieces = around(shard, "x", part // 2)
     mine = vmem_kernel(
-        chips_kernel, jax.ShapeDtypeStruct((RING * block, width), BF16), 1_000_000_000, *pieces
+        chips_kernel,
+        jax.ShapeDtypeStruct((RING * block, width), BF16),
+        1_000_000_000,
+        *pieces,
+        limit=16,
     )
     return vmem_kernel(
         rows_kernel,
@@ -131,6 +135,7 @@
         2_000_000_000,
         mine,
         swap(mine),
+        limit=16,
     )
 
 
@@ -220,14 +225,12 @@
 def norm_kernel(rows_ref, gain_ref, out_ref):
     rows = rows_ref[...].astype(F32)
     meansq = jnp.mean(rows * rows, axis=-1, keepdims=True)
-    normed = rows * lax.rsqrt(meansq + EPSILON) * gain_ref[...].astype(F32)
+    normed = rows * lax.rsqrt(meansq + EPSILON) * gain_ref[...].astype(F32)[None]
     out_ref[...] = normed.astype(BF16)
 
 
 def norm_rows(rows, gain):
-    return vmem_kernel(
-        norm_kernel, jax.ShapeDtypeStruct(rows.shape, BF16), 1_000_000, rows, gain[None]
-    )
+    return vmem_kernel(norm_kernel, jax.ShapeDtypeStruct(rows.shape, BF16), 1_000_000, rows, gain)
 
 
 def decay_kernel(
@@ -299,50 +302,72 @@
     return lax.dot_general(a, b, (((1,), (1,)), ((), ())), preferred_element_type=F32)
 
 
-def local_kernel(qk_ref, v_ref, in_ref, out_ref, tail_ref, far_ref, end_ref, part_ref, qfar_ref, state_ref):
+def state_kernel(qk_ref, v_ref, tail_ref, end_ref, enter_ref, state_ref):
+    heads, value_dim, key_dim = state_ref.shape
+    for h in range(heads):
+        keys = slice(h * key_dim, (h + 1) * key_dim)
+        lanes = slice((heads + h) * key_dim, (heads + h + 1) * key_dim)
+        values = slice(h * value_dim, (h + 1) * value_dim)
+        state = jnp.zeros((value_dim, key_dim), F32)
+        for n in range(v_ref.shape[0] // BLOCK):
+            rows = slice(n * BLOCK, (n + 1) * BLOCK)
+            enter_ref[n, h] = state.astype(BF16)
+            kt = (qk_ref[rows, lanes].astype(F32) * tail_ref[rows, keys]).astype(BF16)
+            update = lax.dot_general(
+                v_ref[rows, values], kt, (((0,), (0,)), ((), ())), preferred_element_type=F32
+            )
+            state = state * end_ref[n : n + 1, keys] + update
+        state_ref[h] = state
+
+
+def near_kernel(qk_ref, v_ref, in_ref, out_ref, far_ref, enter_ref, part_ref, qfar_ref):
     length = qk_ref.shape[0]
-    heads = state_ref.shape[0]
-    key_dim = qk_ref.shape[1] // heads // 2
-    value_dim = v_ref.shape[1] // heads
+    heads, value_dim, key_dim = enter_ref.shape[1:]
     scale = key_dim ** (-0.5)
     low = lax.broadcasted_iota(jnp.int32, (BLOCK, BLOCK), 0)
     high = lax.broadcasted_iota(jnp.int32, (BLOCK, BLOCK), 1)
     causal = high <= low
-    states = [jnp.zeros((value_dim, key_dim), F32) for _ in range(heads)]
     for n in range(length // BLOCK):
         rows = slice(n * BLOCK, (n + 1) * BLOCK)
         for h in range(heads):
             keys = slice(h * key_dim, (h + 1) * key_dim)
+            lanes = slice((heads + h) * key_dim, (heads + h + 1) * key_dim)
             values = slice(h * value_dim, (h + 1) * value_dim)
             q = qk_ref[rows, keys].astype(F32) * scale
-            k = qk_ref[rows, heads * key_dim + h * key_dim : heads * key_dim + (h + 1) * key_dim].astype(F32)
-            v = v_ref[rows, values]
             qd = (q * in_ref[rows, keys]).astype(BF16)
-            ki = (k * out_ref[rows, keys]).astype(BF16)
-            kt = (k * tail_ref[rows, keys]).astype(BF16)
+            ki = (qk_ref[rows, lanes].astype(F32) * out_ref[rows, keys]).astype(BF16)
             qfar_ref[rows, keys] = (q * far_ref[rows, keys]).astype(BF16)
             scores = jnp.where(causal, across(qd, ki), 0.0).astype(BF16)
-            part = dot(scores, v)
-            if n > 0:
-                part = part + across(qd, states[h].astype(BF16))
-            part_ref[rows, values] = part
-            update = lax.dot_general(v, kt, (((0,), (0,)), ((), ())), preferred_element_type=F32)
-            states[h] = states[h] * end_ref[n : n + 1, keys] + update
-    for h in range(heads):
-        state_ref[h] = states[h]
-
-
-def local_attention(qk, v, terms, heads):
+            part_ref[rows, values] = dot(scores, v_ref[rows, values]) + across(qd, enter_ref[n, h])
+
+
+def local_states(qk, v, tail, end, heads):
     length, width = qk.shape[0], qk.shape[1] // 2
-    wide = v.shape[1]
-    return vmem_kernel(
-        local_kernel,
+    shape = (heads, v.shape[1] // heads, width // heads)
+    return vmem_kernel(
+        state_kernel,
         (
-            jax.ShapeDtypeStruct((length, wide), F32),
+            jax.ShapeDtypeStruct((length // BLOCK,) + shape, BF16),
+            jax.ShapeDtypeStruct(shape, F32),
+        ),
+        1_000_000_000,
+        qk,
+        v,
+        tail,
+        end,
+        in_specs=[pl.BlockSpec(memory_space=pltpu.VMEM)] * 4,
+    )
+
+
+def local_attention(qk, v, *terms):
+    length, width = qk.shape[0], qk.shape[1] // 2
+    return vmem_kernel(
+        near_kernel,
+        (
+            jax.ShapeDtypeStruct((length, v.shape[1]), F32),
             jax.ShapeDtypeStruct((length, width), BF16),
-            jax.ShapeDtypeStruct((heads, wide // heads, width // heads), F32),
         ),
-        6_000_000_000,
+        2_000_000_000,
         qk,
         v,
         *terms,
@@ -415,38 +440,77 @@
     line = pack(total)
     outer = empty
     for step in (1, 2, 3):
-        pair = unpack(onward(line, "z", step), value_dim)
+        pair = unpack(hop(line, "z", step), value_dim)
         outer = combine(only(z >= step, pair), outer)
     return combine(outer, before)[1].astype(BF16)
 
 
-def term_kernel(steps, attn_ref, t_ref, b_ref, mixer_ref, filter_ref, own_ref, other_ref):
+TILE = 1024
+
+
+def targets(steps, part):
     x, c = lax.axis_index("x"), lax.axis_index("c")
-    count = own_ref.shape[0]
-    part = count // len(steps)
-    spots = [
+    return [
         pl.multiple_of((lax.rem(x + step, RING) * PAIR + core) * part, HALO)
         for core in (1 - c, c)
         for step in steps
     ]
-    half = t_ref.shape[1]
-    out = None
-    for ref, matrix in (
-        (attn_ref, mixer_ref[...]),
-        (t_ref, filter_ref[:half]),
-        (b_ref, filter_ref[half:]),
-    ):
-        rows = jnp.concatenate([ref[pl.ds(at, part), :] for at in spots], axis=0)
-        term = dot(rows, matrix)
-        out = term if out is None else out + term
-    other_ref[...] = out[:count].astype(BF16)
-    own_ref[...] = out[count:]
-
-
-def term_call(steps, attn, t, b, mixer, filt, part):
+
+
+def stacked(refs, spots, part):
+    lines = [[ref[pl.ds(at, part), :] for ref in refs] for at in spots]
+    lines = [jnp.concatenate(line, axis=1) if len(line) > 1 else line[0] for line in lines]
+    return jnp.concatenate(lines, axis=0)
+
+
+def conv_kernel(groups, t_ref, b_ref, filter_ref, *outs):
+    spots, part = [], outs[0].shape[0] // (PAIR * len(groups[0]))
+    for steps in groups:
+        spots += targets(steps, part)
+    rows = stacked((t_ref, b_ref), spots, part)
+
+    @pl.loop(0, filter_ref.shape[1] // TILE)
+    def _(j):
+        cols = pl.ds(pl.multiple_of(j * TILE, TILE), TILE)
+        out = dot(rows, filter_ref[:, cols])
+        at = 0
+        for ref in outs:
+            ref[:, cols] = out[at : at + ref.shape[0]]
+            at += ref.shape[0]
+
+
+def conv_call(groups, t, b, filt, part):
+    return vmem_kernel(
+        functools.partial(conv_kernel, groups),
+        tuple(
+            jax.ShapeDtypeStruct((PAIR * len(steps) * part, filt.shape[1]), F32)
+            for steps in groups
+        ),
+        2_000_000_000,
+        t,
+        b,
+        filt,
+        in_specs=[pl.BlockSpec(memory_space=pltpu.VMEM)] * 3,
+        out_specs=tuple(pl.BlockSpec(memory_space=pltpu.VMEM) for _ in groups),
+    )
+
+
+def term_kernel(steps, attn_ref, mixer_ref, acc_ref, own_ref, other_ref):
+    count = own_ref.shape[0]
+    part = count // len(steps)
+    attn = stacked((attn_ref,), targets(steps, part), part)
+
+    @pl.loop(0, own_ref.shape[1] // TILE)
+    def _(j):
+        cols = pl.ds(pl.multiple_of(j * TILE, TILE), TILE)
+        out = acc_ref[:, cols] + dot(attn, mixer_ref[:, cols])
+        other_ref[:, cols] = out[:count].astype(BF16)
+        own_ref[:, cols] = out[count:]
+
+
+def term_call(steps, attn, mixer, acc, part):
     width = mixer.shape[1]
     part = part * len(steps)
-    tile = 1024
     whole = pl.BlockSpec(memory_space=pltpu.VMEM)
     return vmem_kernel(
         functools.partial(term_kernel, steps),
@@ -456,17 +520,10 @@
         ),
         2_000_000_000,
         attn,
-        t,
-        b,
         mixer,
-        filt,
-        grid=(width // tile,),
-        in_specs=[whole, whole, whole]
-        + [pl.BlockSpec((m.shape[0], tile), lambda i: (0, i)) for m in (mixer, filt)],
-        out_specs=(
-            pl.BlockSpec((part, tile), lambda i: (0, i)),
-            pl.BlockSpec((part, tile), lambda i: (0, i)),
-        ),
+        acc,
+        in_specs=[whole] * 3,
+        out_specs=(whole, whole),
     )
 
 
@@ -521,14 +578,15 @@
     w_t = around(line_t, "y")
     w_b = around(line_b, "z")
 
-    *terms, total = decay_terms(x, forget_left, forget_right, forget_offset, forget_spike)
+    in_decay, out_decay, tail, far_decay, end, total = decay_terms(x, forget_left, forget_right, forget_offset, forget_spike)
     total = total.reshape(heads, 1, key_dim)
     early, late = (0, 1, 2), (3, 4)
     acc_qk = project_call(x, None, w_qk[:3], early, 1, HALO, F32)
     acc_v = project_call(x, None, w_v[:3], early, 0, HALO, F32)
     qk = project_call(x, acc_qk, w_qk[3:], late, 1, HALO, BF16)
     v = project_call(x, acc_v, w_v[3:], late, 0, HALO, BF16)
-    near, qfar, state = local_attention(qk, v, terms, heads)
+    enter, state = local_states(qk, v, tail, end, heads)
+    near, qfar = local_attention(qk, v, in_decay, out_decay, far_decay, enter)
     incoming = entering(total, state)
     mixed_attn = finish_attention(near, qfar, incoming, head_gain)
 
@@ -537,10 +595,14 @@
     mixed_t = gate_call(x, acc_t, w_t[3:], late, taps[:, :half], 1)
     mixed_b = gate_call(x, acc_b, w_b[3:], late, taps[:, half:], 0)
 
+    groups = ((2,), (1, 3))
+    shares = dict(zip(groups, conv_call(groups, mixed_t, mixed_b, filter_result, part)))
+
     def partial(*steps):
-        own, other = term_call(
-            steps, mixed_attn, mixed_t, mixed_b, mixer_result, filter_result, part
-        )
+        share = shares.get(steps)
+        if share is None:
+            share = conv_call((steps,), mixed_t, mixed_b, filter_result, part)[0]
+        own, other = term_call(steps, mixed_attn, mixer_result, share, part)
         return plus(own, swap(other))
 
     cut = part // 2

time: 250 us -> 240 us (0.960)
  the two profiles are of different devices: /device:TPU:1 before, /device:TPU:54 now
where the time goes in v2:
time: 240 us
  waiting for transfers between devices  112 us (47%)
  starting transfers between devices  61.1 us (25%)
  Pallas kernels  52.5 us (22%)
  local copies, waits for them, and re-layouts  10.5 us (4%)
  other arithmetic  2.76 us (1%)
    ppermute x40, waiting for transfers between devices, hop(): lax.ppermute(value, axis, [(i, (i + steps) % RING) for i in range(RING)])  108 us
    ppermute x40, starting transfers between devices, hop(): lax.ppermute(value, axis, [(i, (i + steps) % RING) for i in range(RING)])  57 us
    pallas_call x22, Pallas kernels, vmem_kernel(): pl.pallas_call(kernel, out_shape=out_shape, compiler_params=pltpu.Compile...  52.5 us
    unnamed x61, local copies, waits for them, and re-layouts  5.34 us
  transfers between devices with their start and end apart: 45, of which 21 were waited for; matrix products, arithmetic and copies ran while one was open for 3% of the time, Pallas kernels for 21%

profile of v2, /device:TPU:54, one launch (start us, length us, event | category | flops | bytes accessed | tf_op | source)
XLA Modules:
  0.0 239.6 jit_solution(12310450242743470731)
XLA Ops:
  2.3 3.3 %collective-permute-start = (bf16[16,4096]{1,0:T(8,128)(2,1)S(1)}, bf16[16,4096]{1,0:T(8,128)(2,1)S(1)}, u32[]{:S(2)}, u32[]{:S(2)}) collective-permute-start(bf16[16,4096]{1,0:T(8,128)(2,1)S(1)} %slice.172), channel_id=1, source_target_pairs={{0,8},{8,16},{16,24},{24,32},{32,40},{40,48},{48,56},{56,64},{64,7... | collective-permute-start | bytes 393224 | tf_op jit(solution)/shard_map/ppermute | solution.py:40
  5.7 3.9 %collective-permute-done = bf16[16,4096]{1,0:T(8,128)(2,1)S(1)} collective-permute-done((bf16[16,4096]{1,0:T(8,128)(2,1)S(1)}, bf16[16,4096]{1,0:T(8,128)(2,1)S(1)}, u32[]{:S(2)}, u32[]{:S(2)}) %collective-permute-start) | collective-permute-done | bytes 131104 | tf_op jit(solution)/shard_map/ppermute | solution.py:40
  10.6 2.4 %collective-permute-start.1 = (bf16[112,4096]{1,0:T(8,128)(2,1)S(1)}, bf16[112,4096]{1,0:T(8,128)(2,1)S(1)}, u32[]{:S(2)}, u32[]{:S(2)}) collective-permute-start(bf16[112,4096]{1,0:T(8,128)(2,1)S(1)} %pad_maximum_fusion.own), channel_id=1, source_target_pairs={{0,2},{2,4},{4,6},{6,0},{1,3},{3,5},{5,7},{7,1},{8,10},{10,12},{12... | collective-permute-start | bytes 2752520 | tf_op jit(solution)/shard_map/ppermute | solution.py:31
  13.1 19.1 %collective-permute-done.2.above = bf16[112,4096]{1,0:T(8,128)(2,1)S(1)} collective-permute-done((bf16[112,4096]{1,0:T(8,128)(2,1)S(1)}, bf16[112,4096]{1,0:T(8,128)(2,1)S(1)}, u32[]{:S(2)}, u32[]{:S(2)}) %collective-permute-start.2) | collective-permute-done | bytes 917536 | tf_op jit(solution)/shard_map/ppermute | solution.py:31
  32.4 3.3 %collective-permute-start.3 = (bf16[48,4096]{1,0:T(8,128)(2,1)S(1)}, bf16[48,4096]{1,0:T(8,128)(2,1)S(1)}, u32[]{:S(2)}, u32[]{:S(2)}) collective-permute-start(bf16[48,4096]{1,0:T(8,128)(2,1)S(1)} %slice.173), channel_id=1, source_target_pairs={{0,2},{2,4},{4,6},{6,0},{1,3},{3,5},{5,7},{7,1},{8,10},{10,12},{12... | collective-permute-start | bytes 1179656 | tf_op jit(solution)/shard_map/ppermute | solution.py:31
  35.7 2.0 collective-permute-start.6
  37.9 1.4 collective-permute-start.14
  39.2 2.9 %collective-permute-done.3.top = bf16[48,4096]{1,0:T(8,128)(2,1)S(1)} collective-permute-done((bf16[48,4096]{1,0:T(8,128)(2,1)S(1)}, bf16[48,4096]{1,0:T(8,128)(2,1)S(1)}, u32[]{:S(2)}, u32[]{:S(2)}) %collective-permute-start.3) | collective-permute-done | bytes 393248 | tf_op jit(solution)/shard_map/ppermute | solution.py:31
  42.5 3.0 %collective-permute-done.4.bottom = bf16[64,4096]{1,0:T(8,128)(2,1)S(1)} collective-permute-done((bf16[64,4096]{1,0:T(8,128)(2,1)S(1)}, bf16[64,4096]{1,0:T(8,128)(2,1)S(1)}, u32[]{:S(2)}, u32[]{:S(2)}) %collective-permute-start.4) | collective-permute-done | bytes 524320 | tf_op jit(solution)/shard_map/ppermute | solution.py:31
  45.5 2.1 shard_map.155.mine
  47.6 2.4 collective-permute-done.6.below
  50.0 2.0 collective-permute-start.8
  52.6 1.4 collective-permute-start.16
  54.0 2.1 collective-permute-done.15.above
  56.1 1.3 collective-permute-start.17
  57.8 1.7 collective-permute-done.9.bottom
  59.5 1.3 shard_map.157
  60.9 1.3 collective-permute-start.10
  62.9 1.7 collective-permute-done.17.bottom
  64.6 1.4 shard_map.160
  66.0 2.2 collective-permute-start.18
  69.6 14.4 %collective-permute-done.10.refs_1_ = bf16[1024,512]{1,0:T(8,128)(2,1)S(1)} collective-permute-done((bf16[1024,512]{1,0:T(8,128)(2,1)S(1)}, bf16[1024,512]{1,0:T(8,128)(2,1)S(1)}, u32[]{:S(2)}, u32[]{:S(2)}) %collective-permute-start.10) | collective-permute-done | bytes 1048608 | tf_op jit(solution)/shard_map/ppermute | solution.py:31
  84.0 1.3 collective-permute-start.28
  85.8 1.8 collective-permute-start.29
  87.6 1.7 collective-permute-start.32
  90.3 1.2 slice.177
  92.7 26.1 %collective-permute-done.28.refs_1_ = bf16[1024,768]{1,0:T(8,128)(2,1)} collective-permute-done((bf16[1024,768]{1,0:T(8,128)(2,1)}, bf16[1024,768]{1,0:T(8,128)(2,1)}, u32[]{:S(2)}, u32[]{:S(2)}) %collective-permute-start.28) | collective-permute-done | bytes 1572896 | tf_op jit(solution)/shard_map/ppermute | solution.py:31
  118.8 1.3 collective-permute-start.12
  123.3 1.7 collective-permute-start.20
  125.6 3.0 %collective-permute-start.30 = (bf16[512,768]{1,0:T(8,128)(2,1)S(1)}, bf16[512,768]{1,0:T(8,128)(2,1)S(1)}, u32[]{:S(2)}, u32[]{:S(2)}) collective-permute-start(bf16[512,768]{1,0:T(8,128)(2,1)S(1)} %slice.194), channel_id=1, source_target_pairs={{0,8},{8,16},{16,24},{24,0},{1,9},{9,17},{17,25},{25,1},{2,10},{10... | collective-permute-start | bytes 2359304 | tf_op jit(solution)/shard_map/ppermute | solution.py:31
  128.6 3.6 %shard_map.156.x_ref = bf16[784,4096]{1,0:T(8,128)(2,1)S(1)} custom-call(bf16[448,4096]{1,0:T(8,128)(2,1)} %shard_map.155.mine, bf16[448,4096]{1,0:T(8,128)(2,1)} %collective-permute-done.5.other), custom_call_target="tpu_custom_call" | custom-call | flops 2000000000 | bytes 8000000 | tf_op jit(solution)/shard_map/pallas_call | solution.py:52
  132.2 6.4 %shard_map.163 = (f32[768,256]{1,0:T(8,128)S(1)}, f32[768,256]{1,0:T(8,128)S(1)}, f32[768,256]{1,0:T(8,128)S(1)}, f32[768,256]{1,0:T(8,128)S(1)}, f32[12,256]{1,0:T(8,128)S(1)}, /*index=5*/f32[1,256]{1,0:T(1,128)S(1)}) custom-call(bf16[784,4096]{1,0:T(8,128)(2,1)S(1)} %shard_map.156.x_ref, bf16[64,4096]{1,0:T(8,128)(2,1)S(1)} %bitcast.23, ...), custom_call_target="tpu_custom_call" | custom-call | flops 4000000000 | bytes 8000000 | tf_op jit(solution)/shard_map/pallas_call | solution.py:52
  138.7 3.1 %shard_map.158.acc_ref = f32[768,512]{1,0:T(8,128)S(1)} custom-call(bf16[784,4096]{1,0:T(8,128)(2,1)S(1)} %shard_map.156.x_ref, bf16[1024,512]{1,0:T(8,128)(2,1)S(1)} %copy-done.11, bf16[1024,512]{1,0:T(8,128)(2,1)S(1)} %copy-done.3, bf16[1024,512]{1,0:T(8,128)(2,1)S(1)} %copy-done.5), custom_call_target="tpu_custom_call" | custom-call | flops 3000000000 | bytes 8000000 | tf_op jit(solution)/shard_map/pallas_call | solution.py:52
  141.9 3.1 %shard_map.161.acc_ref = f32[768,512]{1,0:T(8,128)S(1)} custom-call(bf16[784,4096]{1,0:T(8,128)(2,1)S(1)} %shard_map.156.x_ref, bf16[1024,512]{1,0:T(8,128)(2,1)S(1)} %copy-done.13, bf16[1024,512]{1,0:T(8,128)(2,1)S(1)} %copy-done.7, bf16[1024,512]{1,0:T(8,128)(2,1)S(1)} %copy-done.9), custom_call_target="tpu_custom_call" | custom-call | flops 3000000000 | bytes 8000000 | tf_op jit(solution)/shard_map/pallas_call | solution.py:52
  145.1 1.8 collective-permute-start.34
  146.8 1.4 shard_map.159.qk_ref
  148.3 1.6 collective-permute-start.35
  149.9 1.4 shard_map.162.v_ref
  152.1 2.6 %collective-permute-start.22 = (bf16[2,272,128]{2,1,0:T(8,128)(2,1)S(1)}, bf16[2,272,128]{2,1,0:T(8,128)(2,1)S(1)}, u32[]{:S(2)}, u32[]{:S(2)}) collective-permute-start(bf16[2,272,128]{2,1,0:T(8,128)(2,1)S(1)} %pad_maximum_fusion.2), channel_id=1, source_target_pairs={{0,24},{8,0},{16,8},{24,16},{1,25},{9,1},{17,9},{25,17},{2,26},{10... | collective-permute-start | bytes 417800 | tf_op jit(solution)/shard_map/ppermute | solution.py:31
  154.6 5.8 %shard_map.167.acc_ref = f32[784,768]{1,0:T(8,128)S(1)} custom-call(bf16[784,4096]{1,0:T(8,128)(2,1)S(1)} %shard_map.156.x_ref, bf16[1024,768]{1,0:T(8,128)(2,1)} %get-tuple-element.45.refs_0_, bf16[1024,768]{1,0:T(8,128)(2,1)} %collective-permute-done.28.refs_1_, bf16[1024,768]{1,0:T(8,128)(2,1)} %collective-permute-done.29.refs_2_), custom_call_target="tpu_custom_call" | custom-call | flops 3000000000 | bytes 8000000 | tf_op jit(solution)/shard_map/pallas_call | solution.py:52
  160.5 2.8 %collective-permute-start.23 = (bf16[2,272,128]{2,1,0:T(8,128)(2,1)S(1)}, bf16[2,272,128]{2,1,0:T(8,128)(2,1)S(1)}, u32[]{:S(2)}, u32[]{:S(2)}) collective-permute-start(bf16[2,272,128]{2,1,0:T(8,128)(2,1)S(1)} %pad_maximum_fusion.2), channel_id=1, source_target_pairs={{0,16},{8,24},{16,0},{24,8},{1,17},{9,25},{17,1},{25,9},{2,18},{10... | collective-permute-start | bytes 417800 | tf_op jit(solution)/shard_map/ppermute | solution.py:31
  163.3 1.4 collective-permute-done.31.refs_1_
  164.7 3.0 %collective-permute-start.24 = (bf16[2,272,128]{2,1,0:T(8,128)(2,1)S(1)}, bf16[2,272,128]{2,1,0:T(8,128)(2,1)S(1)}, u32[]{:S(2)}, u32[]{:S(2)}) collective-permute-start(bf16[2,272,128]{2,1,0:T(8,128)(2,1)S(1)} %pad_maximum_fusion.2), channel_id=1, source_target_pairs={{0,8},{8,16},{16,24},{24,0},{1,9},{9,17},{17,25},{25,1},{2,10},{10... | collective-permute-start | bytes 417800 | tf_op jit(solution)/shard_map/ppermute | solution.py:31
  167.6 1.8 shard_map.168.t_ref
  169.5 5.5 %shard_map.169.acc_ref = f32[784,768]{1,0:T(8,128)S(1)} custom-call(bf16[784,4096]{1,0:T(8,128)(2,1)S(1)} %shard_map.156.x_ref, bf16[1024,768]{1,0:T(8,128)(2,1)} %get-tuple-element.46.refs_0_, bf16[1024,768]{1,0:T(8,128)(2,1)S(1)} %collective-permute-done.32.refs_1_, bf16[1024,768]{1,0:T(8,128)(2,1)S(1)} %collective-permute-done.33.refs_2_), custom_call_target="tpu_custom_call" | custom-call | flops 3000000000 | bytes 8000000 | tf_op jit(solution)/shard_map/pallas_call | solution.py:52
  175.0 1.8 shard_map.170.b_ref
  177.2 3.2 %shard_map.173 = (f32[192,4096]{1,0:T(8,128)S(1)}, f32[384,4096]{1,0:T(8,128)S(1)}) custom-call(bf16[768,256]{1,0:T(8,128)(2,1)S(1)} %shard_map.168.t_ref, bf16[768,256]{1,0:T(8,128)(2,1)S(1)} %shard_map.170.b_ref, bf16[512,4096]{1,0:T(8,128)(2,1)S(1)} %copy-done.1), custom_call_target="tpu_custom_call" | custom-call | flops 2000000000 | bytes 8000000 | tf_op jit(solution)/shard_map/pallas_call | solution.py:52
  180.7 1.8 collective-permute-start.26
  182.5 3.0 %collective-permute-start.25 = (bf16[2,272,128]{2,1,0:T(8,128)(2,1)S(1)}, bf16[2,272,128]{2,1,0:T(8,128)(2,1)S(1)}, u32[]{:S(2)}, u32[]{:S(2)}) collective-permute-start(bf16[2,272,128]{2,1,0:T(8,128)(2,1)S(1)} %pad_maximum_fusion.3), channel_id=1, source_target_pairs={{0,64},{32,96},{64,0},{96,32},{1,65},{33,97},{65,1},{97,33},{2,66}... | collective-permute-start | bytes 417800 | tf_op jit(solution)/shard_map/ppermute | solution.py:31
  185.5 1.8 shard_map.165
  187.5 1.5 collective-permute-done.25
  189.1 3.4 %collective-permute-done.27 = bf16[2,272,128]{2,1,0:T(8,128)(2,1)S(1)} collective-permute-done((bf16[2,272,128]{2,1,0:T(8,128)(2,1)S(1)}, bf16[2,272,128]{2,1,0:T(8,128)(2,1)S(1)}, u32[]{:S(2)}, u32[]{:S(2)}) %collective-permute-start.27) | collective-permute-done | bytes 139296 | tf_op jit(solution)/shard_map/ppermute | solution.py:31
  193.3 1.4 copy-done
  194.7 1.5 shard_map.175
  196.3 1.6 shard_map.171.acc_ref
  197.9 1.6 shard_map.172
  200.0 2.3 shard_map.174
  202.8 3.2 %collective-permute-start.39 = (bf16[48,4096]{1,0:T(8,128)(2,1)S(1)}, bf16[48,4096]{1,0:T(8,128)(2,1)S(1)}, u32[]{:S(2)}, u32[]{:S(2)}) collective-permute-start(bf16[48,4096]{1,0:T(8,128)(2,1)S(1)} %get-tuple-element.71), channel_id=1, source_target_pairs={{0,2},{2,4},{4,6},{6,0},{1,3},{3,5},{5,7},{7,1},{8,10},{10,12},{12... | collective-permute-start | bytes 1179656 | tf_op jit(solution)/shard_map/ppermute | solution.py:31
  207.1 8.4 %collective-permute-done.43 = bf16[48,4096]{1,0:T(8,128)(2,1)S(1)} collective-permute-done((bf16[48,4096]{1,0:T(8,128)(2,1)S(1)}, bf16[48,4096]{1,0:T(8,128)(2,1)S(1)}, u32[]{:S(2)}, u32[]{:S(2)}) %collective-permute-start.43) | collective-permute-done | bytes 393248 | tf_op jit(solution)/shard_map/ppermute | solution.py:31
  215.7 3.8 %collective-permute-start.40 = (bf16[48,4096]{1,0:T(8,128)(2,1)S(1)}, bf16[48,4096]{1,0:T(8,128)(2,1)S(1)}, u32[]{:S(2)}, u32[]{:S(2)}) collective-permute-start(bf16[48,4096]{1,0:T(8,128)(2,1)S(1)} %get-tuple-element.67), channel_id=1, source_target_pairs={{0,2},{2,4},{4,6},{6,0},{1,3},{3,5},{5,7},{7,1},{8,10},{10,12},{12... | collective-permute-start | bytes 1179656 | tf_op jit(solution)/shard_map/ppermute | solution.py:31
  219.4 4.5 %collective-permute-done.41 = bf16[48,4096]{1,0:T(8,128)(2,1)S(1)} collective-permute-done((bf16[48,4096]{1,0:T(8,128)(2,1)S(1)}, bf16[48,4096]{1,0:T(8,128)(2,1)S(1)}, u32[]{:S(2)}, u32[]{:S(2)}) %collective-permute-start.41) | collective-permute-done | bytes 393248 | tf_op jit(solution)/shard_map/ppermute | solution.py:31
  223.9 7.7 %collective-permute-done.40 = bf16[48,4096]{1,0:T(8,128)(2,1)S(1)} collective-permute-done((bf16[48,4096]{1,0:T(8,128)(2,1)S(1)}, bf16[48,4096]{1,0:T(8,128)(2,1)S(1)}, u32[]{:S(2)}, u32[]{:S(2)}) %collective-permute-start.40) | collective-permute-done | bytes 393248 | tf_op jit(solution)/shard_map/ppermute | solution.py:31
  232.6 5.8 %collective-permute-done.42 = bf16[48,4096]{1,0:T(8,128)(2,1)S(1)} collective-permute-done((bf16[48,4096]{1,0:T(8,128)(2,1)S(1)}, bf16[48,4096]{1,0:T(8,128)(2,1)S(1)}, u32[]{:S(2)}, u32[]{:S(2)}) %collective-permute-start.42) | collective-permute-done | bytes 393248 | tf_op jit(solution)/shard_map/ppermute | solution.py:31
  238.4 1.3 add_convert_fusion
  (155 shorter events, 19.3 us)
Async XLA Ops:
  1.8 11.2 %copy-start.25 = (bf16[256,256]{1,0:T(8,128)(2,1)S(1)}, bf16[256,256]{1,0:T(8,128)(2,1)}, u32[]{:S(2)}) copy-start(bf16[256,256]{1,0:T(8,128)(2,1)} %param.18) | copy-start | bytes 393220
  2.3 10.7 %copy-start.26 = (bf16[256,256]{1,0:T(8,128)(2,1)S(1)}, bf16[256,256]{1,0:T(8,128)(2,1)}, u32[]{:S(2)}) copy-start(bf16[256,256]{1,0:T(8,128)(2,1)} %param.19) | copy-start | bytes 393220
  2.3 10.7 %copy-start.23 = (bf16[256,512]{1,0:T(8,128)(2,1)S(1)}, bf16[256,512]{1,0:T(8,128)(2,1)}, u32[]{:S(2)}) copy-start(bf16[256,512]{1,0:T(8,128)(2,1)} %param.21) | copy-start | bytes 786436
  2.3 30.0 %copy-start.22 = (bf16[256,512]{1,0:T(8,128)(2,1)S(1)}, bf16[256,512]{1,0:T(8,128)(2,1)}, u32[]{:S(2)}) copy-start(bf16[256,512]{1,0:T(8,128)(2,1)} %param.22) | copy-start | bytes 786436
  2.3 7.3 %collective-permute-start = (bf16[16,4096]{1,0:T(8,128)(2,1)S(1)}, bf16[16,4096]{1,0:T(8,128)(2,1)S(1)}, u32[]{:S(2)}, u32[]{:S(2)}) collective-permute-start(bf16[16,4096]{1,0:T(8,128)(2,1)S(1)} %slice.172), channel_id=1, source_target_pairs={{0,8},{8,16},{16,24},{24,32},{32,40},{40,48},{48,56},{56,64},{64,7... | collective-permute-start | bytes 393224 | tf_op jit(solution)/shard_map/ppermute | solution.py:40
  9.7 26.0 %copy-start.21 = (bf16[256,512]{1,0:T(8,128)(2,1)S(1)}, bf16[256,512]{1,0:T(8,128)(2,1)}, u32[]{:S(2)}) copy-start(bf16[256,512]{1,0:T(8,128)(2,1)} %param.23) | copy-start | bytes 786436
  9.7 22.5 %collective-permute-start.2 = (bf16[112,4096]{1,0:T(8,128)(2,1)S(1)}, bf16[112,4096]{1,0:T(8,128)(2,1)S(1)}, u32[]{:S(2)}, u32[]{:S(2)}) collective-permute-start(bf16[112,4096]{1,0:T(8,128)(2,1)S(1)} %pad_maximum_fusion.own), channel_id=1, source_target_pairs={{0,6},{2,0},{4,2},{6,4},{1,7},{3,1},{5,3},{7,5},{8,14},{10,8},{12,... | collective-permute-start | bytes 2752520 | tf_op jit(solution)/shard_map/ppermute | solution.py:31
  10.6 21.8 %collective-permute-start.1 = (bf16[112,4096]{1,0:T(8,128)(2,1)S(1)}, bf16[112,4096]{1,0:T(8,128)(2,1)S(1)}, u32[]{:S(2)}, u32[]{:S(2)}) collective-permute-start(bf16[112,4096]{1,0:T(8,128)(2,1)S(1)} %pad_maximum_fusion.own), channel_id=1, source_target_pairs={{0,2},{2,4},{4,6},{6,0},{1,3},{3,5},{5,7},{7,1},{8,10},{10,12},{12... | collective-permute-start | bytes 2752520 | tf_op jit(solution)/shard_map/ppermute | solution.py:31
  13.1 24.7 %slice-start = ((bf16[256,512]{1,0:T(8,128)(2,1)}), bf16[256,256]{1,0:T(8,128)(2,1)S(1)}, s32[]{:S(2)}) async-start(bf16[256,512]{1,0:T(8,128)(2,1)} %param.23), calls=%async_computation | async-start | bytes 262144 | tf_op jit(solution)/shard_map/slice | solution.py:562
  13.1 24.7 %slice-start.1 = ((bf16[256,512]{1,0:T(8,128)(2,1)}), bf16[256,256]{1,0:T(8,128)(2,1)S(1)}, s32[]{:S(2)}) async-start(bf16[256,512]{1,0:T(8,128)(2,1)} %param.22), calls=%async_computation.1 | async-start | bytes 262144 | tf_op jit(solution)/shard_map/slice | solution.py:562
  13.1 24.7 %slice-start.2 = ((bf16[256,512]{1,0:T(8,128)(2,1)}), bf16[256,256]{1,0:T(8,128)(2,1)S(1)}, s32[]{:S(2)}) async-start(bf16[256,512]{1,0:T(8,128)(2,1)} %param.21), calls=%async_computation.2 | async-start | bytes 262144 | tf_op jit(solution)/shard_map/slice | solution.py:562
  13.1 24.7 %copy-start.24 = (bf16[256,512]{1,0:T(8,128)(2,1)S(1)}, bf16[256,512]{1,0:T(8,128)(2,1)}, u32[]{:S(2)}) copy-start(bf16[256,512]{1,0:T(8,128)(2,1)} %param.20) | copy-start | bytes 786436
  32.2 13.2 %collective-permute-start.4 = (bf16[64,4096]{1,0:T(8,128)(2,1)S(1)}, bf16[64,4096]{1,0:T(8,128)(2,1)S(1)}, u32[]{:S(2)}, u32[]{:S(2)}) collective-permute-start(bf16[64,4096]{1,0:T(8,128)(2,1)S(1)} %slice.174), channel_id=1, source_target_pairs={{0,6},{2,0},{4,2},{6,4},{1,7},{3,1},{5,3},{7,5},{8,14},{10,8},{12,... | collective-permute-start | bytes 1572872 | tf_op jit(solution)/shard_map/ppermute | solution.py:31
  32.4 9.7 %collective-permute-start.3 = (bf16[48,4096]{1,0:T(8,128)(2,1)S(1)}, bf16[48,4096]{1,0:T(8,128)(2,1)S(1)}, u32[]{:S(2)}, u32[]{:S(2)}) collective-permute-start(bf16[48,4096]{1,0:T(8,128)(2,1)S(1)} %slice.173), channel_id=1, source_target_pairs={{0,2},{2,4},{4,6},{6,0},{1,3},{3,5},{5,7},{7,1},{8,10},{10,12},{12... | collective-permute-start | bytes 1179656 | tf_op jit(solution)/shard_map/ppermute | solution.py:31
  35.7 14.3 %collective-permute-start.6 = (bf16[256,1280]{1,0:T(8,128)(2,1)S(1)}, bf16[256,1280]{1,0:T(8,128)(2,1)S(1)}, u32[]{:S(2)}, u32[]{:S(2)}) collective-permute-start(bf16[256,1280]{1,0:T(8,128)(2,1)S(1)} %slice_dynamic-update-slice_fusion.own), channel_id=1, source_target_pairs={{0,32},{32,64},{64,96},{96,0},{1,33},{33,65},{65,97},{97,1},{2,34}... | collective-permute-start | bytes 1966088 | tf_op jit(solution)/shard_map/ppermute | solution.py:31
  37.7 14.3 %collective-permute-start.7 = (bf16[256,1280]{1,0:T(8,128)(2,1)S(1)}, bf16[256,1280]{1,0:T(8,128)(2,1)S(1)}, u32[]{:S(2)}, u32[]{:S(2)}) collective-permute-start(bf16[256,1280]{1,0:T(8,128)(2,1)S(1)} %slice_dynamic-update-slice_fusion.own), channel_id=1, source_target_pairs={{0,96},{32,0},{64,32},{96,64},{1,97},{33,1},{65,33},{97,65},{2,98}... | collective-permute-start | bytes 1966088 | tf_op jit(solution)/shard_map/ppermute | solution.py:31
  37.9 14.7 %collective-permute-start.14 = (bf16[256,1280]{1,0:T(8,128)(2,1)S(1)}, bf16[256,1280]{1,0:T(8,128)(2,1)S(1)}, u32[]{:S(2)}, u32[]{:S(2)}) collective-permute-start(bf16[256,1280]{1,0:T(8,128)(2,1)S(1)} %pad_maximum_fusion.1.own), channel_id=1, source_target_pairs={{0,8},{8,16},{16,24},{24,0},{1,9},{9,17},{17,25},{25,1},{2,10},{10... | collective-permute-start | bytes 1966088 | tf_op jit(solution)/shard_map/ppermute | solution.py:31
  42.1 14.0 %collective-permute-start.15 = (bf16[256,1280]{1,0:T(8,128)(2,1)S(1)}, bf16[256,1280]{1,0:T(8,128)(2,1)S(1)}, u32[]{:S(2)}, u32[]{:S(2)}) collective-permute-start(bf16[256,1280]{1,0:T(8,128)(2,1)S(1)} %pad_maximum_fusion.1.own), channel_id=1, source_target_pairs={{0,24},{8,0},{16,8},{24,16},{1,25},{9,1},{17,9},{25,17},{2,26},{10... | collective-permute-start | bytes 1966088 | tf_op jit(solution)/shard_map/ppermute | solution.py:31
  47.6 78.0 %collective-permute-start.5 = (bf16[448,4096]{1,0:T(8,128)(2,1)}, bf16[448,4096]{1,0:T(8,128)(2,1)}, u32[]{:S(2)}, u32[]{:S(2)}) collective-permute-start(bf16[448,4096]{1,0:T(8,128)(2,1)} %shard_map.155.mine), channel_id=1, source_target_pairs={{0,1},{1,0},{2,3},{3,2},{4,5},{5,4},{6,7},{7,6},{8,9},{9,8},{10,11... | collective-permute-start | bytes 11010056 | tf_op jit(solution)/shard_map/ppermute | solution.py:35
  50.0 7.8 %collective-permute-start.8 = (bf16[128,1280]{1,0:T(8,128)(2,1)S(1)}, bf16[128,1280]{1,0:T(8,128)(2,1)S(1)}, u32[]{:S(2)}, u32[]{:S(2)}) collective-permute-start(bf16[128,1280]{1,0:T(8,128)(2,1)S(1)} %slice.175), channel_id=1, source_target_pairs={{0,32},{32,64},{64,96},{96,0},{1,33},{33,65},{65,97},{97,1},{2,34}... | collective-permute-start | bytes 983048 | tf_op jit(solution)/shard_map/ppermute | solution.py:31
  52.0 7.5 %collective-permute-start.9 = (bf16[128,1280]{1,0:T(8,128)(2,1)S(1)}, bf16[128,1280]{1,0:T(8,128)(2,1)S(1)}, u32[]{:S(2)}, u32[]{:S(2)}) collective-permute-start(bf16[128,1280]{1,0:T(8,128)(2,1)S(1)} %slice.176), channel_id=1, source_target_pairs={{0,96},{32,0},{64,32},{96,64},{1,97},{33,1},{65,33},{97,65},{2,98}... | collective-permute-start | bytes 983048 | tf_op jit(solution)/shard_map/ppermute | solution.py:31
  52.6 10.3 %collective-permute-start.16 = (bf16[128,1280]{1,0:T(8,128)(2,1)S(1)}, bf16[128,1280]{1,0:T(8,128)(2,1)S(1)}, u32[]{:S(2)}, u32[]{:S(2)}) collective-permute-start(bf16[128,1280]{1,0:T(8,128)(2,1)S(1)} %slice.179), channel_id=1, source_target_pairs={{0,8},{8,16},{16,24},{24,0},{1,9},{9,17},{17,25},{25,1},{2,10},{10... | collective-permute-start | bytes 983048 | tf_op jit(solution)/shard_map/ppermute | solution.py:31
  56.1 8.5 %collective-permute-start.17 = (bf16[128,1280]{1,0:T(8,128)(2,1)S(1)}, bf16[128,1280]{1,0:T(8,128)(2,1)S(1)}, u32[]{:S(2)}, u32[]{:S(2)}) collective-permute-start(bf16[128,1280]{1,0:T(8,128)(2,1)S(1)} %slice.180), channel_id=1, source_target_pairs={{0,24},{8,0},{16,8},{24,16},{1,25},{9,1},{17,9},{25,17},{2,26},{10... | collective-permute-start | bytes 983048 | tf_op jit(solution)/shard_map/ppermute | solution.py:31
  60.9 29.4 %copy-start.27 = (bf16[3,512]{1,0:T(4,128)(2,1)S(1)}, bf16[3,512]{1,0:T(4,128)(2,1)}, u32[]{:S(2)}) copy-start(bf16[3,512]{1,0:T(4,128)(2,1)} %param.29) | copy-start | bytes 9220
  60.9 23.1 %collective-permute-start.10 = (bf16[1024,512]{1,0:T(8,128)(2,1)S(1)}, bf16[1024,512]{1,0:T(8,128)(2,1)S(1)}, u32[]{:S(2)}, u32[]{:S(2)}) collective-permute-start(bf16[1024,512]{1,0:T(8,128)(2,1)S(1)} %get-tuple-element.30.refs_0_), channel_id=1, source_target_pairs={{0,8},{8,16},{16,24},{24,0},{1,9},{9,17},{17,25},{25,1},{2,10},{10... | collective-permute-start | bytes 3145736 | tf_op jit(solution)/shard_map/ppermute | solution.py:31
  62.2 23.6 %collective-permute-start.11 = (bf16[1024,512]{1,0:T(8,128)(2,1)S(1)}, bf16[1024,512]{1,0:T(8,128)(2,1)S(1)}, u32[]{:S(2)}, u32[]{:S(2)}) collective-permute-start(bf16[1024,512]{1,0:T(8,128)(2,1)S(1)} %get-tuple-element.30.refs_0_), channel_id=1, source_target_pairs={{0,24},{8,0},{16,8},{24,16},{1,25},{9,1},{17,9},{25,17},{2,26},{10... | collective-permute-start | bytes 3145736 | tf_op jit(solution)/shard_map/ppermute | solution.py:31
  66.0 21.6 %collective-permute-start.18 = (bf16[1024,512]{1,0:T(8,128)(2,1)S(1)}, bf16[1024,512]{1,0:T(8,128)(2,1)S(1)}, u32[]{:S(2)}, u32[]{:S(2)}) collective-permute-start(bf16[1024,512]{1,0:T(8,128)(2,1)S(1)} %get-tuple-element.34.refs_0_), channel_id=1, source_target_pairs={{0,32},{32,64},{64,96},{96,0},{1,33},{33,65},{65,97},{97,1},{2,34}... | collective-permute-start | bytes 3145736 | tf_op jit(solution)/shard_map/ppermute | solution.py:31
  68.2 21.1 %collective-permute-start.19 = (bf16[1024,512]{1,0:T(8,128)(2,1)S(1)}, bf16[1024,512]{1,0:T(8,128)(2,1)S(1)}, u32[]{:S(2)}, u32[]{:S(2)}) collective-permute-start(bf16[1024,512]{1,0:T(8,128)(2,1)S(1)} %get-tuple-element.34.refs_0_), channel_id=1, source_target_pairs={{0,96},{32,0},{64,32},{96,64},{1,97},{33,1},{65,33},{97,65},{2,98}... | collective-permute-start | bytes 3145736 | tf_op jit(solution)/shard_map/ppermute | solution.py:31
  84.0 5.3 %copy-start.2 = (bf16[1024,512]{1,0:T(8,128)(2,1)}, bf16[1024,512]{1,0:T(8,128)(2,1)S(1)}, u32[]{:S(2)}) copy-start(bf16[1024,512]{1,0:T(8,128)(2,1)S(1)} %collective-permute-done.10.refs_1_) | copy-start | bytes 3145732
  84.0 34.8 %collective-permute-start.28 = (bf16[1024,768]{1,0:T(8,128)(2,1)}, bf16[1024,768]{1,0:T(8,128)(2,1)}, u32[]{:S(2)}, u32[]{:S(2)}) collective-permute-start(bf16[1024,768]{1,0:T(8,128)(2,1)} %get-tuple-element.45.refs_0_), channel_id=1, source_target_pairs={{0,8},{8,16},{16,24},{24,0},{1,9},{9,17},{17,25},{25,1},{2,10},{10... | collective-permute-start | bytes 4718600 | tf_op jit(solution)/shard_map/ppermute | solution.py:31
  85.8 35.5 %collective-permute-start.29 = (bf16[1024,768]{1,0:T(8,128)(2,1)}, bf16[1024,768]{1,0:T(8,128)(2,1)}, u32[]{:S(2)}, u32[]{:S(2)}) collective-permute-start(bf16[1024,768]{1,0:T(8,128)(2,1)} %get-tuple-element.45.refs_0_), channel_id=1, source_target_pairs={{0,24},{8,0},{16,8},{24,16},{1,25},{9,1},{17,9},{25,17},{2,26},{10... | collective-permute-start | bytes 4718600 | tf_op jit(solution)/shard_map/ppermute | solution.py:31
  87.6 35.6 %collective-permute-start.32 = (bf16[1024,768]{1,0:T(8,128)(2,1)}, bf16[1024,768]{1,0:T(8,128)(2,1)S(1)}, u32[]{:S(2)}, u32[]{:S(2)}) collective-permute-start(bf16[1024,768]{1,0:T(8,128)(2,1)} %get-tuple-element.46.refs_0_), channel_id=1, source_target_pairs={{0,32},{32,64},{64,96},{96,0},{1,33},{33,65},{65,97},{97,1},{2,34}... | collective-permute-start | bytes 4718600 | tf_op jit(solution)/shard_map/ppermute | solution.py:31
  89.3 35.7 %collective-permute-start.33 = (bf16[1024,768]{1,0:T(8,128)(2,1)}, bf16[1024,768]{1,0:T(8,128)(2,1)S(1)}, u32[]{:S(2)}, u32[]{:S(2)}) collective-permute-start(bf16[1024,768]{1,0:T(8,128)(2,1)} %get-tuple-element.46.refs_0_), channel_id=1, source_target_pairs={{0,96},{32,0},{64,32},{96,64},{1,97},{33,1},{65,33},{97,65},{2,98}... | collective-permute-start | bytes 4718600 | tf_op jit(solution)/shard_map/ppermute | solution.py:31
  118.8 26.2 %collective-permute-start.12 = (bf16[512,512]{1,0:T(8,128)(2,1)S(1)}, bf16[512,512]{1,0:T(8,128)(2,1)S(1)}, u32[]{:S(2)}, u32[]{:S(2)}) collective-permute-start(bf16[512,512]{1,0:T(8,128)(2,1)S(1)} %slice.177), channel_id=1, source_target_pairs={{0,8},{8,16},{16,24},{24,0},{1,9},{9,17},{17,25},{25,1},{2,10},{10... | collective-permute-start | bytes 1572872 | tf_op jit(solution)/shard_map/ppermute | solution.py:31
  121.3 23.8 %collective-permute-start.13 = (bf16[512,512]{1,0:T(8,128)(2,1)S(1)}, bf16[512,512]{1,0:T(8,128)(2,1)S(1)}, u32[]{:S(2)}, u32[]{:S(2)}) collective-permute-start(bf16[512,512]{1,0:T(8,128)(2,1)S(1)} %slice.178), channel_id=1, source_target_pairs={{0,24},{8,0},{16,8},{24,16},{1,25},{9,1},{17,9},{25,17},{2,26},{10... | collective-permute-start | bytes 1572872 | tf_op jit(solution)/shard_map/ppermute | solution.py:31
  123.3 25.0 %collective-permute-start.20 = (bf16[512,512]{1,0:T(8,128)(2,1)S(1)}, bf16[512,512]{1,0:T(8,128)(2,1)S(1)}, u32[]{:S(2)}, u32[]{:S(2)}) collective-permute-start(bf16[512,512]{1,0:T(8,128)(2,1)S(1)} %slice.181), channel_id=1, source_target_pairs={{0,32},{32,64},{64,96},{96,0},{1,33},{33,65},{65,97},{97,1},{2,34}... | collective-permute-start | bytes 1572872 | tf_op jit(solution)/shard_map/ppermute | solution.py:31
  125.0 24.9 %collective-permute-start.21 = (bf16[512,512]{1,0:T(8,128)(2,1)S(1)}, bf16[512,512]{1,0:T(8,128)(2,1)S(1)}, u32[]{:S(2)}, u32[]{:S(2)}) collective-permute-start(bf16[512,512]{1,0:T(8,128)(2,1)S(1)} %slice.182), channel_id=1, source_target_pairs={{0,96},{32,0},{64,32},{96,64},{1,97},{33,1},{65,33},{97,65},{2,98}... | collective-permute-start | bytes 1572872 | tf_op jit(solution)/shard_map/ppermute | solution.py:31
  125.5 6.6 %copy-start.17 = (bf16[4096,64]{0,1:T(8,128)(2,1)S(1)}, bf16[4096,64]{0,1:T(8,128)(2,1)}, u32[]{:S(2)}) copy-start(bf16[4096,64]{0,1:T(8,128)(2,1)} %param.24) | copy-start | bytes 1572868
  125.6 6.6 %copy-start.18 = (bf16[64,256]{1,0:T(8,128)(2,1)S(1)}, bf16[64,256]{1,0:T(8,128)(2,1)}, u32[]{:S(2)}) copy-start(bf16[64,256]{1,0:T(8,128)(2,1)} %right_ref.1) | copy-start | bytes 98308
  125.6 6.6 %copy-start.19 = (f32[2,768]{1,0:T(2,128)S(1)}, f32[2,768]{1,0:T(2,128)}, u32[]{:S(2)}) copy-start(f32[2,768]{1,0:T(2,128)} %spike_ref.1) | copy-start | bytes 18436
  125.6 6.6 %copy-start.20 = (f32[256]{0:T(256)S(1)}, f32[256]{0:T(256)}, u32[]{:S(2)}) copy-start(f32[256]{0:T(256)} %param.26) | copy-start | bytes 3076
  125.6 34.9 %collective-permute-start.30 = (bf16[512,768]{1,0:T(8,128)(2,1)S(1)}, bf16[512,768]{1,0:T(8,128)(2,1)S(1)}, u32[]{:S(2)}, u32[]{:S(2)}) collective-permute-start(bf16[512,768]{1,0:T(8,128)(2,1)S(1)} %slice.194), channel_id=1, source_target_pairs={{0,8},{8,16},{16,24},{24,0},{1,9},{9,17},{17,25},{25,1},{2,10},{10... | collective-permute-start | bytes 2359304 | tf_op jit(solution)/shard_map/ppermute | solution.py:31
  132.2 6.5 %copy-start.3 = (bf16[1024,512]{1,0:T(8,128)(2,1)S(1)}, bf16[1024,512]{1,0:T(8,128)(2,1)}, u32[]{:S(2)}) copy-start(bf16[1024,512]{1,0:T(8,128)(2,1)} %copy-done.2) | copy-start | bytes 3145732
  132.2 6.5 %copy-start.5 = (bf16[1024,512]{1,0:T(8,128)(2,1)S(1)}, bf16[1024,512]{1,0:T(8,128)(2,1)}, u32[]{:S(2)}) copy-start(bf16[1024,512]{1,0:T(8,128)(2,1)} %copy-done.4) | copy-start | bytes 3145732
  132.2 6.5 %copy-start.11 = (bf16[1024,512]{1,0:T(8,128)(2,1)S(1)}, bf16[1024,512]{1,0:T(8,128)(2,1)}, u32[]{:S(2)}) copy-start(bf16[1024,512]{1,0:T(8,128)(2,1)} %copy-done.10) | copy-start | bytes 3145732
  145.0 19.7 %collective-permute-start.31 = (bf16[512,768]{1,0:T(8,128)(2,1)S(1)}, bf16[512,768]{1,0:T(8,128)(2,1)S(1)}, u32[]{:S(2)}, u32[]{:S(2)}) collective-permute-start(bf16[512,768]{1,0:T(8,128)(2,1)S(1)} %slice.195), channel_id=1, source_target_pairs={{0,24},{8,0},{16,8},{24,16},{1,25},{9,1},{17,9},{25,17},{2,26},{10... | collective-permute-start | bytes 2359304 | tf_op jit(solution)/shard_map/ppermute | solution.py:31
  145.1 29.9 %collective-permute-start.34 = (bf16[512,768]{1,0:T(8,128)(2,1)S(1)}, bf16[512,768]{1,0:T(8,128)(2,1)S(1)}, u32[]{:S(2)}, u32[]{:S(2)}) collective-permute-start(bf16[512,768]{1,0:T(8,128)(2,1)S(1)} %slice.196), channel_id=1, source_target_pairs={{0,32},{32,64},{64,96},{96,0},{1,33},{33,65},{65,97},{97,1},{2,34}... | collective-permute-start | bytes 2359304 | tf_op jit(solution)/shard_map/ppermute | solution.py:31
  148.3 26.7 %collective-permute-start.35 = (bf16[512,768]{1,0:T(8,128)(2,1)S(1)}, bf16[512,768]{1,0:T(8,128)(2,1)S(1)}, u32[]{:S(2)}, u32[]{:S(2)}) collective-permute-start(bf16[512,768]{1,0:T(8,128)(2,1)S(1)} %slice.197), channel_id=1, source_target_pairs={{0,96},{32,0},{64,32},{96,64},{1,97},{33,1},{65,33},{97,65},{2,98}... | collective-permute-start | bytes 2359304 | tf_op jit(solution)/shard_map/ppermute | solution.py:31
  152.1 28.3 %collective-permute-start.22 = (bf16[2,272,128]{2,1,0:T(8,128)(2,1)S(1)}, bf16[2,272,128]{2,1,0:T(8,128)(2,1)S(1)}, u32[]{:S(2)}, u32[]{:S(2)}) collective-permute-start(bf16[2,272,128]{2,1,0:T(8,128)(2,1)S(1)} %pad_maximum_fusion.2), channel_id=1, source_target_pairs={{0,24},{8,0},{16,8},{24,16},{1,25},{9,1},{17,9},{25,17},{2,26},{10... | collective-permute-start | bytes 417800 | tf_op jit(solution)/shard_map/ppermute | solution.py:31
  160.5 19.9 %collective-permute-start.23 = (bf16[2,272,128]{2,1,0:T(8,128)(2,1)S(1)}, bf16[2,272,128]{2,1,0:T(8,128)(2,1)S(1)}, u32[]{:S(2)}, u32[]{:S(2)}) collective-permute-start(bf16[2,272,128]{2,1,0:T(8,128)(2,1)S(1)} %pad_maximum_fusion.2), channel_id=1, source_target_pairs={{0,16},{8,24},{16,0},{24,8},{1,17},{9,25},{17,1},{25,9},{2,18},{10... | collective-permute-start | bytes 417800 | tf_op jit(solution)/shard_map/ppermute | solution.py:31
  164.7 15.8 %collective-permute-start.24 = (bf16[2,272,128]{2,1,0:T(8,128)(2,1)S(1)}, bf16[2,272,128]{2,1,0:T(8,128)(2,1)S(1)}, u32[]{:S(2)}, u32[]{:S(2)}) collective-permute-start(bf16[2,272,128]{2,1,0:T(8,128)(2,1)S(1)} %pad_maximum_fusion.2), channel_id=1, source_target_pairs={{0,8},{8,16},{16,24},{24,0},{1,9},{9,17},{17,25},{25,1},{2,10},{10... | collective-permute-start | bytes 417800 | tf_op jit(solution)/shard_map/ppermute | solution.py:31
  180.7 6.8 %collective-permute-start.26 = (bf16[2,272,128]{2,1,0:T(8,128)(2,1)S(1)}, bf16[2,272,128]{2,1,0:T(8,128)(2,1)S(1)}, u32[]{:S(2)}, u32[]{:S(2)}) collective-permute-start(bf16[2,272,128]{2,1,0:T(8,128)(2,1)S(1)} %pad_maximum_fusion.3), channel_id=1, source_target_pairs={{0,32},{32,64},{64,96},{96,0},{1,33},{33,65},{65,97},{97,1},{2,34}... | collective-permute-start | bytes 417800 | tf_op jit(solution)/shard_map/ppermute | solution.py:31
  182.5 6.6 %collective-permute-start.25 = (bf16[2,272,128]{2,1,0:T(8,128)(2,1)S(1)}, bf16[2,272,128]{2,1,0:T(8,128)(2,1)S(1)}, u32[]{:S(2)}, u32[]{:S(2)}) collective-permute-start(bf16[2,272,128]{2,1,0:T(8,128)(2,1)S(1)} %pad_maximum_fusion.3), channel_id=1, source_target_pairs={{0,64},{32,96},{64,0},{96,32},{1,65},{33,97},{65,1},{97,33},{2,66}... | collective-permute-start | bytes 417800 | tf_op jit(solution)/shard_map/ppermute | solution.py:31
  187.4 5.3 %copy-start.16 = (bf16[2,256]{1,0:T(2,128)(2,1)S(1)}, bf16[2,256]{1,0:T(2,128)(2,1)}, u32[]{:S(2)}) copy-start(bf16[2,256]{1,0:T(2,128)(2,1)} %gain_ref.3) | copy-start | bytes 3076
  187.4 5.1 %collective-permute-start.27 = (bf16[2,272,128]{2,1,0:T(8,128)(2,1)S(1)}, bf16[2,272,128]{2,1,0:T(8,128)(2,1)S(1)}, u32[]{:S(2)}, u32[]{:S(2)}) collective-permute-start(bf16[2,272,128]{2,1,0:T(8,128)(2,1)S(1)} %pad_maximum_fusion.3), channel_id=1, source_target_pairs={{0,96},{32,0},{64,32},{96,64},{1,97},{33,1},{65,33},{97,65},{2,98}... | collective-permute-start | bytes 417800 | tf_op jit(solution)/shard_map/ppermute | solution.py:31
  196.3 6.2 %collective-permute-start.38 = (bf16[96,4096]{1,0:T(8,128)(2,1)S(1)}, bf16[96,4096]{1,0:T(8,128)(2,1)S(1)}, u32[]{:S(2)}, u32[]{:S(2)}) collective-permute-start(bf16[96,4096]{1,0:T(8,128)(2,1)S(1)} %get-tuple-element.54), channel_id=1, source_target_pairs={{0,1},{1,0},{2,3},{3,2},{4,5},{5,4},{6,7},{7,6},{8,9},{9,8},{10,11... | collective-permute-start | bytes 2359304 | tf_op jit(solution)/shard_map/ppermute | solution.py:35
  199.5 20.0 %collective-permute-start.36 = (bf16[96,4096]{1,0:T(8,128)(2,1)S(1)}, bf16[96,4096]{1,0:T(8,128)(2,1)S(1)}, u32[]{:S(2)}, u32[]{:S(2)}) collective-permute-start(bf16[96,4096]{1,0:T(8,128)(2,1)S(1)} %get-tuple-element.48), channel_id=1, source_target_pairs={{0,1},{1,0},{2,3},{3,2},{4,5},{5,4},{6,7},{7,6},{8,9},{9,8},{10,11... | collective-permute-start | bytes 2359304 | tf_op jit(solution)/shard_map/ppermute | solution.py:35
  202.4 3.6 %collective-permute-start.37 = (bf16[192,4096]{1,0:T(8,128)(2,1)S(1)}, bf16[192,4096]{1,0:T(8,128)(2,1)S(1)}, u32[]{:S(2)}, u32[]{:S(2)}) collective-permute-start(bf16[192,4096]{1,0:T(8,128)(2,1)S(1)} %get-tuple-element.51), channel_id=1, source_target_pairs={{0,1},{1,0},{2,3},{3,2},{4,5},{5,4},{6,7},{7,6},{8,9},{9,8},{10,11... | collective-permute-start | bytes 4718600 | tf_op jit(solution)/shard_map/ppermute | solution.py:35
  202.7 12.8 %collective-permute-start.43 = (bf16[48,4096]{1,0:T(8,128)(2,1)S(1)}, bf16[48,4096]{1,0:T(8,128)(2,1)S(1)}, u32[]{:S(2)}, u32[]{:S(2)}) collective-permute-start(bf16[48,4096]{1,0:T(8,128)(2,1)S(1)} %get-tuple-element.70), channel_id=1, source_target_pairs={{0,6},{2,0},{4,2},{6,4},{1,7},{3,1},{5,3},{7,5},{8,14},{10,8},{12,... | collective-permute-start | bytes 1179656 | tf_op jit(solution)/shard_map/ppermute | solution.py:31
  202.8 12.7 %collective-permute-start.39 = (bf16[48,4096]{1,0:T(8,128)(2,1)S(1)}, bf16[48,4096]{1,0:T(8,128)(2,1)S(1)}, u32[]{:S(2)}, u32[]{:S(2)}) collective-permute-start(bf16[48,4096]{1,0:T(8,128)(2,1)S(1)} %get-tuple-element.71), channel_id=1, source_target_pairs={{0,2},{2,4},{4,6},{6,0},{1,3},{3,5},{5,7},{7,1},{8,10},{10,12},{12... | collective-permute-start | bytes 1179656 | tf_op jit(solution)/shard_map/ppermute | solution.py:31
  206.7 17.3 %collective-permute-start.41 = (bf16[48,4096]{1,0:T(8,128)(2,1)S(1)}, bf16[48,4096]{1,0:T(8,128)(2,1)S(1)}, u32[]{:S(2)}, u32[]{:S(2)}) collective-permute-start(bf16[48,4096]{1,0:T(8,128)(2,1)S(1)} %get-tuple-element.69), channel_id=1, source_target_pairs={{0,2},{2,4},{4,6},{6,0},{1,3},{3,5},{5,7},{7,1},{8,10},{10,12},{12... | collective-permute-start | bytes 1179656 | tf_op jit(solution)/shard_map/ppermute | solution.py:31
  215.7 15.9 %collective-permute-start.40 = (bf16[48,4096]{1,0:T(8,128)(2,1)S(1)}, bf16[48,4096]{1,0:T(8,128)(2,1)S(1)}, u32[]{:S(2)}, u32[]{:S(2)}) collective-permute-start(bf16[48,4096]{1,0:T(8,128)(2,1)S(1)} %get-tuple-element.67), channel_id=1, source_target_pairs={{0,2},{2,4},{4,6},{6,0},{1,3},{3,5},{5,7},{7,1},{8,10},{10,12},{12... | collective-permute-start | bytes 1179656 | tf_op jit(solution)/shard_map/ppermute | solution.py:31
  219.4 13.2 %collective-permute-start.44 = (bf16[48,4096]{1,0:T(8,128)(2,1)S(1)}, bf16[48,4096]{1,0:T(8,128)(2,1)S(1)}, u32[]{:S(2)}, u32[]{:S(2)}) collective-permute-start(bf16[48,4096]{1,0:T(8,128)(2,1)S(1)} %get-tuple-element.66), channel_id=1, source_target_pairs={{0,6},{2,0},{4,2},{6,4},{1,7},{3,1},{5,3},{7,5},{8,14},{10,8},{12,... | collective-permute-start | bytes 1179656 | tf_op jit(solution)/shard_map/ppermute | solution.py:31
  219.4 18.9 %collective-permute-start.42 = (bf16[48,4096]{1,0:T(8,128)(2,1)S(1)}, bf16[48,4096]{1,0:T(8,128)(2,1)S(1)}, u32[]{:S(2)}, u32[]{:S(2)}) collective-permute-start(bf16[48,4096]{1,0:T(8,128)(2,1)S(1)} %get-tuple-element.68), channel_id=1, source_target_pairs={{0,6},{2,0},{4,2},{6,4},{1,7},{3,1},{5,3},{7,5},{8,14},{10,8},{12,... | collective-permute-start | bytes 1179656 | tf_op jit(solution)/shard_map/ppermute | solution.py:31
  (12 other events, 26.8 us)

commit v3 on v2

--- a/solution.py
+++ b/solution.py
@@ -463,7 +463,7 @@
     return jnp.concatenate(lines, axis=0)
 
 
-def conv_kernel(groups, t_ref, b_ref, filter_ref, *outs):
+def conv_kernel(groups, t_ref, b_ref, filter_ref, mixer_ref, *outs):
     spots, part = [], outs[0].shape[0] // (PAIR * len(groups[0]))
     for steps in groups:
         spots += targets(steps, part)
@@ -479,7 +479,7 @@
             at += ref.shape[0]
 
 
-def conv_call(groups, t, b, filt, part):
+def conv_call(groups, t, b, filt, mixer, part):
     return vmem_kernel(
         functools.partial(conv_kernel, groups),
         tuple(
@@ -490,7 +490,8 @@
         t,
         b,
         filt,
-        in_specs=[pl.BlockSpec(memory_space=pltpu.VMEM)] * 3,
+        mixer,
+        in_specs=[pl.BlockSpec(memory_space=pltpu.VMEM)] * 4,
         out_specs=tuple(pl.BlockSpec(memory_space=pltpu.VMEM) for _ in groups),
     )
 
@@ -596,12 +597,12 @@
     mixed_b = gate_call(x, acc_b, w_b[3:], late, taps[:, half:], 0)
 
     groups = ((2,), (1, 3))
-    shares = dict(zip(groups, conv_call(groups, mixed_t, mixed_b, filter_result, part)))
+    shares = dict(zip(groups, conv_call(groups, mixed_t, mixed_b, filter_result, mixer_result, part)))
 
     def partial(*steps):
         share = shares.get(steps)
         if share is None:
-            share = conv_call((steps,), mixed_t, mixed_b, filter_result, part)[0]
+            share = conv_call((steps,), mixed_t, mixed_b, filter_result, mixer_result, part)[0]
         own, other = term_call(steps, mixed_attn, mixer_result, share, part)
         return plus(own, swap(other))
 

time: 240 us -> 237 us (0.988)
  the two profiles are of different devices: /device:TPU:54 before, /device:TPU:1 now
where the time goes in v3:
time: 237 us; the launch traced here: 233 us
  waiting for transfers between devices  90.5 us (38%)
  starting transfers between devices  78.5 us (33%)
  Pallas kernels  52.6 us (22%)
  local copies, waits for them, and re-layouts  8.17 us (3%)
  other arithmetic  2.74 us (1%)
    ppermute x40, waiting for transfers between devices, hop(): lax.ppermute(value, axis, [(i, (i + steps) % RING) for i in range(RING)])  87.3 us
    ppermute x40, starting transfers between devices, hop(): lax.ppermute(value, axis, [(i, (i + steps) % RING) for i in range(RING)])  60.9 us
    pallas_call x22, Pallas kernels, vmem_kernel(): pl.pallas_call(kernel, out_shape=out_shape, compiler_params=pltpu.Compile...  52.6 us
    ppermute x4, starting transfers between devices, swap(): return lax.ppermute(value, 'c', [(0, 1), (1, 0)])  13.4 us
  transfers between devices with their start and end apart: 45, of which 17 were waited for; matrix products, arithmetic and copies ran while one was open for 3% of the time, Pallas kernels for 21%

profile of v3, /device:TPU:1, one launch (start us, length us, event | category | flops | bytes accessed | tf_op | source)
XLA Modules:
  0.0 233.4 jit_solution(8732735363411787005)
XLA Ops:
  0.0 1.1 copy-done.14
  2.3 4.2 %collective-permute-start = (bf16[16,4096]{1,0:T(8,128)(2,1)S(1)}, bf16[16,4096]{1,0:T(8,128)(2,1)S(1)}, u32[]{:S(2)}, u32[]{:S(2)}) collective-permute-start(bf16[16,4096]{1,0:T(8,128)(2,1)S(1)} %slice.172), channel_id=1, source_target_pairs={{0,8},{8,16},{16,24},{24,32},{32,40},{40,48},{48,56},{56,64},{64,7... | collective-permute-start | bytes 393224 | tf_op jit(solution)/shard_map/ppermute | solution.py:40
  6.5 2.2 collective-permute-done
  8.7 2.5 %collective-permute-start.2 = (bf16[112,4096]{1,0:T(8,128)(2,1)S(1)}, bf16[112,4096]{1,0:T(8,128)(2,1)S(1)}, u32[]{:S(2)}, u32[]{:S(2)}) collective-permute-start(bf16[112,4096]{1,0:T(8,128)(2,1)S(1)} %pad_maximum_fusion.own), channel_id=1, source_target_pairs={{0,6},{2,0},{4,2},{6,4},{1,7},{3,1},{5,3},{7,5},{8,14},{10,8},{12,... | collective-permute-start | bytes 2752520 | tf_op jit(solution)/shard_map/ppermute | solution.py:31
  11.4 18.0 %collective-permute-done.2.above = bf16[112,4096]{1,0:T(8,128)(2,1)S(1)} collective-permute-done((bf16[112,4096]{1,0:T(8,128)(2,1)S(1)}, bf16[112,4096]{1,0:T(8,128)(2,1)S(1)}, u32[]{:S(2)}, u32[]{:S(2)}) %collective-permute-start.2) | collective-permute-done | bytes 917536 | tf_op jit(solution)/shard_map/ppermute | solution.py:31
  29.5 3.5 %collective-permute-start.4 = (bf16[64,4096]{1,0:T(8,128)(2,1)S(1)}, bf16[64,4096]{1,0:T(8,128)(2,1)S(1)}, u32[]{:S(2)}, u32[]{:S(2)}) collective-permute-start(bf16[64,4096]{1,0:T(8,128)(2,1)S(1)} %slice.174), channel_id=1, source_target_pairs={{0,6},{2,0},{4,2},{6,4},{1,7},{3,1},{5,3},{7,5},{8,14},{10,8},{12,... | collective-permute-start | bytes 1572872 | tf_op jit(solution)/shard_map/ppermute | solution.py:31
  33.2 4.7 %collective-permute-start.6 = (bf16[256,1280]{1,0:T(8,128)(2,1)S(1)}, bf16[256,1280]{1,0:T(8,128)(2,1)S(1)}, u32[]{:S(2)}, u32[]{:S(2)}) collective-permute-start(bf16[256,1280]{1,0:T(8,128)(2,1)S(1)} %slice_dynamic-update-slice_fusion.own), channel_id=1, source_target_pairs={{0,32},{32,64},{64,96},{96,0},{1,33},{33,65},{65,97},{97,1},{2,34}... | collective-permute-start | bytes 1966088 | tf_op jit(solution)/shard_map/ppermute | solution.py:31
  37.9 2.2 collective-permute-start.7
  40.2 2.1 collective-permute-done.3.top
  42.3 3.6 %collective-permute-start.15 = (bf16[256,1280]{1,0:T(8,128)(2,1)S(1)}, bf16[256,1280]{1,0:T(8,128)(2,1)S(1)}, u32[]{:S(2)}, u32[]{:S(2)}) collective-permute-start(bf16[256,1280]{1,0:T(8,128)(2,1)S(1)} %pad_maximum_fusion.1.own), channel_id=1, source_target_pairs={{0,24},{8,0},{16,8},{24,16},{1,25},{9,1},{17,9},{25,17},{2,26},{10... | collective-permute-start | bytes 1966088 | tf_op jit(solution)/shard_map/ppermute | solution.py:31
  46.0 2.1 shard_map.155.mine
  48.1 3.8 %collective-permute-start.5 = (bf16[448,4096]{1,0:T(8,128)(2,1)}, bf16[448,4096]{1,0:T(8,128)(2,1)}, u32[]{:S(2)}, u32[]{:S(2)}) collective-permute-start(bf16[448,4096]{1,0:T(8,128)(2,1)} %shard_map.155.mine), channel_id=1, source_target_pairs={{0,1},{1,0},{2,3},{3,2},{4,5},{5,4},{6,7},{7,6},{8,9},{9,8},{10,11... | collective-permute-start | bytes 11010056 | tf_op jit(solution)/shard_map/ppermute | solution.py:35
  52.5 1.1 collective-permute-start.8
  53.6 2.2 collective-permute-start.9
  56.8 3.2 %collective-permute-start.17 = (bf16[128,1280]{1,0:T(8,128)(2,1)S(1)}, bf16[128,1280]{1,0:T(8,128)(2,1)S(1)}, u32[]{:S(2)}, u32[]{:S(2)}) collective-permute-start(bf16[128,1280]{1,0:T(8,128)(2,1)S(1)} %slice.180), channel_id=1, source_target_pairs={{0,24},{8,0},{16,8},{24,16},{1,25},{9,1},{17,9},{25,17},{2,26},{10... | collective-permute-start | bytes 983048 | tf_op jit(solution)/shard_map/ppermute | solution.py:31
  61.2 1.3 shard_map.157
  62.5 2.5 %collective-permute-start.10 = (bf16[1024,512]{1,0:T(8,128)(2,1)S(1)}, bf16[1024,512]{1,0:T(8,128)(2,1)S(1)}, u32[]{:S(2)}, u32[]{:S(2)}) collective-permute-start(bf16[1024,512]{1,0:T(8,128)(2,1)S(1)} %get-tuple-element.30.refs_0_), channel_id=1, source_target_pairs={{0,8},{8,16},{16,24},{24,0},{1,9},{9,17},{17,25},{25,1},{2,10},{10... | collective-permute-start | bytes 3145736 | tf_op jit(solution)/shard_map/ppermute | solution.py:31
  65.2 1.4 shard_map.160
  66.6 1.8 collective-permute-start.18
  68.3 2.1 collective-permute-start.19
  71.5 14.8 %collective-permute-done.10.refs_1_ = bf16[1024,512]{1,0:T(8,128)(2,1)S(1)} collective-permute-done((bf16[1024,512]{1,0:T(8,128)(2,1)S(1)}, bf16[1024,512]{1,0:T(8,128)(2,1)S(1)}, u32[]{:S(2)}, u32[]{:S(2)}) %collective-permute-start.10) | collective-permute-done | bytes 1048608 | tf_op jit(solution)/shard_map/ppermute | solution.py:31
  86.2 1.9 collective-permute-start.28
  88.2 3.4 %collective-permute-start.29 = (bf16[1024,768]{1,0:T(8,128)(2,1)}, bf16[1024,768]{1,0:T(8,128)(2,1)}, u32[]{:S(2)}, u32[]{:S(2)}) collective-permute-start(bf16[1024,768]{1,0:T(8,128)(2,1)} %get-tuple-element.45.refs_0_), channel_id=1, source_target_pairs={{0,24},{8,0},{16,8},{24,16},{1,25},{9,1},{17,9},{25,17},{2,26},{10... | collective-permute-start | bytes 4718600 | tf_op jit(solution)/shard_map/ppermute | solution.py:31
  91.6 1.7 collective-permute-start.32
  93.3 1.1 collective-permute-start.33
  94.4 1.2 slice.177
  95.6 1.1 slice.178
  96.8 23.2 %collective-permute-done.28.refs_1_ = bf16[1024,768]{1,0:T(8,128)(2,1)} collective-permute-done((bf16[1024,768]{1,0:T(8,128)(2,1)}, bf16[1024,768]{1,0:T(8,128)(2,1)}, u32[]{:S(2)}, u32[]{:S(2)}) %collective-permute-start.28) | collective-permute-done | bytes 1572896 | tf_op jit(solution)/shard_map/ppermute | solution.py:31
  120.0 1.9 collective-permute-start.12
  121.9 1.2 slice.194
  123.1 2.3 collective-permute-start.13
  125.4 1.2 slice.195
  126.6 1.8 collective-permute-start.20
  128.5 1.0 collective-permute-start.21
  129.9 3.7 %shard_map.156.x_ref = bf16[784,4096]{1,0:T(8,128)(2,1)S(1)} custom-call(bf16[448,4096]{1,0:T(8,128)(2,1)} %shard_map.155.mine, bf16[448,4096]{1,0:T(8,128)(2,1)} %collective-permute-done.5.other), custom_call_target="tpu_custom_call" | custom-call | flops 2000000000 | bytes 8000000 | tf_op jit(solution)/shard_map/pallas_call | solution.py:52
  133.6 3.1 %shard_map.158.acc_ref = f32[768,512]{1,0:T(8,128)S(1)} custom-call(bf16[784,4096]{1,0:T(8,128)(2,1)S(1)} %shard_map.156.x_ref, bf16[1024,512]{1,0:T(8,128)(2,1)S(1)} %copy-done.11, bf16[1024,512]{1,0:T(8,128)(2,1)S(1)} %copy-done.3, bf16[1024,512]{1,0:T(8,128)(2,1)S(1)} %copy-done.5), custom_call_target="tpu_custom_call" | custom-call | flops 3000000000 | bytes 8000000 | tf_op jit(solution)/shard_map/pallas_call | solution.py:52
  136.8 3.1 %shard_map.161.acc_ref = f32[768,512]{1,0:T(8,128)S(1)} custom-call(bf16[784,4096]{1,0:T(8,128)(2,1)S(1)} %shard_map.156.x_ref, bf16[1024,512]{1,0:T(8,128)(2,1)S(1)} %copy-done.13, bf16[1024,512]{1,0:T(8,128)(2,1)S(1)} %copy-done.7, bf16[1024,512]{1,0:T(8,128)(2,1)S(1)} %copy-done.9), custom_call_target="tpu_custom_call" | custom-call | flops 3000000000 | bytes 8000000 | tf_op jit(solution)/shard_map/pallas_call | solution.py:52
  140.0 2.6 %collective-permute-start.31 = (bf16[512,768]{1,0:T(8,128)(2,1)S(1)}, bf16[512,768]{1,0:T(8,128)(2,1)S(1)}, u32[]{:S(2)}, u32[]{:S(2)}) collective-permute-start(bf16[512,768]{1,0:T(8,128)(2,1)S(1)} %slice.195), channel_id=1, source_target_pairs={{0,24},{8,0},{16,8},{24,16},{1,25},{9,1},{17,9},{25,17},{2,26},{10... | collective-permute-start | bytes 2359304 | tf_op jit(solution)/shard_map/ppermute | solution.py:31
  143.1 1.4 shard_map.159.qk_ref
  144.6 6.4 %shard_map.163 = (f32[768,256]{1,0:T(8,128)S(1)}, f32[768,256]{1,0:T(8,128)S(1)}, f32[768,256]{1,0:T(8,128)S(1)}, f32[768,256]{1,0:T(8,128)S(1)}, f32[12,256]{1,0:T(8,128)S(1)}, /*index=5*/f32[1,256]{1,0:T(1,128)S(1)}) custom-call(bf16[784,4096]{1,0:T(8,128)(2,1)S(1)} %shard_map.156.x_ref, bf16[64,4096]{1,0:T(8,128)(2,1)S(1)} %bitcast.23, ...), custom_call_target="tpu_custom_call" | custom-call | flops 4000000000 | bytes 8000000 | tf_op jit(solution)/shard_map/pallas_call | solution.py:52
  151.0 2.2 collective-permute-start.35
  153.2 1.4 shard_map.162.v_ref
  155.5 1.9 shard_map.165
  157.4 5.8 %shard_map.167.acc_ref = f32[784,768]{1,0:T(8,128)S(1)} custom-call(bf16[784,4096]{1,0:T(8,128)(2,1)S(1)} %shard_map.156.x_ref, bf16[1024,768]{1,0:T(8,128)(2,1)} %get-tuple-element.45.refs_0_, bf16[1024,768]{1,0:T(8,128)(2,1)} %collective-permute-done.28.refs_1_, bf16[1024,768]{1,0:T(8,128)(2,1)} %collective-permute-done.29.refs_2_), custom_call_target="tpu_custom_call" | custom-call | flops 3000000000 | bytes 8000000 | tf_op jit(solution)/shard_map/pallas_call | solution.py:52
  163.9 1.0 collective-permute-start.24
  165.0 1.9 shard_map.168.t_ref
  166.8 5.5 %shard_map.169.acc_ref = f32[784,768]{1,0:T(8,128)S(1)} custom-call(bf16[784,4096]{1,0:T(8,128)(2,1)S(1)} %shard_map.156.x_ref, bf16[1024,768]{1,0:T(8,128)(2,1)} %get-tuple-element.46.refs_0_, bf16[1024,768]{1,0:T(8,128)(2,1)S(1)} %collective-permute-done.32.refs_1_, bf16[1024,768]{1,0:T(8,128)(2,1)S(1)} %collective-permute-done.33.refs_2_), custom_call_target="tpu_custom_call" | custom-call | flops 3000000000 | bytes 8000000 | tf_op jit(solution)/shard_map/pallas_call | solution.py:52
  172.4 1.8 shard_map.170.b_ref
  174.6 1.2 collective-permute-start.25
  175.8 3.2 %shard_map.173 = (f32[192,4096]{1,0:T(8,128)S(1)}, f32[384,4096]{1,0:T(8,128)S(1)}) custom-call(bf16[768,256]{1,0:T(8,128)(2,1)S(1)} %shard_map.168.t_ref, bf16[768,256]{1,0:T(8,128)(2,1)S(1)} %shard_map.170.b_ref, bf16[512,4096]{1,0:T(8,128)(2,1)S(1)} %copy-done.1, bf16[512,4096]{1,0:T(8,128)(2,1)S(1)} %copy-done), custom_call_target="tpu_custom_call" | custom-call | flops 2000000000 | bytes 8000000 | tf_op jit(solution)/shard_map/pallas_call | solution.py:52
  179.0 1.6 collective-permute-start.27
  181.3 2.3 collective-permute-done.27
  184.3 1.6 shard_map.175
  185.9 9.0 %collective-permute-start.38 = (bf16[96,4096]{1,0:T(8,128)(2,1)S(1)}, bf16[96,4096]{1,0:T(8,128)(2,1)S(1)}, u32[]{:S(2)}, u32[]{:S(2)}) collective-permute-start(bf16[96,4096]{1,0:T(8,128)(2,1)S(1)} %get-tuple-element.54), channel_id=1, source_target_pairs={{0,1},{1,0},{2,3},{3,2},{4,5},{5,4},{6,7},{7,6},{8,9},{9,8},{10,11... | collective-permute-start | bytes 2359304 | tf_op jit(solution)/shard_map/ppermute | solution.py:35
  194.8 1.5 shard_map.171.acc_ref
  196.4 1.6 shard_map.172
  198.0 2.4 %shard_map.174 = (f32[192,4096]{1,0:T(8,128)S(1)}, bf16[192,4096]{1,0:T(8,128)(2,1)S(1)}) custom-call(bf16[768,512]{1,0:T(8,128)(2,1)S(1)} %shard_map.166.attn_ref, bf16[512,4096]{1,0:T(8,128)(2,1)S(1)} %copy-done, f32[384,4096]{1,0:T(8,128)S(1)} %get-tuple-element.49.acc_ref), custom_call_target="tpu_custom_call" | custom-call | flops 2000000000 | bytes 8000000 | tf_op jit(solution)/shard_map/pallas_call | solution.py:52
  201.2 1.8 collective-permute-start.43
  204.7 7.2 %collective-permute-done.43 = bf16[48,4096]{1,0:T(8,128)(2,1)S(1)} collective-permute-done((bf16[48,4096]{1,0:T(8,128)(2,1)S(1)}, bf16[48,4096]{1,0:T(8,128)(2,1)S(1)}, u32[]{:S(2)}, u32[]{:S(2)}) %collective-permute-start.43) | collective-permute-done | bytes 393248 | tf_op jit(solution)/shard_map/ppermute | solution.py:31
  211.9 2.7 %collective-permute-done.39 = bf16[48,4096]{1,0:T(8,128)(2,1)S(1)} collective-permute-done((bf16[48,4096]{1,0:T(8,128)(2,1)S(1)}, bf16[48,4096]{1,0:T(8,128)(2,1)S(1)}, u32[]{:S(2)}, u32[]{:S(2)}) %collective-permute-start.39) | collective-permute-done | bytes 393248 | tf_op jit(solution)/shard_map/ppermute | solution.py:31
  214.8 2.7 %collective-permute-start.44 = (bf16[48,4096]{1,0:T(8,128)(2,1)S(1)}, bf16[48,4096]{1,0:T(8,128)(2,1)S(1)}, u32[]{:S(2)}, u32[]{:S(2)}) collective-permute-start(bf16[48,4096]{1,0:T(8,128)(2,1)S(1)} %get-tuple-element.66), channel_id=1, source_target_pairs={{0,6},{2,0},{4,2},{6,4},{1,7},{3,1},{5,3},{7,5},{8,14},{10,8},{12,... | collective-permute-start | bytes 1179656 | tf_op jit(solution)/shard_map/ppermute | solution.py:31
  217.5 5.5 %collective-permute-done.41 = bf16[48,4096]{1,0:T(8,128)(2,1)S(1)} collective-permute-done((bf16[48,4096]{1,0:T(8,128)(2,1)S(1)}, bf16[48,4096]{1,0:T(8,128)(2,1)S(1)}, u32[]{:S(2)}, u32[]{:S(2)}) %collective-permute-start.41) | collective-permute-done | bytes 393248 | tf_op jit(solution)/shard_map/ppermute | solution.py:31
  223.0 8.4 %collective-permute-done.40 = bf16[48,4096]{1,0:T(8,128)(2,1)S(1)} collective-permute-done((bf16[48,4096]{1,0:T(8,128)(2,1)S(1)}, bf16[48,4096]{1,0:T(8,128)(2,1)S(1)}, u32[]{:S(2)}, u32[]{:S(2)}) %collective-permute-start.40) | collective-permute-done | bytes 393248 | tf_op jit(solution)/shard_map/ppermute | solution.py:31
  232.1 1.3 add_convert_fusion
  (155 shorter events, 13.5 us)
Async XLA Ops:
  1.8 9.5 %copy-start.25 = (bf16[256,256]{1,0:T(8,128)(2,1)S(1)}, bf16[256,256]{1,0:T(8,128)(2,1)}, u32[]{:S(2)}) copy-start(bf16[256,256]{1,0:T(8,128)(2,1)} %param.18) | copy-start | bytes 393220
  2.3 9.0 %copy-start.26 = (bf16[256,256]{1,0:T(8,128)(2,1)S(1)}, bf16[256,256]{1,0:T(8,128)(2,1)}, u32[]{:S(2)}) copy-start(bf16[256,256]{1,0:T(8,128)(2,1)} %param.19) | copy-start | bytes 393220
  2.3 9.0 %copy-start.23 = (bf16[256,512]{1,0:T(8,128)(2,1)S(1)}, bf16[256,512]{1,0:T(8,128)(2,1)}, u32[]{:S(2)}) copy-start(bf16[256,512]{1,0:T(8,128)(2,1)} %param.21) | copy-start | bytes 786436
  2.3 30.7 %copy-start.22 = (bf16[256,512]{1,0:T(8,128)(2,1)S(1)}, bf16[256,512]{1,0:T(8,128)(2,1)}, u32[]{:S(2)}) copy-start(bf16[256,512]{1,0:T(8,128)(2,1)} %param.22) | copy-start | bytes 786436
  2.3 6.3 %collective-permute-start = (bf16[16,4096]{1,0:T(8,128)(2,1)S(1)}, bf16[16,4096]{1,0:T(8,128)(2,1)S(1)}, u32[]{:S(2)}, u32[]{:S(2)}) collective-permute-start(bf16[16,4096]{1,0:T(8,128)(2,1)S(1)} %slice.172), channel_id=1, source_target_pairs={{0,8},{8,16},{16,24},{24,32},{32,40},{40,48},{48,56},{56,64},{64,7... | collective-permute-start | bytes 393224 | tf_op jit(solution)/shard_map/ppermute | solution.py:40
  8.7 24.4 %copy-start.21 = (bf16[256,512]{1,0:T(8,128)(2,1)S(1)}, bf16[256,512]{1,0:T(8,128)(2,1)}, u32[]{:S(2)}) copy-start(bf16[256,512]{1,0:T(8,128)(2,1)} %param.23) | copy-start | bytes 786436
  8.7 20.7 %collective-permute-start.2 = (bf16[112,4096]{1,0:T(8,128)(2,1)S(1)}, bf16[112,4096]{1,0:T(8,128)(2,1)S(1)}, u32[]{:S(2)}, u32[]{:S(2)}) collective-permute-start(bf16[112,4096]{1,0:T(8,128)(2,1)S(1)} %pad_maximum_fusion.own), channel_id=1, source_target_pairs={{0,6},{2,0},{4,2},{6,4},{1,7},{3,1},{5,3},{7,5},{8,14},{10,8},{12,... | collective-permute-start | bytes 2752520 | tf_op jit(solution)/shard_map/ppermute | solution.py:31
  11.3 21.7 %collective-permute-start.1 = (bf16[112,4096]{1,0:T(8,128)(2,1)S(1)}, bf16[112,4096]{1,0:T(8,128)(2,1)S(1)}, u32[]{:S(2)}, u32[]{:S(2)}) collective-permute-start(bf16[112,4096]{1,0:T(8,128)(2,1)S(1)} %pad_maximum_fusion.own), channel_id=1, source_target_pairs={{0,2},{2,4},{4,6},{6,0},{1,3},{3,5},{5,7},{7,1},{8,10},{10,12},{12... | collective-permute-start | bytes 2752520 | tf_op jit(solution)/shard_map/ppermute | solution.py:31
  11.4 28.7 %slice-start = ((bf16[256,512]{1,0:T(8,128)(2,1)}), bf16[256,256]{1,0:T(8,128)(2,1)S(1)}, s32[]{:S(2)}) async-start(bf16[256,512]{1,0:T(8,128)(2,1)} %param.23), calls=%async_computation | async-start | bytes 262144 | tf_op jit(solution)/shard_map/slice | solution.py:563
  11.4 28.7 %slice-start.1 = ((bf16[256,512]{1,0:T(8,128)(2,1)}), bf16[256,256]{1,0:T(8,128)(2,1)S(1)}, s32[]{:S(2)}) async-start(bf16[256,512]{1,0:T(8,128)(2,1)} %param.22), calls=%async_computation.1 | async-start | bytes 262144 | tf_op jit(solution)/shard_map/slice | solution.py:563
  11.4 28.7 %slice-start.2 = ((bf16[256,512]{1,0:T(8,128)(2,1)}), bf16[256,256]{1,0:T(8,128)(2,1)S(1)}, s32[]{:S(2)}) async-start(bf16[256,512]{1,0:T(8,128)(2,1)} %param.21), calls=%async_computation.2 | async-start | bytes 262144 | tf_op jit(solution)/shard_map/slice | solution.py:563
  11.4 28.7 %copy-start.24 = (bf16[256,512]{1,0:T(8,128)(2,1)S(1)}, bf16[256,512]{1,0:T(8,128)(2,1)}, u32[]{:S(2)}) copy-start(bf16[256,512]{1,0:T(8,128)(2,1)} %param.20) | copy-start | bytes 786436
  29.5 16.5 %collective-permute-start.4 = (bf16[64,4096]{1,0:T(8,128)(2,1)S(1)}, bf16[64,4096]{1,0:T(8,128)(2,1)S(1)}, u32[]{:S(2)}, u32[]{:S(2)}) collective-permute-start(bf16[64,4096]{1,0:T(8,128)(2,1)S(1)} %slice.174), channel_id=1, source_target_pairs={{0,6},{2,0},{4,2},{6,4},{1,7},{3,1},{5,3},{7,5},{8,14},{10,8},{12,... | collective-permute-start | bytes 1572872 | tf_op jit(solution)/shard_map/ppermute | solution.py:31
  33.1 9.3 %collective-permute-start.3 = (bf16[48,4096]{1,0:T(8,128)(2,1)S(1)}, bf16[48,4096]{1,0:T(8,128)(2,1)S(1)}, u32[]{:S(2)}, u32[]{:S(2)}) collective-permute-start(bf16[48,4096]{1,0:T(8,128)(2,1)S(1)} %slice.173), channel_id=1, source_target_pairs={{0,2},{2,4},{4,6},{6,0},{1,3},{3,5},{5,7},{7,1},{8,10},{10,12},{12... | collective-permute-start | bytes 1179656 | tf_op jit(solution)/shard_map/ppermute | solution.py:31
  33.2 19.3 %collective-permute-start.6 = (bf16[256,1280]{1,0:T(8,128)(2,1)S(1)}, bf16[256,1280]{1,0:T(8,128)(2,1)S(1)}, u32[]{:S(2)}, u32[]{:S(2)}) collective-permute-start(bf16[256,1280]{1,0:T(8,128)(2,1)S(1)} %slice_dynamic-update-slice_fusion.own), channel_id=1, source_target_pairs={{0,32},{32,64},{64,96},{96,0},{1,33},{33,65},{65,97},{97,1},{2,34}... | collective-permute-start | bytes 1966088 | tf_op jit(solution)/shard_map/ppermute | solution.py:31
  37.9 15.7 %collective-permute-start.7 = (bf16[256,1280]{1,0:T(8,128)(2,1)S(1)}, bf16[256,1280]{1,0:T(8,128)(2,1)S(1)}, u32[]{:S(2)}, u32[]{:S(2)}) collective-permute-start(bf16[256,1280]{1,0:T(8,128)(2,1)S(1)} %slice_dynamic-update-slice_fusion.own), channel_id=1, source_target_pairs={{0,96},{32,0},{64,32},{96,64},{1,97},{33,1},{65,33},{97,65},{2,98}... | collective-permute-start | bytes 1966088 | tf_op jit(solution)/shard_map/ppermute | solution.py:31
  40.2 15.7 %collective-permute-start.14 = (bf16[256,1280]{1,0:T(8,128)(2,1)S(1)}, bf16[256,1280]{1,0:T(8,128)(2,1)S(1)}, u32[]{:S(2)}, u32[]{:S(2)}) collective-permute-start(bf16[256,1280]{1,0:T(8,128)(2,1)S(1)} %pad_maximum_fusion.1.own), channel_id=1, source_target_pairs={{0,8},{8,16},{16,24},{24,0},{1,9},{9,17},{17,25},{25,1},{2,10},{10... | collective-permute-start | bytes 1966088 | tf_op jit(solution)/shard_map/ppermute | solution.py:31
  42.3 14.5 %collective-permute-start.15 = (bf16[256,1280]{1,0:T(8,128)(2,1)S(1)}, bf16[256,1280]{1,0:T(8,128)(2,1)S(1)}, u32[]{:S(2)}, u32[]{:S(2)}) collective-permute-start(bf16[256,1280]{1,0:T(8,128)(2,1)S(1)} %pad_maximum_fusion.1.own), channel_id=1, source_target_pairs={{0,24},{8,0},{16,8},{24,16},{1,25},{9,1},{17,9},{25,17},{2,26},{10... | collective-permute-start | bytes 1966088 | tf_op jit(solution)/shard_map/ppermute | solution.py:31
  48.1 81.5 %collective-permute-start.5 = (bf16[448,4096]{1,0:T(8,128)(2,1)}, bf16[448,4096]{1,0:T(8,128)(2,1)}, u32[]{:S(2)}, u32[]{:S(2)}) collective-permute-start(bf16[448,4096]{1,0:T(8,128)(2,1)} %shard_map.155.mine), channel_id=1, source_target_pairs={{0,1},{1,0},{2,3},{3,2},{4,5},{5,4},{6,7},{7,6},{8,9},{9,8},{10,11... | collective-permute-start | bytes 11010056 | tf_op jit(solution)/shard_map/ppermute | solution.py:35
  52.5 8.4 %collective-permute-start.8 = (bf16[128,1280]{1,0:T(8,128)(2,1)S(1)}, bf16[128,1280]{1,0:T(8,128)(2,1)S(1)}, u32[]{:S(2)}, u32[]{:S(2)}) collective-permute-start(bf16[128,1280]{1,0:T(8,128)(2,1)S(1)} %slice.175), channel_id=1, source_target_pairs={{0,32},{32,64},{64,96},{96,0},{1,33},{33,65},{65,97},{97,1},{2,34}... | collective-permute-start | bytes 983048 | tf_op jit(solution)/shard_map/ppermute | solution.py:31
  53.6 7.5 %collective-permute-start.9 = (bf16[128,1280]{1,0:T(8,128)(2,1)S(1)}, bf16[128,1280]{1,0:T(8,128)(2,1)S(1)}, u32[]{:S(2)}, u32[]{:S(2)}) collective-permute-start(bf16[128,1280]{1,0:T(8,128)(2,1)S(1)} %slice.176), channel_id=1, source_target_pairs={{0,96},{32,0},{64,32},{96,64},{1,97},{33,1},{65,33},{97,65},{2,98}... | collective-permute-start | bytes 983048 | tf_op jit(solution)/shard_map/ppermute | solution.py:31
  55.9 9.3 %collective-permute-start.16 = (bf16[128,1280]{1,0:T(8,128)(2,1)S(1)}, bf16[128,1280]{1,0:T(8,128)(2,1)S(1)}, u32[]{:S(2)}, u32[]{:S(2)}) collective-permute-start(bf16[128,1280]{1,0:T(8,128)(2,1)S(1)} %slice.179), channel_id=1, source_target_pairs={{0,8},{8,16},{16,24},{24,0},{1,9},{9,17},{17,25},{25,1},{2,10},{10... | collective-permute-start | bytes 983048 | tf_op jit(solution)/shard_map/ppermute | solution.py:31
  56.8 8.3 %collective-permute-start.17 = (bf16[128,1280]{1,0:T(8,128)(2,1)S(1)}, bf16[128,1280]{1,0:T(8,128)(2,1)S(1)}, u32[]{:S(2)}, u32[]{:S(2)}) collective-permute-start(bf16[128,1280]{1,0:T(8,128)(2,1)S(1)} %slice.180), channel_id=1, source_target_pairs={{0,24},{8,0},{16,8},{24,16},{1,25},{9,1},{17,9},{25,17},{2,26},{10... | collective-permute-start | bytes 983048 | tf_op jit(solution)/shard_map/ppermute | solution.py:31
  62.5 4.1 %copy-start.10 = (bf16[1024,512]{1,0:T(8,128)(2,1)}, bf16[1024,512]{1,0:T(8,128)(2,1)S(1)}, u32[]{:S(2)}) copy-start(bf16[1024,512]{1,0:T(8,128)(2,1)S(1)} %get-tuple-element.30.refs_0_) | copy-start | bytes 3145732
  62.5 31.8 %copy-start.27 = (bf16[3,512]{1,0:T(4,128)(2,1)S(1)}, bf16[3,512]{1,0:T(4,128)(2,1)}, u32[]{:S(2)}) copy-start(bf16[3,512]{1,0:T(4,128)(2,1)} %param.29) | copy-start | bytes 9220
  62.5 23.7 %collective-permute-start.10 = (bf16[1024,512]{1,0:T(8,128)(2,1)S(1)}, bf16[1024,512]{1,0:T(8,128)(2,1)S(1)}, u32[]{:S(2)}, u32[]{:S(2)}) collective-permute-start(bf16[1024,512]{1,0:T(8,128)(2,1)S(1)} %get-tuple-element.30.refs_0_), channel_id=1, source_target_pairs={{0,8},{8,16},{16,24},{24,0},{1,9},{9,17},{17,25},{25,1},{2,10},{10... | collective-permute-start | bytes 3145736 | tf_op jit(solution)/shard_map/ppermute | solution.py:31
  65.0 23.2 %collective-permute-start.11 = (bf16[1024,512]{1,0:T(8,128)(2,1)S(1)}, bf16[1024,512]{1,0:T(8,128)(2,1)S(1)}, u32[]{:S(2)}, u32[]{:S(2)}) collective-permute-start(bf16[1024,512]{1,0:T(8,128)(2,1)S(1)} %get-tuple-element.30.refs_0_), channel_id=1, source_target_pairs={{0,24},{8,0},{16,8},{24,16},{1,25},{9,1},{17,9},{25,17},{2,26},{10... | collective-permute-start | bytes 3145736 | tf_op jit(solution)/shard_map/ppermute | solution.py:31
  66.6 25.0 %collective-permute-start.18 = (bf16[1024,512]{1,0:T(8,128)(2,1)S(1)}, bf16[1024,512]{1,0:T(8,128)(2,1)S(1)}, u32[]{:S(2)}, u32[]{:S(2)}) collective-permute-start(bf16[1024,512]{1,0:T(8,128)(2,1)S(1)} %get-tuple-element.34.refs_0_), channel_id=1, source_target_pairs={{0,32},{32,64},{64,96},{96,0},{1,33},{33,65},{65,97},{97,1},{2,34}... | collective-permute-start | bytes 3145736 | tf_op jit(solution)/shard_map/ppermute | solution.py:31
  68.3 24.9 %collective-permute-start.19 = (bf16[1024,512]{1,0:T(8,128)(2,1)S(1)}, bf16[1024,512]{1,0:T(8,128)(2,1)S(1)}, u32[]{:S(2)}, u32[]{:S(2)}) collective-permute-start(bf16[1024,512]{1,0:T(8,128)(2,1)S(1)} %get-tuple-element.34.refs_0_), channel_id=1, source_target_pairs={{0,96},{32,0},{64,32},{96,64},{1,97},{33,1},{65,33},{97,65},{2,98}... | collective-permute-start | bytes 3145736 | tf_op jit(solution)/shard_map/ppermute | solution.py:31
  86.2 7.0 %copy-start.2 = (bf16[1024,512]{1,0:T(8,128)(2,1)}, bf16[1024,512]{1,0:T(8,128)(2,1)S(1)}, u32[]{:S(2)}) copy-start(bf16[1024,512]{1,0:T(8,128)(2,1)S(1)} %collective-permute-done.10.refs_1_) | copy-start | bytes 3145732
  86.2 33.7 %collective-permute-start.28 = (bf16[1024,768]{1,0:T(8,128)(2,1)}, bf16[1024,768]{1,0:T(8,128)(2,1)}, u32[]{:S(2)}, u32[]{:S(2)}) collective-permute-start(bf16[1024,768]{1,0:T(8,128)(2,1)} %get-tuple-element.45.refs_0_), channel_id=1, source_target_pairs={{0,8},{8,16},{16,24},{24,0},{1,9},{9,17},{17,25},{25,1},{2,10},{10... | collective-permute-start | bytes 4718600 | tf_op jit(solution)/shard_map/ppermute | solution.py:31
  88.2 5.1 %copy-start.4 = (bf16[1024,512]{1,0:T(8,128)(2,1)}, bf16[1024,512]{1,0:T(8,128)(2,1)S(1)}, u32[]{:S(2)}) copy-start(bf16[1024,512]{1,0:T(8,128)(2,1)S(1)} %collective-permute-done.11.refs_2_) | copy-start | bytes 3145732
  88.2 34.9 %collective-permute-start.29 = (bf16[1024,768]{1,0:T(8,128)(2,1)}, bf16[1024,768]{1,0:T(8,128)(2,1)}, u32[]{:S(2)}, u32[]{:S(2)}) collective-permute-start(bf16[1024,768]{1,0:T(8,128)(2,1)} %get-tuple-element.45.refs_0_), channel_id=1, source_target_pairs={{0,24},{8,0},{16,8},{24,16},{1,25},{9,1},{17,9},{25,17},{2,26},{10... | collective-permute-start | bytes 4718600 | tf_op jit(solution)/shard_map/ppermute | solution.py:31
  91.6 35.0 %collective-permute-start.32 = (bf16[1024,768]{1,0:T(8,128)(2,1)}, bf16[1024,768]{1,0:T(8,128)(2,1)S(1)}, u32[]{:S(2)}, u32[]{:S(2)}) collective-permute-start(bf16[1024,768]{1,0:T(8,128)(2,1)} %get-tuple-element.46.refs_0_), channel_id=1, source_target_pairs={{0,32},{32,64},{64,96},{96,0},{1,33},{33,65},{65,97},{97,1},{2,34}... | collective-permute-start | bytes 4718600 | tf_op jit(solution)/shard_map/ppermute | solution.py:31
  93.3 35.2 %collective-permute-start.33 = (bf16[1024,768]{1,0:T(8,128)(2,1)}, bf16[1024,768]{1,0:T(8,128)(2,1)S(1)}, u32[]{:S(2)}, u32[]{:S(2)}) collective-permute-start(bf16[1024,768]{1,0:T(8,128)(2,1)} %get-tuple-element.46.refs_0_), channel_id=1, source_target_pairs={{0,96},{32,0},{64,32},{96,64},{1,97},{33,1},{65,33},{97,65},{2,98}... | collective-permute-start | bytes 4718600 | tf_op jit(solution)/shard_map/ppermute | solution.py:31
  120.0 20.0 %collective-permute-start.12 = (bf16[512,512]{1,0:T(8,128)(2,1)S(1)}, bf16[512,512]{1,0:T(8,128)(2,1)S(1)}, u32[]{:S(2)}, u32[]{:S(2)}) collective-permute-start(bf16[512,512]{1,0:T(8,128)(2,1)S(1)} %slice.177), channel_id=1, source_target_pairs={{0,8},{8,16},{16,24},{24,0},{1,9},{9,17},{17,25},{25,1},{2,10},{10... | collective-permute-start | bytes 1572872 | tf_op jit(solution)/shard_map/ppermute | solution.py:31
  123.1 19.4 %collective-permute-start.13 = (bf16[512,512]{1,0:T(8,128)(2,1)S(1)}, bf16[512,512]{1,0:T(8,128)(2,1)S(1)}, u32[]{:S(2)}, u32[]{:S(2)}) collective-permute-start(bf16[512,512]{1,0:T(8,128)(2,1)S(1)} %slice.178), channel_id=1, source_target_pairs={{0,24},{8,0},{16,8},{24,16},{1,25},{9,1},{17,9},{25,17},{2,26},{10... | collective-permute-start | bytes 1572872 | tf_op jit(solution)/shard_map/ppermute | solution.py:31
  126.6 24.4 %collective-permute-start.20 = (bf16[512,512]{1,0:T(8,128)(2,1)S(1)}, bf16[512,512]{1,0:T(8,128)(2,1)S(1)}, u32[]{:S(2)}, u32[]{:S(2)}) collective-permute-start(bf16[512,512]{1,0:T(8,128)(2,1)S(1)} %slice.181), channel_id=1, source_target_pairs={{0,32},{32,64},{64,96},{96,0},{1,33},{33,65},{65,97},{97,1},{2,34}... | collective-permute-start | bytes 1572872 | tf_op jit(solution)/shard_map/ppermute | solution.py:31
  128.5 24.7 %collective-permute-start.21 = (bf16[512,512]{1,0:T(8,128)(2,1)S(1)}, bf16[512,512]{1,0:T(8,128)(2,1)S(1)}, u32[]{:S(2)}, u32[]{:S(2)}) collective-permute-start(bf16[512,512]{1,0:T(8,128)(2,1)S(1)} %slice.182), channel_id=1, source_target_pairs={{0,96},{32,0},{64,32},{96,64},{1,97},{33,1},{65,33},{97,65},{2,98}... | collective-permute-start | bytes 1572872 | tf_op jit(solution)/shard_map/ppermute | solution.py:31
  129.6 4.0 %copy-start.3 = (bf16[1024,512]{1,0:T(8,128)(2,1)S(1)}, bf16[1024,512]{1,0:T(8,128)(2,1)}, u32[]{:S(2)}) copy-start(bf16[1024,512]{1,0:T(8,128)(2,1)} %copy-done.2) | copy-start | bytes 3145732
  129.6 33.6 %collective-permute-start.30 = (bf16[512,768]{1,0:T(8,128)(2,1)S(1)}, bf16[512,768]{1,0:T(8,128)(2,1)S(1)}, u32[]{:S(2)}, u32[]{:S(2)}) collective-permute-start(bf16[512,768]{1,0:T(8,128)(2,1)S(1)} %slice.194), channel_id=1, source_target_pairs={{0,8},{8,16},{16,24},{24,0},{1,9},{9,17},{17,25},{25,1},{2,10},{10... | collective-permute-start | bytes 2359304 | tf_op jit(solution)/shard_map/ppermute | solution.py:31
  139.9 4.6 %copy-start.17 = (bf16[4096,64]{0,1:T(8,128)(2,1)S(1)}, bf16[4096,64]{0,1:T(8,128)(2,1)}, u32[]{:S(2)}) copy-start(bf16[4096,64]{0,1:T(8,128)(2,1)} %param.24) | copy-start | bytes 1572868
  139.9 4.6 %copy-start.18 = (bf16[64,256]{1,0:T(8,128)(2,1)S(1)}, bf16[64,256]{1,0:T(8,128)(2,1)}, u32[]{:S(2)}) copy-start(bf16[64,256]{1,0:T(8,128)(2,1)} %right_ref.1) | copy-start | bytes 98308
  139.9 4.6 %copy-start.19 = (f32[2,768]{1,0:T(2,128)S(1)}, f32[2,768]{1,0:T(2,128)}, u32[]{:S(2)}) copy-start(f32[2,768]{1,0:T(2,128)} %spike_ref.1) | copy-start | bytes 18436
  139.9 4.6 %copy-start.20 = (f32[256]{0:T(256)S(1)}, f32[256]{0:T(256)}, u32[]{:S(2)}) copy-start(f32[256]{0:T(256)} %param.26) | copy-start | bytes 3076
  140.0 24.0 %collective-permute-start.31 = (bf16[512,768]{1,0:T(8,128)(2,1)S(1)}, bf16[512,768]{1,0:T(8,128)(2,1)S(1)}, u32[]{:S(2)}, u32[]{:S(2)}) collective-permute-start(bf16[512,768]{1,0:T(8,128)(2,1)S(1)} %slice.195), channel_id=1, source_target_pairs={{0,24},{8,0},{16,8},{24,16},{1,25},{9,1},{17,9},{25,17},{2,26},{10... | collective-permute-start | bytes 2359304 | tf_op jit(solution)/shard_map/ppermute | solution.py:31
  142.6 29.8 %collective-permute-start.34 = (bf16[512,768]{1,0:T(8,128)(2,1)S(1)}, bf16[512,768]{1,0:T(8,128)(2,1)S(1)}, u32[]{:S(2)}, u32[]{:S(2)}) collective-permute-start(bf16[512,768]{1,0:T(8,128)(2,1)S(1)} %slice.196), channel_id=1, source_target_pairs={{0,32},{32,64},{64,96},{96,0},{1,33},{33,65},{65,97},{97,1},{2,34}... | collective-permute-start | bytes 2359304 | tf_op jit(solution)/shard_map/ppermute | solution.py:31
  151.0 21.4 %collective-permute-start.35 = (bf16[512,768]{1,0:T(8,128)(2,1)S(1)}, bf16[512,768]{1,0:T(8,128)(2,1)S(1)}, u32[]{:S(2)}, u32[]{:S(2)}) collective-permute-start(bf16[512,768]{1,0:T(8,128)(2,1)S(1)} %slice.197), channel_id=1, source_target_pairs={{0,96},{32,0},{64,32},{96,64},{1,97},{33,1},{65,33},{97,65},{2,98}... | collective-permute-start | bytes 2359304 | tf_op jit(solution)/shard_map/ppermute | solution.py:31
  155.4 18.8 %collective-permute-start.22 = (bf16[2,272,128]{2,1,0:T(8,128)(2,1)S(1)}, bf16[2,272,128]{2,1,0:T(8,128)(2,1)S(1)}, u32[]{:S(2)}, u32[]{:S(2)}) collective-permute-start(bf16[2,272,128]{2,1,0:T(8,128)(2,1)S(1)} %pad_maximum_fusion.2), channel_id=1, source_target_pairs={{0,24},{8,0},{16,8},{24,16},{1,25},{9,1},{17,9},{25,17},{2,26},{10... | collective-permute-start | bytes 417800 | tf_op jit(solution)/shard_map/ppermute | solution.py:31
  163.2 11.0 %collective-permute-start.23 = (bf16[2,272,128]{2,1,0:T(8,128)(2,1)S(1)}, bf16[2,272,128]{2,1,0:T(8,128)(2,1)S(1)}, u32[]{:S(2)}, u32[]{:S(2)}) collective-permute-start(bf16[2,272,128]{2,1,0:T(8,128)(2,1)S(1)} %pad_maximum_fusion.2), channel_id=1, source_target_pairs={{0,16},{8,24},{16,0},{24,8},{1,17},{9,25},{17,1},{25,9},{2,18},{10... | collective-permute-start | bytes 417800 | tf_op jit(solution)/shard_map/ppermute | solution.py:31
  163.9 10.3 %collective-permute-start.24 = (bf16[2,272,128]{2,1,0:T(8,128)(2,1)S(1)}, bf16[2,272,128]{2,1,0:T(8,128)(2,1)S(1)}, u32[]{:S(2)}, u32[]{:S(2)}) collective-permute-start(bf16[2,272,128]{2,1,0:T(8,128)(2,1)S(1)} %pad_maximum_fusion.2), channel_id=1, source_target_pairs={{0,8},{8,16},{16,24},{24,0},{1,9},{9,17},{17,25},{25,1},{2,10},{10... | collective-permute-start | bytes 417800 | tf_op jit(solution)/shard_map/ppermute | solution.py:31
  174.6 6.7 %collective-permute-start.26 = (bf16[2,272,128]{2,1,0:T(8,128)(2,1)S(1)}, bf16[2,272,128]{2,1,0:T(8,128)(2,1)S(1)}, u32[]{:S(2)}, u32[]{:S(2)}) collective-permute-start(bf16[2,272,128]{2,1,0:T(8,128)(2,1)S(1)} %pad_maximum_fusion.3), channel_id=1, source_target_pairs={{0,32},{32,64},{64,96},{96,0},{1,33},{33,65},{65,97},{97,1},{2,34}... | collective-permute-start | bytes 417800 | tf_op jit(solution)/shard_map/ppermute | solution.py:31
  174.6 6.6 %collective-permute-start.25 = (bf16[2,272,128]{2,1,0:T(8,128)(2,1)S(1)}, bf16[2,272,128]{2,1,0:T(8,128)(2,1)S(1)}, u32[]{:S(2)}, u32[]{:S(2)}) collective-permute-start(bf16[2,272,128]{2,1,0:T(8,128)(2,1)S(1)} %pad_maximum_fusion.3), channel_id=1, source_target_pairs={{0,64},{32,96},{64,0},{96,32},{1,65},{33,97},{65,1},{97,33},{2,66}... | collective-permute-start | bytes 417800 | tf_op jit(solution)/shard_map/ppermute | solution.py:31
  179.0 4.7 %copy-start.16 = (bf16[2,256]{1,0:T(2,128)(2,1)S(1)}, bf16[2,256]{1,0:T(2,128)(2,1)}, u32[]{:S(2)}) copy-start(bf16[2,256]{1,0:T(2,128)(2,1)} %gain_ref.3) | copy-start | bytes 3076
  179.0 4.6 %collective-permute-start.27 = (bf16[2,272,128]{2,1,0:T(8,128)(2,1)S(1)}, bf16[2,272,128]{2,1,0:T(8,128)(2,1)S(1)}, u32[]{:S(2)}, u32[]{:S(2)}) collective-permute-start(bf16[2,272,128]{2,1,0:T(8,128)(2,1)S(1)} %pad_maximum_fusion.3), channel_id=1, source_target_pairs={{0,96},{32,0},{64,32},{96,64},{1,97},{33,1},{65,33},{97,65},{2,98}... | collective-permute-start | bytes 417800 | tf_op jit(solution)/shard_map/ppermute | solution.py:31
  185.9 15.1 %collective-permute-start.38 = (bf16[96,4096]{1,0:T(8,128)(2,1)S(1)}, bf16[96,4096]{1,0:T(8,128)(2,1)S(1)}, u32[]{:S(2)}, u32[]{:S(2)}) collective-permute-start(bf16[96,4096]{1,0:T(8,128)(2,1)S(1)} %get-tuple-element.54), channel_id=1, source_target_pairs={{0,1},{1,0},{2,3},{3,2},{4,5},{5,4},{6,7},{7,6},{8,9},{9,8},{10,11... | collective-permute-start | bytes 2359304 | tf_op jit(solution)/shard_map/ppermute | solution.py:35
  197.9 19.6 %collective-permute-start.36 = (bf16[96,4096]{1,0:T(8,128)(2,1)S(1)}, bf16[96,4096]{1,0:T(8,128)(2,1)S(1)}, u32[]{:S(2)}, u32[]{:S(2)}) collective-permute-start(bf16[96,4096]{1,0:T(8,128)(2,1)S(1)} %get-tuple-element.48), channel_id=1, source_target_pairs={{0,1},{1,0},{2,3},{3,2},{4,5},{5,4},{6,7},{7,6},{8,9},{9,8},{10,11... | collective-permute-start | bytes 2359304 | tf_op jit(solution)/shard_map/ppermute | solution.py:35
  200.4 3.6 %collective-permute-start.37 = (bf16[192,4096]{1,0:T(8,128)(2,1)S(1)}, bf16[192,4096]{1,0:T(8,128)(2,1)S(1)}, u32[]{:S(2)}, u32[]{:S(2)}) collective-permute-start(bf16[192,4096]{1,0:T(8,128)(2,1)S(1)} %get-tuple-element.51), channel_id=1, source_target_pairs={{0,1},{1,0},{2,3},{3,2},{4,5},{5,4},{6,7},{7,6},{8,9},{9,8},{10,11... | collective-permute-start | bytes 4718600 | tf_op jit(solution)/shard_map/ppermute | solution.py:35
  201.2 10.7 %collective-permute-start.43 = (bf16[48,4096]{1,0:T(8,128)(2,1)S(1)}, bf16[48,4096]{1,0:T(8,128)(2,1)S(1)}, u32[]{:S(2)}, u32[]{:S(2)}) collective-permute-start(bf16[48,4096]{1,0:T(8,128)(2,1)S(1)} %get-tuple-element.70), channel_id=1, source_target_pairs={{0,6},{2,0},{4,2},{6,4},{1,7},{3,1},{5,3},{7,5},{8,14},{10,8},{12,... | collective-permute-start | bytes 1179656 | tf_op jit(solution)/shard_map/ppermute | solution.py:31
  203.0 11.6 %collective-permute-start.39 = (bf16[48,4096]{1,0:T(8,128)(2,1)S(1)}, bf16[48,4096]{1,0:T(8,128)(2,1)S(1)}, u32[]{:S(2)}, u32[]{:S(2)}) collective-permute-start(bf16[48,4096]{1,0:T(8,128)(2,1)S(1)} %get-tuple-element.71), channel_id=1, source_target_pairs={{0,2},{2,4},{4,6},{6,0},{1,3},{3,5},{5,7},{7,1},{8,10},{10,12},{12... | collective-permute-start | bytes 1179656 | tf_op jit(solution)/shard_map/ppermute | solution.py:31
  204.6 18.4 %collective-permute-start.41 = (bf16[48,4096]{1,0:T(8,128)(2,1)S(1)}, bf16[48,4096]{1,0:T(8,128)(2,1)S(1)}, u32[]{:S(2)}, u32[]{:S(2)}) collective-permute-start(bf16[48,4096]{1,0:T(8,128)(2,1)S(1)} %get-tuple-element.69), channel_id=1, source_target_pairs={{0,2},{2,4},{4,6},{6,0},{1,3},{3,5},{5,7},{7,1},{8,10},{10,12},{12... | collective-permute-start | bytes 1179656 | tf_op jit(solution)/shard_map/ppermute | solution.py:31
  214.7 16.7 %collective-permute-start.40 = (bf16[48,4096]{1,0:T(8,128)(2,1)S(1)}, bf16[48,4096]{1,0:T(8,128)(2,1)S(1)}, u32[]{:S(2)}, u32[]{:S(2)}) collective-permute-start(bf16[48,4096]{1,0:T(8,128)(2,1)S(1)} %get-tuple-element.67), channel_id=1, source_target_pairs={{0,2},{2,4},{4,6},{6,0},{1,3},{3,5},{5,7},{7,1},{8,10},{10,12},{12... | collective-permute-start | bytes 1179656 | tf_op jit(solution)/shard_map/ppermute | solution.py:31
  214.8 16.6 %collective-permute-start.44 = (bf16[48,4096]{1,0:T(8,128)(2,1)S(1)}, bf16[48,4096]{1,0:T(8,128)(2,1)S(1)}, u32[]{:S(2)}, u32[]{:S(2)}) collective-permute-start(bf16[48,4096]{1,0:T(8,128)(2,1)S(1)} %get-tuple-element.66), channel_id=1, source_target_pairs={{0,6},{2,0},{4,2},{6,4},{1,7},{3,1},{5,3},{7,5},{8,14},{10,8},{12,... | collective-permute-start | bytes 1179656 | tf_op jit(solution)/shard_map/ppermute | solution.py:31
  217.5 14.7 %collective-permute-start.42 = (bf16[48,4096]{1,0:T(8,128)(2,1)S(1)}, bf16[48,4096]{1,0:T(8,128)(2,1)S(1)}, u32[]{:S(2)}, u32[]{:S(2)}) collective-permute-start(bf16[48,4096]{1,0:T(8,128)(2,1)S(1)} %get-tuple-element.68), channel_id=1, source_target_pairs={{0,6},{2,0},{4,2},{6,4},{1,7},{3,1},{5,3},{7,5},{8,14},{10,8},{12,... | collective-permute-start | bytes 1179656 | tf_op jit(solution)/shard_map/ppermute | solution.py:31
  (12 other events, 29.5 us)
